TPU v7x, 32 devices: a whole 2x2x4 slice. The times are simulated.
32 devices in a mesh: kv: 16 (over z, y, x), tp: 2 (over core).
Axes of the slice: x: 2, y: 2, z: 4, core: 2. Of those that a mesh axis runs over, the one named last changes fastest.
Arguments:
- tokens: bfloat16 [16, 4096], P(None, ('kv', 'tp')), may hold values from -12 to 12
- lengths: int32 [16], replicated, may hold values from 1 to 2048, 10922 in all
- attn_gain: bfloat16 [4096], P('kv'), may hold values from 0.099609375 to 1.8984375
- w_query: bfloat16 [4096, 2048], P('kv', 'tp'), may hold values from -0.09375 to 0.09375
- w_key: bfloat16 [4096, 2048], P('kv', 'tp'), may hold values from -0.09375 to 0.09375
- w_value: bfloat16 [4096, 4096], P('kv', 'tp'), may hold values from -0.09375 to 0.09375
- w_gate: bfloat16 [4096, 4096], P('kv', 'tp'), may hold values from -0.09375 to 0.09375
- decay_rate: float32 [32], P('tp'), may hold values from 4.8828125e-05 to 0.05
- key_cache: bfloat16 [16, 2048, 2048], P(None, 'kv', 'tp'), may hold values from -6 to 6
- value_cache: bfloat16 [16, 2048, 4096], P(None, 'kv', 'tp'), may hold values from -6 to 6
- head_gain: bfloat16 [4096], P('tp'), may hold values from 0.099609375 to 1.8984375
- w_output: bfloat16 [4096, 4096], P('tp', 'kv'), may hold values from -0.09375 to 0.09375
- mlp_gain: bfloat16 [4096], replicated, may hold values from 0.099609375 to 1.8984375
- w_up: bfloat16 [4096, 16384], P(None, ('kv', 'tp')), may hold values from -0.09375 to 0.09375
- w_down: bfloat16 [16384, 4096], P(('kv', 'tp')), may hold values from -0.09375 to 0.09375
Outputs:
- layer_out: bfloat16 [16, 4096], P(None, ('kv', 'tp'))
Inputs may be any that keep to these rules, and one draw needn't show every extreme that they name: Sequence s has lengths[s] live cache positions, 0 to lengths[s] - 1, and its new token stands at position lengths[s]; the longest fills all 2048 positions.
All inputs are finite; a program needn't handle non-finite values.
Results may differ from a plain program's by a relative error of at most 0.012.
Values may be sent and summed in bfloat16 or wider, within the bound.
No kernel may reach another device: no remote copies, remote signals or barrier semaphores. Data moves between devices by JAX's collectives and lax.ppermute only.
A program may use at most 64 MiB of HBM per device.

v0:
```python
import jax
import jax.numpy as jnp
from jax import lax
from jax.sharding import PartitionSpec as P

WIDTH = 4096
HEAD_KEY = 64
HEAD_VALUE = 128


EPS = 1e-05
THETA = 10000.0


def rotate(flattened, position):
    row_count = flattened.shape[0]
    grouped = flattened.reshape(row_count, -1, HEAD_KEY)
    halfway = HEAD_KEY // 2
    inverse = jnp.power(THETA, -jnp.arange(halfway, dtype=jnp.float32) / halfway)
    angles = position.astype(jnp.float32)[:, None] * inverse[None, :]
    cosine = jnp.cos(angles)[:, None, :]
    sine_part = jnp.sin(angles)[:, None, :]
    first_half = grouped[..., :halfway]
    second_half = grouped[..., halfway:]
    turned = jnp.concatenate(
        [
            first_half * cosine - second_half * sine_part,
            second_half * cosine + first_half * sine_part,
        ],
        -1,
    )
    return turned.reshape(row_count, -1)


def affine(product_sum, column, average, inverse_std):
    return inverse_std[:, None] * (product_sum - average[:, None] * column[None, :])


def on_device(
    tokens,
    lengths,
    attn_gain,
    w_query,
    w_key,
    w_value,
    w_gate,
    decay_rate,
    key_cache,
    value_cache,
    head_gain,
    w_output,
    mlp_gain,
    w_up,
    w_down,
):
    seq_count = tokens.shape[0]
    head_count = decay_rate.shape[0]
    span_rows = key_cache.shape[1]
    block_cols = lax.all_gather(tokens, "tp", axis=1, tiled=True)
    widened = block_cols.astype(jnp.float32)
    scaled = (widened * attn_gain.astype(jnp.float32)).astype(jnp.bfloat16)
    gain_row = attn_gain[None, :]
    part_query = jnp.dot(scaled, w_query, preferred_element_type=jnp.float32)
    part_key = jnp.dot(scaled, w_key, preferred_element_type=jnp.float32)
    part_value = jnp.dot(scaled, w_value, preferred_element_type=jnp.float32)
    part_gate = jnp.dot(scaled, w_gate, preferred_element_type=jnp.float32)
    col_query = jnp.dot(gain_row, w_query, preferred_element_type=jnp.float32)[0]
    col_key = jnp.dot(gain_row, w_key, preferred_element_type=jnp.float32)[0]
    col_value = jnp.dot(gain_row, w_value, preferred_element_type=jnp.float32)[0]
    col_gate = jnp.dot(gain_row, w_gate, preferred_element_type=jnp.float32)[0]
    (
        sum_query,
        sum_key,
        sum_value,
        sum_gate,
        csum_query,
        csum_key,
        csum_value,
        csum_gate,
        first_moment,
        second_moment,
    ) = lax.psum(
        (
            part_query,
            part_key,
            part_value,
            part_gate,
            col_query,
            col_key,
            col_value,
            col_gate,
            jnp.sum(widened, -1),
            jnp.sum(widened * widened, -1),
        ),
        "kv",
    )
    average = first_moment / WIDTH
    inverse_std = lax.rsqrt(second_moment / WIDTH - average * average + EPS)
    query_rows = rotate(affine(sum_query, csum_query, average, inverse_std), lengths).astype(
        jnp.bfloat16
    )
    new_key = rotate(affine(sum_key, csum_key, average, inverse_std), lengths).astype(jnp.bfloat16)
    new_value = affine(sum_value, csum_value, average, inverse_std).astype(jnp.bfloat16)
    gate_value = affine(sum_gate, csum_gate, average, inverse_std)
    queries = query_rows.reshape(seq_count, head_count, HEAD_KEY)
    keys_local = key_cache.reshape(seq_count, span_rows, head_count, HEAD_KEY)
    values_local = value_cache.reshape(seq_count, span_rows, head_count, HEAD_VALUE)
    scores = jnp.einsum(
        "bhd,bjhd->bhj", queries, keys_local, preferred_element_type=jnp.float32
    ) * HEAD_KEY ** (-0.5)
    places = lax.axis_index("kv") * span_rows + jnp.arange(span_rows, dtype=jnp.int32)
    distance = jnp.maximum(lengths[:, None] - places[None, :], 0).astype(jnp.float32)
    live_mask = (places[None, :] < lengths[:, None])[:, None, :]
    weights = jnp.where(live_mask, jnp.exp(-decay_rate[None, :, None] * distance[:, None, :]), 0.0)
    coefficients = (scores * weights).astype(jnp.bfloat16)
    partial_out = jnp.einsum(
        "bhj,bjhe->bhe", coefficients, values_local, preferred_element_type=jnp.float32
    )
    cached = lax.psum(partial_out, "kv")
    own_score = jnp.sum(
        queries.astype(jnp.float32)
        * new_key.reshape(seq_count, head_count, HEAD_KEY).astype(jnp.float32),
        -1,
    ) * HEAD_KEY ** (-0.5)
    retained = cached + own_score[:, :, None] * new_value.reshape(
        seq_count, head_count, HEAD_VALUE
    ).astype(jnp.float32)
    centered = retained - jnp.mean(retained, -1, keepdims=True)
    normed = (
        centered
        * lax.rsqrt(jnp.mean(centered * centered, -1, keepdims=True) + EPS)
        * head_gain.reshape(head_count, HEAD_VALUE).astype(jnp.float32)
    )
    gated_out = (jax.nn.silu(gate_value) * normed.reshape(seq_count, -1)).astype(jnp.bfloat16)
    partial_branch = jnp.dot(gated_out, w_output, preferred_element_type=jnp.float32)
    branch = lax.psum_scatter(
        partial_branch.astype(jnp.bfloat16), "tp", scatter_dimension=1, tiled=True
    ).astype(jnp.float32)
    own_residual = (tokens.astype(jnp.float32) + branch).astype(jnp.bfloat16)
    piece_wide = lax.all_gather(own_residual, ("kv", "tp"), axis=1, tiled=True).astype(jnp.float32)
    scaled_piece = (piece_wide * mlp_gain.astype(jnp.float32)).astype(jnp.bfloat16)
    totals = (
        jnp.dot(scaled_piece, w_up, preferred_element_type=jnp.float32),
        jnp.sum(piece_wide, -1),
        jnp.sum(piece_wide * piece_wide, -1),
    )
    accumulated, first_sum, second_sum = totals
    mid_average = first_sum / WIDTH
    mid_inverse = lax.rsqrt(second_sum / WIDTH - mid_average * mid_average + EPS)
    column_up = jnp.dot(mlp_gain[None, :], w_up, preferred_element_type=jnp.float32)[0]
    hidden = jnp.square(
        jax.nn.relu(affine(accumulated, column_up, mid_average, mid_inverse))
    ).astype(jnp.bfloat16)
    down_terms = jnp.dot(hidden, w_down, preferred_element_type=jnp.float32)
    kv_block = lax.psum_scatter(down_terms, "kv", scatter_dimension=1, tiled=True)
    mixer_sum = lax.psum_scatter(kv_block, "tp", scatter_dimension=1, tiled=True)
    return (own_residual.astype(jnp.float32) + mixer_sum).astype(jnp.bfloat16)


def solution(mesh):
    in_specs = (
        P(None, ("kv", "tp")),
        P(),
        P("kv"),
        P("kv", "tp"),
        P("kv", "tp"),
        P("kv", "tp"),
        P("kv", "tp"),
        P("tp"),
        P(None, "kv", "tp"),
        P(None, "kv", "tp"),
        P("tp"),
        P("tp", "kv"),
        P(),
        P(None, ("kv", "tp")),
        P(("kv", "tp"), None),
    )
    out_specs = P(None, ("kv", "tp"))
    return jax.shard_map(
        on_device, mesh=mesh, in_specs=in_specs, out_specs=out_specs, check_vma=False
    )
```

profile of v0, /device:TPU:0, one launch (start us, length us, event | category | flops | bytes accessed | tf_op | source)
XLA Modules:
  0.0 387.7 jit_solution(13604022745507007239)
XLA Ops:
  6.5 2.3 all_gather.6
  8.9 0.7 convert_element_type.87
  9.5 1.8 fusion.36
  11.6 0.7 reshape.195
  12.2 0.7 convert_element_type.89
  12.9 0.7 maximum_convert_fusion
  13.6 0.7 broadcast_compare_fusion
  14.4 1.2 fusion.44
  15.8 0.9 fusion.32
  16.7 1.5 fusion.43
  18.2 0.9 fusion.38
  19.3 0.8 fusion.34
  20.2 78.5 %all-reduce = (f32[1024]{0:T(1024)S(1)}, f32[16]{0:T(128)S(1)}, f32[16]{0:T(128)S(1)}, f32[2048]{0:T(1024)S(1)}, f32[1024]{0:T(1024)S(1)}, /*index=5*/f32[2048]{0:T(1024)S(1)}) all-reduce(f32[1024]{0:T(1024)S(1)} %bitcast.62, f32[16]{0:T(128)S(1)} %get-tuple-element.8, ...), channel_id=1, replica_groups=mesh['kv'=16,'tp'=2] {'kv'}, use_global_device_ids=true, to_apply=%region_7.0 | all-reduce | flops 6176 | bytes 49408 | tf_op jit(solution)/shard_map/psum | solution.py:82
  98.7 6.4 %copy.17 = bf16[16,128,1024]{1,2,0:T(8,128)(2,1)} copy(bf16[16,128,1024]{2,1,0:T(8,128)(2,1)} %param.23) | data formatting | bytes 8388608 | tf_op args[8]
  105.1 13.9 %all-reduce.5.cloned.1.call-done = f32[16,1024]{1,0:T(8,128)} async-done(((f32[16,1024]{1,0:T(8,128)}), f32[16,1024]{1,0:T(8,128)}) %all-reduce.5.cloned.1.call-update) | async-done | bytes 65552 | tf_op jit(solution)/shard_map/psum | solution.py:82
  119.1 0.9 subtract_multiply_fusion.1
  120.3 3.4 fusion.14
  123.8 6.4 %fusion = f32[16,16,1,128]{3,2,1,0:T(1,128)} fusion(bf16[16,16,128,1]{2,1,0,3:T(8,128)(2,1)S(1)} %fusion.18, bf16[16,128,2048]{2,1,0:T(8,128)(2,1)} %param.24), kind=kOutput, calls=%fused_computation | convolution fusion | flops 8388608 | bytes 8585216 | tf_op jit(solution)/shard_map/bhj,bjhe->bhe/dot_general | solution.py:116
  130.3 109.1 %all-reduce.7.cloned.1.call-done = (f32[16,16,128]{2,1,0:T(8,128)}, f32[16,2048]{1,0:T(8,128)}, f32[16,1024]{1,0:T(8,128)}, f32[16,2048]{1,0:T(8,128)}) async-done(((f32[16,16,128]{2,1,0:T(8,128)}, f32[16,2048]{1,0:T(8,128)}, f32[16,1024]{1,0:T(8,128)}, f32[16,2048]{1,0:T(8,128)}), (f32[16,16,128]{2,1,0:T(8,128)}, f32[16,2048]{1,0:T(8,128)}, f32[16,1024]{1,0:T(8,128)}, ...) | async-done | bytes 458768 | tf_op jit(solution)/shard_map/psum | solution.py:119
  239.5 0.9 subtract_multiply_fusion
  240.8 1.0 convert_bitcast_fusion
  241.9 1.0 fusion.42
  243.3 1.2 convolution_convert_fusion
  244.5 0.7 copy.23
  245.4 2.8 fusion.47
  248.2 3.9 %reduce-scatter.10.cloned.1.call-done = bf16[128,16]{1,0:T(8,128)(2,1)} async-done(((bf16[256,16]{1,0:T(8,128)(2,1)}), bf16[128,16]{1,0:T(8,128)(2,1)}) %reduce-scatter.10.cloned.1.call-update) | async-done | bytes 4112
  252.1 0.8 copy.24
  253.0 42.0 %all_gather.7 = bf16[16,4096]{1,0:T(8,128)(2,1)S(1)} all-gather(bf16[16,128]{1,0:T(8,128)(2,1)S(1)} %add_convert_fusion.3), channel_id=1, replica_groups=mesh['kv'=16,'tp'=2] {'kv','tp'}, dimensions={1}, use_global_device_ids=true | all-gather | bytes 135168 | tf_op jit(solution)/shard_map/all_gather | solution.py:140
  295.1 5.5 %fusion.7 = f32[16,4096]{1,0:T(8,128)} fusion(bf16[512,4096]{1,0:T(8,128)(2,1)} %param.29, bf16[4096,512]{1,0:T(8,128)(2,1)} %param.28, bf16[16,4096]{1,0:T(8,128)(2,1)S(1)} %all_gather.7, f32[4096]{0:T(1024)S(1)} %convert_element_type.105, f32[512]{0:T(512)S(1)} %bitcast.64, f32[16]{0:T(128)S(1)} %get-tuple-element.28, f32[16]{0:T(128)S(1)} %get-tuple-element.27), kind=kOutput, calls=%fused_computation.8 | convolution fusion | flops 134463488 | bytes 8800384 | tf_op jit(solution)/shard_map/dot_general | solution.py:154
  300.7 73.3 %reduce-scatter.6.cloned.1.call-done = f32[16,256]{1,0:T(8,128)} async-done(((f32[16,4096]{1,0:T(8,128)}), f32[16,256]{1,0:T(8,128)}) %reduce-scatter.6.cloned.1.call-update) | async-done | bytes 16400 | tf_op jit(solution)/shard_map/reduce_scatter | solution.py:155
  374.0 5.9 %reduce-scatter.8.cloned.1.call-done = f32[16,128]{1,0:T(8,128)} async-done(((f32[16,256]{1,0:T(8,128)}), f32[16,128]{1,0:T(8,128)}) %reduce-scatter.8.cloned.1.call-update) | async-done | bytes 8208 | tf_op jit(solution)/shard_map/reduce_scatter | solution.py:156
  379.9 1.3 add_convert_fusion.2
  (54 shorter events, 2.4 us)
Async XLA Ops:
  6.5 9.1 %copy-start = (bf16[256,2048]{1,0:T(8,128)(2,1)S(1)}, bf16[256,2048]{1,0:T(8,128)(2,1)}, u32[]{:S(2)}) copy-start(bf16[256,2048]{1,0:T(8,128)(2,1)} %param.20) | copy-start | bytes 3145732
  6.5 11.7 %copy-start.1 = (bf16[256,2048]{1,0:T(8,128)(2,1)S(1)}, bf16[256,2048]{1,0:T(8,128)(2,1)}, u32[]{:S(2)}) copy-start(bf16[256,2048]{1,0:T(8,128)(2,1)} %param.21) | copy-start | bytes 3145732
  6.5 12.6 %copy-start.2 = (bf16[256,1024]{1,0:T(8,128)(2,1)S(1)}, bf16[256,1024]{1,0:T(8,128)(2,1)}, u32[]{:S(2)}) copy-start(bf16[256,1024]{1,0:T(8,128)(2,1)} %param.19) | copy-start | bytes 1572868
  6.5 112.5 %all-reduce.5.cloned.1.call-start = ((), (), s32[]{:S(2)}) async-start(), calls=%async_computation.3 | async-start | bytes 131072 | tf_op jit(solution)/shard_map/psum | solution.py:82
  11.4 228.1 %all-reduce.7.cloned.1.call-start = ((), (), s32[]{:S(2)}) async-start(), calls=%async_computation.7 | async-start | bytes 917504 | tf_op jit(solution)/shard_map/psum | solution.py:119
  98.7 6.4 %copy-start.7 = (f32[16]{0:T(128)S(1)}, f32[16]{0:T(128)}, u32[]{:S(2)}) copy-start(f32[16]{0:T(128)} %param.22) | copy-start | bytes 196
  123.8 6.5 %copy-start.4 = (bf16[4096]{0:T(1024)(128)(2,1)S(1)}, bf16[4096]{0:T(1024)(128)(2,1)}, u32[]{:S(2)}) copy-start(bf16[4096]{0:T(1024)(128)(2,1)} %param.27) | copy-start | bytes 24580
  123.8 6.5 %copy-start.6 = (bf16[2048]{0:T(1024)(128)(2,1)S(1)}, bf16[2048]{0:T(1024)(128)(2,1)}, u32[]{:S(2)}) copy-start(bf16[2048]{0:T(1024)(128)(2,1)} %param.25) | copy-start | bytes 12292
  123.8 119.5 %copy-start.3 = (bf16[2048,256]{1,0:T(8,128)(2,1)S(1)}, bf16[2048,256]{1,0:T(8,128)(2,1)}, u32[]{:S(2)}) copy-start(bf16[2048,256]{1,0:T(8,128)(2,1)} %param.26) | copy-start | bytes 3145732
  130.2 121.9 %reduce-scatter.10.cloned.1.call-start = ((), (), s32[]{:S(2)}) async-start(), calls=%async_computation.6 | async-start | bytes 98304
  240.4 12.6 %copy-start.5 = (bf16[16,128]{1,0:T(8,128)(2,1)S(1)}, bf16[16,128]{1,0:T(8,128)(2,1)}, u32[]{:S(2)}) copy-start(bf16[16,128]{1,0:T(8,128)(2,1)} %param.15) | copy-start | bytes 12292
  245.3 128.7 %reduce-scatter.6.cloned.1.call-start = ((), (), s32[]{:S(2)}) async-start(), calls=%async_computation.4 | async-start | bytes 278528 | tf_op jit(solution)/shard_map/reduce_scatter | solution.py:155
  300.6 79.3 %reduce-scatter.8.cloned.1.call-start = ((), (), s32[]{:S(2)}) async-start(), calls=%async_computation.5 | async-start | bytes 24576 | tf_op jit(solution)/shard_map/reduce_scatter | solution.py:156
Sparse Core Ops, SparseCore 0:
  12.8 106.1 all-reduce.4
  130.4 109.0 all-reduce.6
  245.4 6.6 reduce-scatter.9
  300.7 73.1 reduce-scatter.5
  376.0 3.8 reduce-scatter.7
where the time goes:
time: 388 us
  waiting for transfers between devices  206 us (53%)
  blocking collectives  123 us (32%)
  matrix products  26.8 us (7%)
  between operations  13.3 us (3%)
  other arithmetic  9.4 us (2%)
  local copies, waits for them, and re-layouts  8.86 us (2%)
    psum x1, waiting for transfers between devices, on_device(): cached = lax.psum(partial_out, 'kv')  109 us
    psum x1, blocking collectives, on_device(): lax.psum((part_query, part_key, part_value, part_gate, col_query, col_key...  78.5 us
    reduce_scatter x1, waiting for transfers between devices, on_device(): lax.psum_scatter(down_terms, 'kv', scatter_dimension=1, tiled=True)  73.3 us
    all_gather x1, blocking collectives, on_device(): lax.all_gather(own_residual, ('kv', 'tp'), axis=1, tiled=True)  42 us
    psum x1, waiting for transfers between devices, on_device(): lax.psum((part_query, part_key, part_value, part_gate, col_query, col_key...  13.9 us
    unnamed x22, local copies, waits for them, and re-layouts  8.69 us
  transfers between devices with their start and end apart: 5, of which 5 were waited for; matrix products, arithmetic and copies ran while one was open for 5% of the time, Pallas kernels for 0%

commit v1 on v0

v1 whole, which is shorter than its diff:
```python
import jax
import jax.numpy as jnp
from jax import lax
from jax.sharding import PartitionSpec as P

HEAD_KEY = 64
HEAD_VALUE = 128
EPS = 1e-05
THETA = 10000.0

BF = jnp.bfloat16
F32 = jnp.float32


def split_two(x):
    high = x.astype(BF)
    return high, (x - high.astype(F32)).astype(BF)


def rotate(flat, cosine, sine):
    rows = flat.shape[0]
    grouped = flat.reshape(rows, -1, HEAD_KEY)
    half = HEAD_KEY // 2
    a, b = grouped[..., :half], grouped[..., half:]
    c, s = cosine[:, None, :], sine[:, None, :]
    return jnp.concatenate([a * c - b * s, b * c + a * s], -1).reshape(rows, -1)


def broadcast_gather(x, axes, size):
    spread = jnp.broadcast_to(x[None], (size,) + x.shape)
    return lax.all_to_all(spread, axes, 0, 0, tiled=True)


def make_on_device(kv, tp):
    def on_device(
        tokens,
        lengths,
        attn_gain,
        w_query,
        w_key,
        w_value,
        w_gate,
        decay_rate,
        key_cache,
        value_cache,
        head_gain,
        w_output,
        mlp_gain,
        w_up,
        w_down,
    ):
        S = tokens.shape[0]
        H = decay_rate.shape[0]
        span = key_cache.shape[1]
        width = tokens.shape[1] * kv * tp
        own = tokens.shape[1]
        kvi = lax.axis_index("kv")
        tpi = lax.axis_index("tp")
        groups = kv // H
        rows = S // groups

        if tp == 2:
            other = lax.ppermute(tokens, "tp", [(0, 1), (1, 0)])
            low = jnp.where(tpi == 0, tokens, other)
            high = jnp.where(tpi == 0, other, tokens)
            block = jnp.concatenate([low, high], 1)
        else:
            block = lax.all_gather(tokens, "tp", axis=1, tiled=True)
        wide = block.astype(F32)
        scaled = (wide * attn_gain.astype(F32)).astype(BF)
        lhs = jnp.concatenate([scaled, attn_gain[None, :]], 0)
        part_q = jnp.dot(lhs, w_query, preferred_element_type=F32)
        moments = jnp.stack([jnp.sum(wide, -1), jnp.sum(wide * wide, -1)], -1)

        small = jnp.concatenate([part_q[S], moments.reshape(-1)])
        q_sum = part_q[:S]
        stride = 1
        while stride < kv:
            count = 4 if kv % (stride * 4) == 0 else 2
            high, low = split_two(small)
            tail = jnp.concatenate([high, low])
            pad = -tail.shape[0] % S
            tail = jnp.pad(tail, (0, pad)).reshape(S, -1)
            message = jnp.concatenate([q_sum.astype(BF), tail], 1)
            for j in range(1, count):
                got = lax.ppermute(message, "kv", [(i, i ^ (j * stride)) for i in range(kv)])
                got = got.astype(F32)
                q_sum = q_sum + got[:, : q_sum.shape[1]]
                flat = got[:, q_sum.shape[1] :].reshape(-1)
                n = small.shape[0]
                small = small + flat[:n] + flat[n : 2 * n]
            stride *= count
        csum_q = small[: q_sum.shape[1]]
        moments = small[q_sum.shape[1] :].reshape(S, 2)
        average = moments[:, 0] / width
        inverse = lax.rsqrt(moments[:, 1] / width - average * average + EPS)

        half = HEAD_KEY // 2
        turn = jnp.power(THETA, -jnp.arange(half, dtype=F32) / half)
        angles = lengths.astype(F32)[:, None] * turn[None, :]
        q_plain = inverse[:, None] * (q_sum - average[:, None] * csum_q[None, :])
        queries = rotate(q_plain, jnp.cos(angles), jnp.sin(angles)).astype(BF)
        queries = queries.reshape(S, H, HEAD_KEY)

        def partial(w):
            p = jnp.dot(lhs, w, preferred_element_type=F32)
            return inverse[:, None] * (p[:S] - average[:, None] * p[S:])

        part_k = partial(w_key).reshape(S, H, HEAD_KEY)
        part_v = partial(w_value).reshape(S, H, HEAD_VALUE)
        part_g = partial(w_gate).reshape(S, H, HEAD_VALUE)
        part_score = jnp.sum(q_plain.reshape(S, H, HEAD_KEY) * part_k, -1) * HEAD_KEY ** (-0.5)

        keys = key_cache.reshape(S, span, H, HEAD_KEY)
        values = value_cache.reshape(S, span, H, HEAD_VALUE)
        scores = jnp.einsum("bhd,bjhd->bhj", queries, keys, preferred_element_type=F32)
        places = kvi * span + jnp.arange(span, dtype=jnp.int32)
        distance = jnp.maximum(lengths[:, None] - places[None, :], 0).astype(F32)
        live = (places[None, :] < lengths[:, None])[:, None, :]
        decays = jnp.where(
            live, jnp.exp(-decay_rate[None, :, None] * distance[:, None, :]), 0.0
        )
        coefficients = (scores * HEAD_KEY ** (-0.5) * decays).astype(BF)
        part_c = jnp.einsum("bhj,bjhe->bhe", coefficients, values, preferred_element_type=F32)

        high, low = split_two(part_score)
        pieces = jnp.concatenate(
            [
                part_c.astype(BF),
                part_v.astype(BF),
                part_g.astype(BF),
                high[..., None],
                low[..., None],
                jnp.zeros((S, H, 126), BF),
            ],
            -1,
        )
        pieces = pieces.transpose(1, 0, 2).reshape(kv, rows, 4 * HEAD_VALUE)
        mine = jnp.sum(
            lax.all_to_all(pieces, "kv", 0, 0, tiled=True).astype(F32), 0
        )
        cached, value, gate = (
            mine[:, i * HEAD_VALUE : (i + 1) * HEAD_VALUE] for i in range(3)
        )
        score = mine[:, 3 * HEAD_VALUE] + mine[:, 3 * HEAD_VALUE + 1]
        retained = cached + score[:, None] * value
        centered = retained - jnp.mean(retained, -1, keepdims=True)
        gain = lax.dynamic_slice(head_gain, ((kvi // groups) * HEAD_VALUE,), (HEAD_VALUE,))
        normed = (
            centered
            * lax.rsqrt(jnp.mean(centered * centered, -1, keepdims=True) + EPS)
            * gain.astype(F32)
        )
        gated = (jax.nn.silu(gate) * normed).astype(BF)
        gathered = broadcast_gather(gated, "kv", kv).reshape(H, S, HEAD_VALUE)
        gathered = gathered.transpose(1, 0, 2).reshape(S, H * HEAD_VALUE)
        part_b = jnp.dot(gathered, w_output, preferred_element_type=F32).astype(BF)
        part_b = part_b.reshape(S, tp, own).transpose(1, 0, 2)
        if tp == 2:
            keep = jnp.where(tpi == 0, part_b[0], part_b[1])
            send = jnp.where(tpi == 0, part_b[1], part_b[0])
            got = lax.ppermute(send, "tp", [(0, 1), (1, 0)])
            branch = keep.astype(F32) + got.astype(F32)
        else:
            branch = jnp.sum(
                lax.all_to_all(part_b, "tp", 0, 0, tiled=True).astype(F32), 0
            )
        own_residual = (tokens.astype(F32) + branch).astype(BF)

        residual = broadcast_gather(own_residual, ("kv", "tp"), kv * tp)
        residual = residual.transpose(1, 0, 2).reshape(S, width)
        wide = residual.astype(F32)
        scaled = (wide * mlp_gain.astype(F32)).astype(BF)
        lhs = jnp.concatenate([scaled, mlp_gain[None, :]], 0)
        up = jnp.dot(lhs, w_up, preferred_element_type=F32)
        average = jnp.sum(wide, -1) / width
        inverse = lax.rsqrt(jnp.sum(wide * wide, -1) / width - average * average + EPS)
        hidden = inverse[:, None] * (up[:S] - average[:, None] * up[S:])
        hidden = jnp.square(jax.nn.relu(hidden)).astype(BF)
        down = jnp.dot(hidden, w_down, preferred_element_type=F32).astype(BF)
        down = down.reshape(S, kv * tp, own).transpose(1, 0, 2)
        mixer = jnp.sum(
            lax.all_to_all(down, ("kv", "tp"), 0, 0, tiled=True).astype(F32), 0
        )
        return (own_residual.astype(F32) + mixer).astype(BF)

    return on_device


def solution(mesh):
    in_specs = (
        P(None, ("kv", "tp")),
        P(),
        P("kv"),
        P("kv", "tp"),
        P("kv", "tp"),
        P("kv", "tp"),
        P("kv", "tp"),
        P("tp"),
        P(None, "kv", "tp"),
        P(None, "kv", "tp"),
        P("tp"),
        P("tp", "kv"),
        P(),
        P(None, ("kv", "tp")),
        P(("kv", "tp"), None),
    )
    return jax.shard_map(
        make_on_device(mesh.shape["kv"], mesh.shape["tp"]),
        mesh=mesh,
        in_specs=in_specs,
        out_specs=P(None, ("kv", "tp")),
        check_vma=False,
    )
```

time: 388 us -> 117 us (0.30)
  waiting for transfers between devices: 206 us -> 21.7 us
  blocking collectives: 123 us -> 20.8 us
  local copies, waits for them, and re-layouts: 8.86 us -> 27.8 us
  starting transfers between devices: 0.17 us -> 15.6 us
  matrix products: 26.8 us -> 13.9 us
  between operations: 13.3 us -> 0.63 us
  other arithmetic: 9.4 us -> 15.1 us
    psum x2 -> x0, waiting for transfers between devices: 123 us -> none  [the longest x1 109 us: on_device(): cached = lax.psum(partial_out, 'kv')]
    reduce_scatter x2 -> x0, waiting for transfers between devices: 79.2 us -> none  [the longest x1 73.3 us: on_device(): lax.psum_scatter(down_terms, 'kv', scatter_dimension=1, tiled=True)]
    psum x1 -> x0, blocking collectives: 78.5 us -> none  [on_device(): lax.psum((part_query, part_key, part_value, part_gate, col_query, col_key...]
    all_gather x2 -> x0, blocking collectives: 44.3 us -> none  [the longest x1 42 us: on_device(): lax.all_gather(own_residual, ('kv', 'tp'), axis=1, tiled=True)]
    all_to_all x0 -> x2, blocking collectives: none -> 20.8 us  [the longest x1 10.8 us: broadcast_gather(): return lax.all_to_all(spread, axes, 0, 0, tiled=True)]
    slice x0 -> x39, local copies, waits for them, and re-layouts: none -> 17.2 us  [the longest x30 17.2 us: on_device(): small = small + flat[:n] + flat[n:2 * n]]
    all_to_all x0 -> x2, waiting for transfers between devices: none -> 15.9 us  [the longest x1 8.16 us: broadcast_gather(): return lax.all_to_all(spread, axes, 0, 0, tiled=True)]
    dot_general x13 -> x9, matrix products: 26.8 us -> 13.9 us  [the longest x1 5.76 us: on_device(): jnp.einsum('bhj,bjhe->bhe', coefficients, values, preferred_element_type=...]
  transfers between devices with their start and end apart: 5 -> 10, of which waited for: 5 -> 6; matrix products, arithmetic and copies ran while one was open for 5% -> 21% of each run, Pallas kernels for 0% -> 0%
where the time goes in v1:
time: 117 us; the launch traced here: 115 us
  local copies, waits for them, and re-layouts  27.8 us (24%)
  waiting for transfers between devices  21.7 us (19%)
  blocking collectives  20.8 us (18%)
  starting transfers between devices  15.6 us (13%)
  other arithmetic  15.1 us (13%)
  matrix products  13.9 us (12%)
    slice x30, local copies, waits for them, and re-layouts, on_device(): small = small + flat[:n] + flat[n:2 * n]  17.2 us
    all_to_all x1, blocking collectives, broadcast_gather(): return lax.all_to_all(spread, axes, 0, 0, tiled=True)  10.8 us
    all_to_all x1, blocking collectives, on_device(): lax.all_to_all(down, ('kv', 'tp'), 0, 0, tiled=True).astype(F32)  9.91 us
    ppermute x6, starting transfers between devices, on_device(): got = lax.ppermute(message, 'kv', [(i, i ^ j * stride) for i in range(kv)])  8.56 us
    all_to_all x1, waiting for transfers between devices, broadcast_gather(): return lax.all_to_all(spread, axes, 0, 0, tiled=True)  8.16 us
    all_to_all x1, waiting for transfers between devices, on_device(): lax.all_to_all(pieces, 'kv', 0, 0, tiled=True).astype(F32)  7.74 us
    unnamed x43, local copies, waits for them, and re-layouts  7.28 us
    dot_general x1, matrix products, on_device(): jnp.einsum('bhj,bjhe->bhe', coefficients, values, preferred_element_type=...  5.76 us
  transfers between devices with their start and end apart: 10, of which 6 were waited for; matrix products, arithmetic and copies ran while one was open for 21% of the time, Pallas kernels for 0%

profile of v1, /device:TPU:0, one launch (start us, length us, event | category | flops | bytes accessed | tf_op | source)
XLA Modules:
  0.0 115.5 jit_solution(17767088963699575244)
XLA Ops:
  1.2 1.3 %maximum_convert_fusion = f32[16,128]{1,0:T(8,128)} fusion(s32[128]{0:T(128)S(1)} %iota_add_fusion, s32[16]{0:T(128)} %param.16), kind=kLoop, calls=%fused_computation.95 | loop fusion | flops 6144 | bytes 8768 | tf_op jit(solution)/shard_map/convert_element_type | solution.py:118
  3.2 1.3 %broadcast_compare_fusion = pred[16,128]{1,0:T(8,128)(4,1)} fusion(s32[128]{0:T(128)S(1)} %iota_add_fusion, s32[16]{0:T(128)} %param.16), kind=kLoop, calls=%fused_computation.108 | loop fusion | flops 2048 | bytes 2624 | tf_op jit(solution)/shard_map/lt | solution.py:119
  5.9 6.5 %copy.55 = bf16[16,128,1024]{1,2,0:T(8,128)(2,1)} copy(bf16[16,128,1024]{2,1,0:T(8,128)(2,1)} %param.23) | data formatting | bytes 8388608 | tf_op args[8]
  13.7 2.6 %collective-permute-start.1 = (bf16[16,1156]{1,0:T(8,128)(2,1)S(1)}, bf16[16,1156]{1,0:T(8,128)(2,1)S(1)}, u32[]{:S(2)}, u32[]{:S(2)}) collective-permute-start(bf16[16,1156]{1,0:T(8,128)(2,1)S(1)} %maximum_maximum_fusion), channel_id=1, source_target_pairs={{0,2},{2,0},{4,6},{6,4},{8,10},{10,8},{12,14},{14,12},{16,18},{18,... | collective-permute-start | bytes 110984 | tf_op jit(solution)/shard_map/ppermute | solution.py:86
  16.3 1.5 %collective-permute-start.2 = (bf16[16,1156]{1,0:T(8,128)(2,1)S(1)}, bf16[16,1156]{1,0:T(8,128)(2,1)S(1)}, u32[]{:S(2)}, u32[]{:S(2)}) collective-permute-start(bf16[16,1156]{1,0:T(8,128)(2,1)S(1)} %maximum_maximum_fusion), channel_id=1, source_target_pairs={{0,4},{2,6},{4,0},{6,2},{8,12},{10,14},{12,8},{14,10},{16,20},{18,... | collective-permute-start | bytes 110984 | tf_op jit(solution)/shard_map/ppermute | solution.py:86
  19.2 1.1 collective-permute-done.2
  20.3 2.4 %collective-permute-done.3 = bf16[16,1156]{1,0:T(8,128)(2,1)S(1)} collective-permute-done((bf16[16,1156]{1,0:T(8,128)(2,1)S(1)}, bf16[16,1156]{1,0:T(8,128)(2,1)S(1)}, u32[]{:S(2)}, u32[]{:S(2)}) %collective-permute-start.3) | collective-permute-done | bytes 37024 | tf_op jit(solution)/shard_map/ppermute | solution.py:86
  23.4 1.6 %collective-permute-start.4 = (bf16[16,1156]{1,0:T(8,128)(2,1)}, bf16[16,1156]{1,0:T(8,128)(2,1)S(1)}, u32[]{:S(2)}, u32[]{:S(2)}) collective-permute-start(bf16[16,1156]{1,0:T(8,128)(2,1)} %maximum_maximum_fusion.1), channel_id=1, source_target_pairs={{0,8},{2,10},{4,12},{6,14},{8,0},{10,2},{12,4},{14,6},{16,24},{18,... | collective-permute-start | bytes 110984 | tf_op jit(solution)/shard_map/ppermute | solution.py:86
  25.0 2.6 %collective-permute-start.5 = (bf16[16,1156]{1,0:T(8,128)(2,1)}, bf16[16,1156]{1,0:T(8,128)(2,1)S(1)}, u32[]{:S(2)}, u32[]{:S(2)}) collective-permute-start(bf16[16,1156]{1,0:T(8,128)(2,1)} %maximum_maximum_fusion.1), channel_id=1, source_target_pairs={{0,16},{2,18},{4,20},{6,22},{8,24},{10,26},{12,28},{14,30},{16,0},... | collective-permute-start | bytes 110984 | tf_op jit(solution)/shard_map/ppermute | solution.py:86
  29.8 1.1 collective-permute-done.5
  33.1 0.8 slice.224
  33.9 1.4 %slice.246 = f32[1056]{0:T(1024)} reshape(f32[8,132]{1,0:T(8,128)} %get-tuple-element.29) | data formatting | bytes 8448 | tf_op jit(solution)/shard_map/slice | solution.py:91
  35.3 1.6 %slice.226 = f32[528,2]{1,0:T(8,128)} reshape(f32[8,132]{1,0:T(8,128)} %get-tuple-element.29) | data formatting | bytes 8448 | tf_op jit(solution)/shard_map/slice | solution.py:91
  36.8 1.4 %slice.247 = f32[1056]{0:T(1024)} reshape(f32[8,132]{1,0:T(8,128)} %get-tuple-element.30) | data formatting | bytes 8448 | tf_op jit(solution)/shard_map/slice | solution.py:91
  38.2 1.6 %slice.228 = f32[528,2]{1,0:T(8,128)} reshape(f32[8,132]{1,0:T(8,128)} %get-tuple-element.30) | data formatting | bytes 8448 | tf_op jit(solution)/shard_map/slice | solution.py:91
  39.8 1.3 %fusion.65 = (f32[8,132]{1,0:T(8,128)}, f32[8,132]{1,0:T(8,128)}) fusion(bf16[16,1156]{1,0:T(8,128)(2,1)} %collective-permute-done.6), kind=kLoop, calls=%fused_computation.136 | loop fusion | bytes 16896 | tf_op jit(solution)/shard_map/slice | solution.py:91
  41.1 1.4 %slice.248 = f32[1056]{0:T(1024)} reshape(f32[8,132]{1,0:T(8,128)} %get-tuple-element.31) | data formatting | bytes 8448 | tf_op jit(solution)/shard_map/slice | solution.py:91
  42.4 1.5 %slice.230 = f32[528,2]{1,0:T(8,128)} reshape(f32[8,132]{1,0:T(8,128)} %get-tuple-element.31) | data formatting | bytes 8448 | tf_op jit(solution)/shard_map/slice | solution.py:91
  44.0 1.4 %slice.249 = f32[1056]{0:T(1024)} reshape(f32[8,132]{1,0:T(8,128)} %get-tuple-element.32) | data formatting | bytes 8448 | tf_op jit(solution)/shard_map/slice | solution.py:91
  45.4 1.5 %slice.232 = f32[528,2]{1,0:T(8,128)} reshape(f32[8,132]{1,0:T(8,128)} %get-tuple-element.32) | data formatting | bytes 8448 | tf_op jit(solution)/shard_map/slice | solution.py:91
  46.9 1.5 %add_add_fusion = f32[528,2]{1,0:T(8,128)S(1)} fusion(f32[528,2]{1,0:T(8,128)} %slice.232, f32[528,2]{1,0:T(8,128)} %slice.230, f32[528,2]{1,0:T(8,128)} %slice.228, f32[528,2]{1,0:T(8,128)} %slice.226, f32[528,2]{1,0:T(8,128)S(1)} %slice.224, f32[528,2]{1,0:T(8,128)S(1)} %slice.222, f32[528,2]{1,0:T(8,128)S(1)} %slice.217, f32[528,2]{1,0:T(8,128)S(1)} %slice.215, ...), kind=kLoop, calls=%fused_computation.11 | loop fusion | flops 12672 | bytes 59136 | tf_op jit(solution)/shard_map/add | solution.py:91
  53.4 3.4 %fusion.16 = f32[16,16,1,128]{3,2,1,0:T(1,128)S(1)} fusion(bf16[16,128,16,64]{1,3,2,0:T(8,128)(2,1)} %bitcast.85, bf16[16,16,64,1]{2,1,0,3:T(8,128)(2,1)S(1)} %maximum_bitcast_fusion), kind=kOutput, calls=%fused_computation.29 | convolution fusion | flops 4194304 | bytes 4358144 | tf_op jit(solution)/shard_map/bhd,bjhd->bhj/dot_general | solution.py:116
  57.0 5.8 %fusion = bf16[16,16,1,128]{3,2,1,0:T(2,128)(2,1)S(1)} fusion(bf16[16,16,128,1]{2,1,0,3:T(8,128)(2,1)S(1)} %fusion.18, bf16[16,128,2048]{2,1,0:T(8,128)(2,1)} %param.24), kind=kOutput, calls=%fused_computation | convolution fusion | flops 8388608 | bytes 8519680 | tf_op jit(solution)/shard_map/bhj,bjhe->bhe/dot_general | solution.py:124
  63.0 0.8 concatenate.47
  63.8 3.9 %all-to-all-start = ((bf16[16,16,512]{2,1,0:T(8,128)(2,1)}), bf16[16,16,512]{2,1,0:T(8,128)(2,1)S(1)}, u32[]{:S(2)}, u32[]{:S(2)}) async-start(bf16[16,16,512]{2,1,0:T(8,128)(2,1)} %bitcast.13), calls=%async_computation | async-start | bytes 524288 | tf_op jit(solution)/shard_map/all_to_all | solution.py:140
  68.5 7.7 %all-to-all-done = bf16[16,16,512]{2,1,0:T(8,128)(2,1)S(1)} async-done(((bf16[16,16,512]{2,1,0:T(8,128)(2,1)}), bf16[16,16,512]{2,1,0:T(8,128)(2,1)S(1)}, u32[]{:S(2)}, u32[]{:S(2)}) %all-to-all-start) | async-done | bytes 262176 | tf_op jit(solution)/shard_map/all_to_all | solution.py:140
  76.9 10.8 %all_to_all.20 = bf16[16,16,128]{2,1,0:T(8,128)(2,1)S(1)} all-to-all(bf16[16,16,128]{2,1,0:T(8,128)(2,1)S(1)} %broadcast_in_dim.22), channel_id=1, replica_groups=mesh['kv'=16,'tp'=2] {'kv'}, dimensions={0} | all-to-all | bytes 131072 | tf_op jit(solution)/shard_map/all_to_all | solution.py:31
  88.1 1.2 collective-permute-done.7
  90.0 2.6 %all-to-all-start.2 = ((bf16[32,16,128]{2,1,0:T(8,128)(2,1)}), bf16[32,16,128]{2,1,0:T(8,128)(2,1)S(1)}, u32[]{:S(2)}, u32[]{:S(2)}) async-start(bf16[32,16,128]{2,1,0:T(8,128)(2,1)} %broadcast_in_dim.23), calls=%async_computation.2 | async-start | bytes 262144 | tf_op jit(solution)/shard_map/all_to_all | solution.py:31
  92.6 8.2 %all-to-all-done.2 = bf16[32,16,128]{2,1,0:T(8,128)(2,1)S(1)} async-done(((bf16[32,16,128]{2,1,0:T(8,128)(2,1)}), bf16[32,16,128]{2,1,0:T(8,128)(2,1)S(1)}, u32[]{:S(2)}, u32[]{:S(2)}) %all-to-all-start.2) | async-done | bytes 131104 | tf_op jit(solution)/shard_map/all_to_all | solution.py:31
  100.8 3.0 %fusion.7 = f32[17,512]{1,0:T(8,128)S(1)} fusion(bf16[4096,512]{1,0:T(8,128)(2,1)} %param.28, bf16[1,4096]{1,0:T(2,128)(2,1)S(1)} %broadcast_in_dim.24, bf16[16,4096]{1,0:T(8,128)(2,1)S(1)} %fusion.6), kind=kOutput, calls=%fused_computation.16 | convolution fusion | flops 71581696 | bytes 4368384 | tf_op jit(solution)/shard_map/dot_general | solution.py:175
  104.9 9.9 %all_to_all.21 = bf16[32,16,128]{2,1,0:T(8,128)(2,1)S(1)} all-to-all(bf16[32,16,128]{2,1,0:T(8,128)(2,1)S(1)} %bitcast.88), channel_id=1, replica_groups=mesh['kv'=16,'tp'=2] {'kv','tp'}, dimensions={0} | all-to-all | bytes 262144 | tf_op jit(solution)/shard_map/all_to_all | solution.py:183
  (150 shorter events, 20.3 us)
Async XLA Ops:
  0.0 17.8 %copy-start = (bf16[256,2048]{1,0:T(8,128)(2,1)S(1)}, bf16[256,2048]{1,0:T(8,128)(2,1)}, u32[]{:S(2)}) copy-start(bf16[256,2048]{1,0:T(8,128)(2,1)} %param.21) | copy-start | bytes 3145732
  0.0 13.0 %collective-permute-start = (bf16[16,128]{1,0:T(8,128)(2,1)}, bf16[16,128]{1,0:T(8,128)(2,1)S(1)}, u32[]{:S(2)}, u32[]{:S(2)}) collective-permute-start(bf16[16,128]{1,0:T(8,128)(2,1)} %param.15), channel_id=1, source_target_pairs={{0,1},{1,0},{2,3},{3,2},{4,5},{5,4},{6,7},{7,6},{8,9},{9,8},{10,11... | collective-permute-start | bytes 12296 | tf_op jit(solution)/shard_map/ppermute | solution.py:63
  5.8 6.6 %copy-start.20 = (f32[16]{0:T(128)S(1)}, f32[16]{0:T(128)}, u32[]{:S(2)}) copy-start(f32[16]{0:T(128)} %param.22) | copy-start | bytes 196
  5.8 7.2 %copy-start.17 = (bf16[16,128]{1,0:T(8,128)(2,1)S(1)}, bf16[16,128]{1,0:T(8,128)(2,1)}, u32[]{:S(2)}) copy-start(bf16[16,128]{1,0:T(8,128)(2,1)} %param.15) | copy-start | bytes 12292
  5.8 7.3 %copy-start.8 = (bf16[256,1024]{1,0:T(8,128)(2,1)S(1)}, bf16[256,1024]{1,0:T(8,128)(2,1)}, u32[]{:S(2)}) copy-start(bf16[256,1024]{1,0:T(8,128)(2,1)} %param.18) | copy-start | bytes 1572868
  5.8 12.2 %copy-start.2 = (bf16[256,2048]{1,0:T(8,128)(2,1)S(1)}, bf16[256,2048]{1,0:T(8,128)(2,1)}, u32[]{:S(2)}) copy-start(bf16[256,2048]{1,0:T(8,128)(2,1)} %param.20) | copy-start | bytes 3145732
  5.8 12.5 %copy-start.9 = (bf16[256,1024]{1,0:T(8,128)(2,1)S(1)}, bf16[256,1024]{1,0:T(8,128)(2,1)}, u32[]{:S(2)}) copy-start(bf16[256,1024]{1,0:T(8,128)(2,1)} %param.19) | copy-start | bytes 1572868
  13.7 5.5 %collective-permute-start.1 = (bf16[16,1156]{1,0:T(8,128)(2,1)S(1)}, bf16[16,1156]{1,0:T(8,128)(2,1)S(1)}, u32[]{:S(2)}, u32[]{:S(2)}) collective-permute-start(bf16[16,1156]{1,0:T(8,128)(2,1)S(1)} %maximum_maximum_fusion), channel_id=1, source_target_pairs={{0,2},{2,0},{4,6},{6,4},{8,10},{10,8},{12,14},{14,12},{16,18},{18,... | collective-permute-start | bytes 110984 | tf_op jit(solution)/shard_map/ppermute | solution.py:86
  16.3 4.0 %collective-permute-start.2 = (bf16[16,1156]{1,0:T(8,128)(2,1)S(1)}, bf16[16,1156]{1,0:T(8,128)(2,1)S(1)}, u32[]{:S(2)}, u32[]{:S(2)}) collective-permute-start(bf16[16,1156]{1,0:T(8,128)(2,1)S(1)} %maximum_maximum_fusion), channel_id=1, source_target_pairs={{0,4},{2,6},{4,0},{6,2},{8,12},{10,14},{12,8},{14,10},{16,20},{18,... | collective-permute-start | bytes 110984 | tf_op jit(solution)/shard_map/ppermute | solution.py:86
  17.8 4.9 %collective-permute-start.3 = (bf16[16,1156]{1,0:T(8,128)(2,1)S(1)}, bf16[16,1156]{1,0:T(8,128)(2,1)S(1)}, u32[]{:S(2)}, u32[]{:S(2)}) collective-permute-start(bf16[16,1156]{1,0:T(8,128)(2,1)S(1)} %maximum_maximum_fusion), channel_id=1, source_target_pairs={{0,6},{2,4},{4,2},{6,0},{8,14},{10,12},{12,10},{14,8},{16,22},{18,... | collective-permute-start | bytes 110984 | tf_op jit(solution)/shard_map/ppermute | solution.py:86
  18.1 11.0 %copy-start.4 = (f32[17,2048]{1,0:T(8,128)}, f32[17,2048]{1,0:T(8,128)S(1)}, u32[]{:S(2)}) copy-start(f32[17,2048]{1,0:T(8,128)S(1)} %fusion.48) | copy-start | bytes 417796
  18.3 10.9 %copy-start.6 = (f32[17,2048]{1,0:T(8,128)}, f32[17,2048]{1,0:T(8,128)S(1)}, u32[]{:S(2)}) copy-start(f32[17,2048]{1,0:T(8,128)S(1)} %fusion.49) | copy-start | bytes 417796
  22.7 28.9 %slice-start.2 = ((f32[17,1024]{1,0:T(8,128)}), f32[1,1024]{1,0:T(1,128)S(1)}, s32[]{:S(2)}) async-start(f32[17,1024]{1,0:T(8,128)} %copy-done.10), calls=%async_computation.6 | async-start | bytes 8192 | tf_op jit(solution)/shard_map/slice | solution.py:107
  23.4 6.4 %collective-permute-start.4 = (bf16[16,1156]{1,0:T(8,128)(2,1)}, bf16[16,1156]{1,0:T(8,128)(2,1)S(1)}, u32[]{:S(2)}, u32[]{:S(2)}) collective-permute-start(bf16[16,1156]{1,0:T(8,128)(2,1)} %maximum_maximum_fusion.1), channel_id=1, source_target_pairs={{0,8},{2,10},{4,12},{6,14},{8,0},{10,2},{12,4},{14,6},{16,24},{18,... | collective-permute-start | bytes 110984 | tf_op jit(solution)/shard_map/ppermute | solution.py:86
  25.0 6.0 %collective-permute-start.5 = (bf16[16,1156]{1,0:T(8,128)(2,1)}, bf16[16,1156]{1,0:T(8,128)(2,1)S(1)}, u32[]{:S(2)}, u32[]{:S(2)}) collective-permute-start(bf16[16,1156]{1,0:T(8,128)(2,1)} %maximum_maximum_fusion.1), channel_id=1, source_target_pairs={{0,16},{2,18},{4,20},{6,22},{8,24},{10,26},{12,28},{14,30},{16,0},... | collective-permute-start | bytes 110984 | tf_op jit(solution)/shard_map/ppermute | solution.py:86
  27.6 12.2 %collective-permute-start.6 = (bf16[16,1156]{1,0:T(8,128)(2,1)}, bf16[16,1156]{1,0:T(8,128)(2,1)}, u32[]{:S(2)}, u32[]{:S(2)}) collective-permute-start(bf16[16,1156]{1,0:T(8,128)(2,1)} %maximum_maximum_fusion.1), channel_id=1, source_target_pairs={{0,24},{2,26},{4,28},{6,30},{8,16},{10,18},{12,20},{14,22},{16,8},... | collective-permute-start | bytes 110984 | tf_op jit(solution)/shard_map/ppermute | solution.py:86
  29.8 1.8 %copy-start.12 = (bf16[16,1156]{1,0:T(8,128)(2,1)}, bf16[16,1156]{1,0:T(8,128)(2,1)S(1)}, u32[]{:S(2)}) copy-start(bf16[16,1156]{1,0:T(8,128)(2,1)S(1)} %collective-permute-done.4) | copy-start | bytes 110980
  29.8 2.6 %copy-start.14 = (f32[8,132]{1,0:T(8,128)}, f32[8,132]{1,0:T(8,128)S(1)}, u32[]{:S(2)}) copy-start(f32[8,132]{1,0:T(8,128)S(1)} %get-tuple-element.28) | copy-start | bytes 12676
  46.9 4.8 %copy-start.11 = (f32[17,1024]{1,0:T(8,128)S(1)}, f32[17,1024]{1,0:T(8,128)}, u32[]{:S(2)}) copy-start(f32[17,1024]{1,0:T(8,128)} %copy-done.10) | copy-start | bytes 208900
  48.4 8.4 %copy-start.16 = (f32[16,128]{1,0:T(8,128)S(1)}, f32[16,128]{1,0:T(8,128)}, u32[]{:S(2)}) copy-start(f32[16,128]{1,0:T(8,128)} %maximum_convert_fusion) | copy-start | bytes 24580
  48.4 8.4 %copy-start.18 = (pred[16,128]{1,0:T(8,128)(4,1)S(1)}, pred[16,128]{1,0:T(8,128)(4,1)}, u32[]{:S(2)}) copy-start(pred[16,128]{1,0:T(8,128)(4,1)} %broadcast_compare_fusion) | copy-start | bytes 6148
  48.4 8.4 %copy-start.19 = (f32[16]{0:T(128)S(1)}, f32[16]{0:T(128)}, u32[]{:S(2)}) copy-start(f32[16]{0:T(128)} %neg.16) | copy-start | bytes 196
  56.9 5.9 %copy-start.5 = (f32[17,2048]{1,0:T(8,128)S(1)}, f32[17,2048]{1,0:T(8,128)}, u32[]{:S(2)}) copy-start(f32[17,2048]{1,0:T(8,128)} %copy-done.4) | copy-start | bytes 417796
  56.9 5.9 %slice-start = ((f32[17,2048]{1,0:T(8,128)}), f32[1,2048]{1,0:T(1,128)S(1)}, s32[]{:S(2)}) async-start(f32[17,2048]{1,0:T(8,128)} %copy-done.4), calls=%async_computation.4 | async-start | bytes 16384 | tf_op jit(solution)/shard_map/slice | solution.py:107
  56.9 5.9 %copy-start.7 = (f32[17,2048]{1,0:T(8,128)S(1)}, f32[17,2048]{1,0:T(8,128)}, u32[]{:S(2)}) copy-start(f32[17,2048]{1,0:T(8,128)} %copy-done.6) | copy-start | bytes 417796
  56.9 5.9 %slice-start.1 = ((f32[17,2048]{1,0:T(8,128)}), f32[1,2048]{1,0:T(1,128)S(1)}, s32[]{:S(2)}) async-start(f32[17,2048]{1,0:T(8,128)} %copy-done.6), calls=%async_computation.5 | async-start | bytes 16384 | tf_op jit(solution)/shard_map/slice | solution.py:107
  57.0 30.8 %copy-start.3 = (bf16[2048,256]{1,0:T(8,128)(2,1)S(1)}, bf16[2048,256]{1,0:T(8,128)(2,1)}, u32[]{:S(2)}) copy-start(bf16[2048,256]{1,0:T(8,128)(2,1)} %param.26) | copy-start | bytes 3145732
  62.7 29.8 %copy-start.15 = (bf16[4096]{0:T(1024)(128)(2,1)S(1)}, bf16[4096]{0:T(1024)(128)(2,1)}, u32[]{:S(2)}) copy-start(bf16[4096]{0:T(1024)(128)(2,1)} %param.27) | copy-start | bytes 24580
  63.8 12.4 %all-to-all-start = ((bf16[16,16,512]{2,1,0:T(8,128)(2,1)}), bf16[16,16,512]{2,1,0:T(8,128)(2,1)S(1)}, u32[]{:S(2)}, u32[]{:S(2)}) async-start(bf16[16,16,512]{2,1,0:T(8,128)(2,1)} %bitcast.13), calls=%async_computation | async-start | bytes 524288 | tf_op jit(solution)/shard_map/all_to_all | solution.py:140
  88.1 1.2 %collective-permute-start.7 = (bf16[16,128]{1,0:T(8,128)(2,1)S(1)}, bf16[16,128]{1,0:T(8,128)(2,1)S(1)}, u32[]{:S(2)}, u32[]{:S(2)}) collective-permute-start(bf16[16,128]{1,0:T(8,128)(2,1)S(1)} %select_bitcast_fusion), channel_id=1, source_target_pairs={{0,1},{1,0},{2,3},{3,2},{4,5},{5,4},{6,7},{7,6},{8,9},{9,8},{10,11... | collective-permute-start | bytes 12296 | tf_op jit(solution)/shard_map/ppermute | solution.py:162
  90.0 10.8 %all-to-all-start.2 = ((bf16[32,16,128]{2,1,0:T(8,128)(2,1)}), bf16[32,16,128]{2,1,0:T(8,128)(2,1)S(1)}, u32[]{:S(2)}, u32[]{:S(2)}) async-start(bf16[32,16,128]{2,1,0:T(8,128)(2,1)} %broadcast_in_dim.23), calls=%async_computation.2 | async-start | bytes 262144 | tf_op jit(solution)/shard_map/all_to_all | solution.py:31
  100.7 3.4 %copy-start.1 = (bf16[512,4096]{1,0:T(8,128)(2,1)S(1)}, bf16[512,4096]{1,0:T(8,128)(2,1)}, u32[]{:S(2)}) copy-start(bf16[512,4096]{1,0:T(8,128)(2,1)} %param.29) | copy-start | bytes 12582916
  (2 other events, 1.3 us)

commit v2 on v1

--- a/solution.py
+++ b/solution.py
@@ -1,12 +1,18 @@
+import functools
+import math
+
 import jax
 import jax.numpy as jnp
 from jax import lax
+from jax.experimental import pallas as pl
+from jax.experimental.pallas import tpu as pltpu
 from jax.sharding import PartitionSpec as P
 
 HEAD_KEY = 64
 HEAD_VALUE = 128
 EPS = 1e-05
 THETA = 10000.0
+LANES = 128
 
 BF = jnp.bfloat16
 F32 = jnp.float32
@@ -187,6 +193,394 @@
     return on_device
 
 
+def lane_ids(rows):
+    return lax.broadcasted_iota(jnp.int32, (rows, LANES), 1)
+
+
+def row_ids(rows, columns=LANES):
+    return lax.broadcasted_iota(jnp.int32, (rows, columns), 0)
+
+
+def column_of(scalars, rows, dtype):
+    ids = row_ids(rows)
+    out = jnp.zeros((rows, LANES), dtype)
+    for i in range(rows):
+        out = jnp.where(ids == i, scalars[i].astype(dtype), out)
+    return out
+
+
+def projection_rows(first, second, gain):
+    t = lax.axis_index("tp")
+    a, b = first[...].astype(F32), second[...].astype(F32)
+    wide = jnp.concatenate([jnp.where(t == 0, a, b), jnp.where(t == 0, b, a)], 1)
+    row = gain[...]
+    scaled = (wide * row.astype(F32)).astype(BF)
+    return jnp.concatenate([scaled, jnp.broadcast_to(row, scaled.shape)], 0), wide
+
+
+def pack(q, csum, moments, message):
+    columns = q.shape[1]
+    half = csum.shape[0]
+    message[:, :columns] = q.astype(BF)
+    high = csum.astype(BF)
+    low = (csum - high.astype(F32)).astype(BF)
+    message[:, columns : columns + LANES] = jnp.concatenate([high, low], 0)
+    high = moments.astype(BF).astype(F32)
+    low = moments - high
+    lanes = lane_ids(q.shape[0])
+    both = jnp.where(lanes < 2, high, jnp.where(lanes < 4, pltpu.roll(low, 2, 1), 0.0))
+    message[:, columns + LANES :] = both.astype(BF)
+    assert 2 * half == q.shape[0]
+
+
+def unpack_sum(state, messages):
+    rows, total = state.shape
+    columns = total - 2 * LANES
+    half = rows // 2
+    q = state[:, :columns]
+    csum = state[:half, columns : columns + LANES]
+    moments = state[:, columns + LANES :]
+    for m in messages:
+        q = q + m[:, :columns].astype(F32)
+        c = m[:, columns : columns + LANES].astype(F32)
+        csum = csum + c[:half] + c[half:]
+        v = m[:, columns + LANES :].astype(F32)
+        moments = moments + v + pltpu.roll(v, LANES - 2, 1)
+    return q, csum, jnp.where(lane_ids(rows) < 2, moments, 0.0)
+
+
+def store_state(q, csum, moments, state):
+    columns = q.shape[1]
+    state[:, :columns] = q
+    state[:, columns : columns + LANES] = jnp.concatenate([csum, jnp.zeros_like(csum)], 0)
+    state[:, columns + LANES :] = moments
+
+
+def query_kernel(first, second, gain, w_query, state, message):
+    lhs, wide = projection_rows(first, second, gain)
+    rows = wide.shape[0]
+    product = jnp.dot(lhs, w_query[...], preferred_element_type=F32)
+    half = rows // 2
+    ids = row_ids(half)
+    csum = jnp.zeros((half, LANES), F32)
+    for i in range(product.shape[1] // LANES):
+        csum = jnp.where(
+            ids == i, product[rows : rows + half, i * LANES : (i + 1) * LANES], csum
+        )
+    lanes = lane_ids(rows)
+    first_sum = jnp.sum(wide, 1, keepdims=True)
+    second_sum = jnp.sum(wide * wide, 1, keepdims=True)
+    moments = jnp.where(lanes == 0, first_sum, jnp.where(lanes == 1, second_sum, 0.0))
+    store_state(product[:rows], csum, moments, state)
+    pack(product[:rows], csum, moments, message)
+
+
+def middle_kernel(old, m1, m2, m3, state, message):
+    q, csum, moments = unpack_sum(old, (m1, m2, m3))
+    store_state(q, csum, moments, state)
+    pack(q, csum, moments, message)
+
+
+def other_kernel(lengths, first, second, gain, w_key, w_value, w_gate, k_out, v_out, g_out, turn):
+    lhs, wide = projection_rows(first, second, gain)
+    rows = wide.shape[0]
+    for w, out in ((w_key, k_out), (w_value, v_out), (w_gate, g_out)):
+        product = jnp.dot(lhs, w[...], preferred_element_type=F32)
+        out[...] = product[: rows + 8]
+    half = HEAD_KEY // 2
+    entry = (lane_ids(rows) % half).astype(F32)
+    inverse = jnp.exp(entry * (-math.log(THETA) / half))
+    angle = column_of(lengths, rows, F32) * inverse
+    turn[0] = jnp.cos(angle)
+    turn[1] = jnp.sin(angle)
+
+
+def attend_kernel(
+    width,
+    lengths,
+    decay,
+    old,
+    m1,
+    m2,
+    m3,
+    k_part,
+    v_part,
+    g_part,
+    turn,
+    keys,
+    values,
+    out,
+    key_buffer,
+    value_buffer,
+    query_rows,
+    cached,
+    key_sem,
+    value_sem,
+):
+    rows, span, key_columns = keys.shape
+    heads = key_columns // HEAD_KEY
+
+    def copies(s):
+        return (
+            pltpu.make_async_copy(keys.at[s], key_buffer.at[s], key_sem.at[s]),
+            pltpu.make_async_copy(values.at[s], value_buffer.at[s], value_sem.at[s]),
+        )
+
+    for s in range(rows):
+        for copy in copies(s):
+            copy.start()
+
+    q, csum, moments = unpack_sum(old, (m1, m2, m3))
+    average = moments[:, 0:1] / width
+    inverse = lax.rsqrt(moments[:, 1:2] / width - average * average + EPS)
+    lanes = lane_ids(rows)
+    in_first = lanes % HEAD_KEY < HEAD_KEY // 2
+    low_head = lanes < HEAD_KEY
+    cosine, sine = turn[0], turn[1]
+    for i in range(key_columns // LANES):
+        cut = slice(i * LANES, (i + 1) * LANES)
+        plain = inverse * (q[:, cut] - average * csum[i : i + 1])
+        partner = jnp.where(
+            in_first,
+            -pltpu.roll(plain, LANES - HEAD_KEY // 2, 1),
+            pltpu.roll(plain, HEAD_KEY // 2, 1),
+        )
+        turned = plain * cosine + partner * sine
+        query_rows[:, cut] = turned.astype(BF).astype(F32)
+        part = inverse * (k_part[:rows, cut] - average * k_part[rows : rows + 1, cut])
+        both = plain * part * HEAD_KEY ** (-0.5)
+        for j in range(2):
+            picked = jnp.where(low_head == (j == 0), both, 0.0)
+            score = jnp.sum(picked, 1, keepdims=True)
+            high = score.astype(BF).astype(F32)
+            out[2 * i + j, :, 3 * LANES :] = jnp.where(low_head, high, score - high).astype(BF)
+    for h in range(heads):
+        cut = slice(h * LANES, (h + 1) * LANES)
+        for place, part in ((1, v_part), (2, g_part)):
+            normed = inverse * (part[:rows, cut] - average * part[rows : rows + 1, cut])
+            out[h, :, place * LANES : (place + 1) * LANES] = normed.astype(BF)
+
+    base = lax.axis_index("kv") * span
+    places = base + lax.broadcasted_iota(jnp.int32, (heads, span), 1)
+    rate = column_of(decay, heads, F32)
+    if span != LANES:
+        rate = jnp.broadcast_to(rate[:, :1], (heads, span))
+    head_of_key = lax.broadcasted_iota(jnp.int32, (heads, key_columns), 1) // HEAD_KEY
+    own_key = head_of_key == row_ids(heads, key_columns)
+    value_columns = heads * HEAD_VALUE
+    head_of_value = lax.broadcasted_iota(jnp.int32, (heads, value_columns), 1) // HEAD_VALUE
+    own_value = head_of_value == row_ids(heads, value_columns)
+    for s in range(rows):
+        for copy in copies(s):
+            copy.wait()
+        spread = jnp.broadcast_to(query_rows[s : s + 1, :], (heads, key_columns))
+        query = jnp.where(own_key, spread, 0.0).astype(BF)
+        scores = lax.dot_general(
+            query, key_buffer[s], (((1,), (1,)), ((), ())), preferred_element_type=F32
+        )
+        distance = lengths[s] - places
+        weight = jnp.exp(-rate * jnp.maximum(distance, 0).astype(F32))
+        weight = jnp.where(distance > 0, weight, 0.0)
+        coefficients = (scores * HEAD_KEY ** (-0.5) * weight).astype(BF)
+        product = jnp.dot(coefficients, value_buffer[s], preferred_element_type=F32)
+        cached[s : s + 1, :] = jnp.sum(
+            jnp.where(own_value, product, 0.0), 0, keepdims=True
+        )
+    for h in range(heads):
+        out[h, :, :LANES] = cached[:, h * LANES : (h + 1) * LANES].astype(BF)
+
+
+def gate_kernel(pieces, head_gain, out):
+    total = jnp.sum(pieces[...].astype(F32), 0)
+    cached, value, gate, score = (total[:, i * LANES : (i + 1) * LANES] for i in range(4))
+    score = score[:, 0:1] + score[:, HEAD_KEY : HEAD_KEY + 1]
+    retained = cached + score * value
+    centered = retained - jnp.mean(retained, -1, keepdims=True)
+    spread = lax.rsqrt(jnp.mean(centered * centered, -1, keepdims=True) + EPS)
+    gains = head_gain[...].astype(F32)
+    mine = row_ids(gains.shape[0]) == lax.axis_index("kv")
+    gain = jnp.sum(jnp.where(mine, gains, 0.0), 0, keepdims=True)
+    normed = centered * spread * gain
+    gated = (gate * jax.nn.sigmoid(gate) * normed).astype(BF)
+    out[...] = jnp.broadcast_to(gated[None], out.shape)
+
+
+def output_kernel(gated, w_output, keep, send):
+    heads = gated.shape[0]
+    lhs = jnp.concatenate([gated[h] for h in range(heads)], 1)
+    part = jnp.dot(lhs, w_output[...], preferred_element_type=F32)
+    t = lax.axis_index("tp")
+    half = keep.shape[1]
+    low, high = part[:, :half], part[:, half:]
+    keep[...] = jnp.where(t == 0, low, high).astype(BF)
+    send[...] = jnp.where(t == 0, high, low).astype(BF)
+
+
+def residual_kernel(tokens, keep, got, own, out):
+    branch = keep[...].astype(F32) + got[...].astype(F32)
+    residual = (tokens[...].astype(F32) + branch).astype(BF)
+    own[...] = residual
+    out[...] = jnp.broadcast_to(residual[None], out.shape)
+
+
+def mixer_kernel(residual, mlp_gain, w_up, w_down, out):
+    blocks, rows, own = residual.shape
+    width = blocks * own
+    first = jnp.zeros((rows, own), F32)
+    second = jnp.zeros((rows, own), F32)
+    scaled = []
+    for i in range(blocks):
+        wide = residual[i].astype(F32)
+        first = first + wide
+        second = second + wide * wide
+        row = mlp_gain[:, i * own : (i + 1) * own]
+        scaled.append((wide * row.astype(F32)).astype(BF))
+    scaled = jnp.concatenate(scaled, 1)
+    lhs = jnp.concatenate([scaled, jnp.broadcast_to(mlp_gain[...], scaled.shape)], 0)
+    up = jnp.dot(lhs, w_up[...], preferred_element_type=F32)
+    average = jnp.sum(first, 1, keepdims=True) / width
+    inverse = lax.rsqrt(jnp.sum(second, 1, keepdims=True) / width - average * average + EPS)
+    hidden = inverse * (up[:rows] - average * up[rows : rows + 1])
+    hidden = jnp.square(jnp.maximum(hidden, 0.0)).astype(BF)
+    down = jnp.dot(hidden, w_down[...], preferred_element_type=F32)
+    for i in range(blocks):
+        out[i] = down[:, i * own : (i + 1) * own].astype(BF)
+
+
+def final_kernel(pieces, own, out):
+    total = jnp.sum(pieces[...].astype(F32), 0)
+    out[...] = (own[...].astype(F32) + total).astype(BF)
+
+
+VMEM = pl.BlockSpec(memory_space=pltpu.VMEM)
+SMEM = pl.BlockSpec(memory_space=pltpu.SMEM)
+ANY = pl.BlockSpec(memory_space=pl.ANY)
+
+
+def call(kernel, name, outs, in_specs, flops=0, bytes_accessed=0, scratch=(), limit=None):
+    return pl.pallas_call(
+        kernel,
+        name=name,
+        out_shape=outs,
+        in_specs=in_specs,
+        out_specs=jax.tree.map(lambda _: VMEM, outs),
+        scratch_shapes=list(scratch),
+        cost_estimate=pl.CostEstimate(
+            flops=flops, bytes_accessed=bytes_accessed, transcendentals=0
+        ),
+        compiler_params=pltpu.CompilerParams(vmem_limit_bytes=limit),
+    )
+
+
+def make_kernels_on_device(kv, tp):
+    def on_device(
+        tokens,
+        lengths,
+        attn_gain,
+        w_query,
+        w_key,
+        w_value,
+        w_gate,
+        decay_rate,
+        key_cache,
+        value_cache,
+        head_gain,
+        w_output,
+        mlp_gain,
+        w_up,
+        w_down,
+    ):
+        S, own = tokens.shape
+        H = decay_rate.shape[0]
+        span = key_cache.shape[1]
+        width = own * kv * tp
+        qc, vc = H * HEAD_KEY, H * HEAD_VALUE
+        swap = [(0, 1), (1, 0)]
+        mib = 1 << 20
+        sds = jax.ShapeDtypeStruct
+
+        other = lax.ppermute(tokens, "tp", swap)
+        gain = attn_gain[None, :]
+        columns = qc + 2 * LANES
+        message_types = (sds((S, columns), F32), sds((S, columns), BF))
+        state, message = call(
+            query_kernel, "query", message_types, [VMEM] * 4, limit=4 * mib
+        )(tokens, other, gain, w_query)
+
+        def exchange(message, stride):
+            return [
+                lax.ppermute(message, "kv", [(i, i ^ (j * stride)) for i in range(kv)])
+                for j in range(1, 4)
+            ]
+
+        k_part, v_part, g_part, turn = call(
+            other_kernel,
+            "other",
+            (
+                sds((S + 8, qc), F32),
+                sds((S + 8, vc), F32),
+                sds((S + 8, vc), F32),
+                sds((2, S, LANES), F32),
+            ),
+            [SMEM] + [VMEM] * 6,
+            flops=10**9,
+            bytes_accessed=4 * mib,
+            limit=8 * mib,
+        )(lengths, tokens, other, gain, w_key, w_value, w_gate)
+
+        got = exchange(message, 1)
+        stride = 4
+        while stride < kv:
+            state, message = call(
+                middle_kernel, "middle", message_types, [VMEM] * 4, limit=2 * mib
+            )(state, *got)
+            got = exchange(message, stride)
+            stride *= 4
+
+        pieces = call(
+            functools.partial(attend_kernel, width),
+            "attend",
+            sds((H, S, 4 * LANES), BF),
+            [SMEM] * 2 + [VMEM] * 8 + [ANY] * 2,
+            scratch=[
+                pltpu.VMEM(key_cache.shape, BF),
+                pltpu.VMEM(value_cache.shape, BF),
+                pltpu.VMEM((S, qc), F32),
+                pltpu.VMEM((S, vc), F32),
+                pltpu.SemaphoreType.DMA((S,)),
+                pltpu.SemaphoreType.DMA((S,)),
+            ],
+            limit=20 * mib,
+        )(lengths, decay_rate, state, *got, k_part, v_part, g_part, turn, key_cache, value_cache)
+
+        pieces = lax.all_to_all(pieces, "kv", 0, 0, tiled=True)
+        spread = call(gate_kernel, "gate", sds((kv, S, LANES), BF), [VMEM] * 2, limit=2 * mib)(
+            pieces, head_gain.reshape(H, HEAD_VALUE)
+        )
+        gated = lax.all_to_all(spread, "kv", 0, 0, tiled=True)
+        keep, send = call(
+            output_kernel, "output", (sds((S, own), BF),) * 2, [VMEM] * 2, limit=4 * mib
+        )(gated, w_output)
+        got = lax.ppermute(send, "tp", swap)
+        residual, spread = call(
+            residual_kernel,
+            "residual",
+            (sds((S, own), BF), sds((kv * tp, S, own), BF)),
+            [VMEM] * 3,
+            limit=2 * mib,
+        )(tokens, keep, got)
+        spread = lax.all_to_all(spread, ("kv", "tp"), 0, 0, tiled=True)
+        down = call(
+            mixer_kernel, "mixer", sds((kv * tp, S, own), BF), [VMEM] * 4, limit=16 * mib
+        )(spread, mlp_gain[None, :], w_up, w_down)
+        down = lax.all_to_all(down, ("kv", "tp"), 0, 0, tiled=True)
+        return call(final_kernel, "final", sds((S, own), BF), [VMEM] * 2, limit=2 * mib)(
+            down, residual
+        )
+
+    return on_device
+
+
 def solution(mesh):
     in_specs = (
         P(None, ("kv", "tp")),
@@ -205,8 +599,15 @@
         P(None, ("kv", "tp")),
         P(("kv", "tp"), None),
     )
+    kv, tp = mesh.shape["kv"], mesh.shape["tp"]
+
+    def on_device(*arrays):
+        fits = tp == 2 and arrays[7].shape[0] == kv and arrays[0].shape[1] == LANES
+        make = make_kernels_on_device if fits else make_on_device
+        return make(kv, tp)(*arrays)
+
     return jax.shard_map(
-        make_on_device(mesh.shape["kv"], mesh.shape["tp"]),
+        on_device,
         mesh=mesh,
         in_specs=in_specs,
         out_specs=P(None, ("kv", "tp")),

time: 117 us -> 92.5 us (0.79)
  other arithmetic: 15.1 us -> 0 us
  Pallas kernels: 0 us -> 15 us
  matrix products: 13.9 us -> 0 us
  blocking collectives: 20.8 us -> 34 us
  local copies, waits for them, and re-layouts: 27.8 us -> 16.6 us
  waiting for transfers between devices: 21.7 us -> 14.4 us
  starting transfers between devices: 15.6 us -> 11.9 us
    slice x39 -> x0, local copies, waits for them, and re-layouts: 17.2 us -> none  [the longest x30 17.2 us: on_device(): small = small + flat[:n] + flat[n:2 * n]]
    pallas_call x0 -> x9, Pallas kernels: none -> 15 us  [the longest x1 10.2 us: on_device(): call(functools.partial(attend_kernel, width), 'attend', sds((H, S, 4 * LA...]
    dot_general x9 -> x0, matrix products: 13.9 us -> none  [the longest x1 5.76 us: on_device(): jnp.einsum('bhj,bjhe->bhe', coefficients, values, preferred_element_type=...]
    all_to_all x2 -> x3, blocking collectives: 20.8 us -> 34 us  [the longest x1 13.3 us: on_device(): pieces = lax.all_to_all(pieces, 'kv', 0, 0, tiled=True)]
    unnamed x43 -> x34, local copies, waits for them, and re-layouts: 7.28 us -> 15.6 us
    all_to_all x2 -> x1, waiting for transfers between devices: 15.9 us -> 8.17 us  [on_device(): spread = lax.all_to_all(spread, ('kv', 'tp'), 0, 0, tiled=True)]
    convert_element_type x21 -> x0, other arithmetic: 6.64 us -> none  [the longest x6 2.38 us: on_device(): got = got.astype(F32)]
    all_to_all x2 -> x1, starting transfers between devices: 6.43 us -> 2.57 us  [on_device(): spread = lax.all_to_all(spread, ('kv', 'tp'), 0, 0, tiled=True)]
  transfers between devices with their start and end apart: 10 -> 9, of which waited for: 6 -> 6; matrix products, arithmetic and copies ran while one was open for 21% -> 1% of each run, Pallas kernels for 0% -> 1%
where the time goes in v2:
time: 92.5 us; the launch traced here: 91.9 us
  blocking collectives  34 us (37%)
  local copies, waits for them, and re-layouts  16.6 us (18%)
  Pallas kernels  15 us (16%)
  waiting for transfers between devices  14.4 us (16%)
  starting transfers between devices  11.9 us (13%)
    unnamed x34, local copies, waits for them, and re-layouts  15.6 us
    all_to_all x1, blocking collectives, on_device(): pieces = lax.all_to_all(pieces, 'kv', 0, 0, tiled=True)  13.3 us
    all_to_all x1, blocking collectives, on_device(): gated = lax.all_to_all(spread, 'kv', 0, 0, tiled=True)  10.8 us
    pallas_call x1, Pallas kernels, on_device(): call(functools.partial(attend_kernel, width), 'attend', sds((H, S, 4 * LA...  10.2 us
    all_to_all x1, blocking collectives, on_device(): down = lax.all_to_all(down, ('kv', 'tp'), 0, 0, tiled=True)  9.9 us
    ppermute x6, starting transfers between devices, exchange(): lax.ppermute(message, 'kv', [(i, i ^ j * stride) for i in range(kv)])  8.81 us
    all_to_all x1, waiting for transfers between devices, on_device(): spread = lax.all_to_all(spread, ('kv', 'tp'), 0, 0, tiled=True)  8.17 us
    ppermute x6, waiting for transfers between devices, exchange(): lax.ppermute(message, 'kv', [(i, i ^ j * stride) for i in range(kv)])  4.89 us
  transfers between devices with their start and end apart: 9, of which 6 were waited for; matrix products, arithmetic and copies ran while one was open for 1% of the time, Pallas kernels for 1%

profile of v2, /device:TPU:0, one launch (start us, length us, event | category | flops | bytes accessed | tf_op | source)
XLA Modules:
  0.0 91.9 jit_solution(13160315540809826733)
XLA Ops:
  0.0 0.5 collective-permute-start
  0.5 0.9 broadcast_in_dim.6.gain
  1.5 1.0 %copy-done.5 = bf16[256,1024]{1,0:T(8,128)(2,1)S(1)} copy-done((bf16[256,1024]{1,0:T(8,128)(2,1)S(1)}, bf16[256,1024]{1,0:T(8,128)(2,1)}, u32[]{:S(2)}) %copy-start.5) | copy-done | bytes 524312
  2.6 0.7 copy-done.6
  3.5 2.9 %collective-permute-start.1 = (bf16[16,1280]{1,0:T(8,128)(2,1)S(1)}, bf16[16,1280]{1,0:T(8,128)(2,1)S(1)}, u32[]{:S(2)}, u32[]{:S(2)}) collective-permute-start(bf16[16,1280]{1,0:T(8,128)(2,1)S(1)} %get-tuple-element.18), channel_id=1, source_target_pairs={{0,2},{2,0},{4,6},{6,4},{8,10},{10,8},{12,14},{14,12},{16,18},{18,... | collective-permute-start | bytes 122888 | tf_op jit(solution)/shard_map/ppermute | solution.py:512
  6.4 1.5 %collective-permute-start.2 = (bf16[16,1280]{1,0:T(8,128)(2,1)S(1)}, bf16[16,1280]{1,0:T(8,128)(2,1)S(1)}, u32[]{:S(2)}, u32[]{:S(2)}) collective-permute-start(bf16[16,1280]{1,0:T(8,128)(2,1)S(1)} %get-tuple-element.18), channel_id=1, source_target_pairs={{0,4},{2,6},{4,0},{6,2},{8,12},{10,14},{12,8},{14,10},{16,20},{18,... | collective-permute-start | bytes 122888 | tf_op jit(solution)/shard_map/ppermute | solution.py:512
  7.9 0.4 collective-permute-done.1.m1
  8.3 2.0 %collective-permute-done.2.m2 = bf16[16,1280]{1,0:T(8,128)(2,1)S(1)} collective-permute-done((bf16[16,1280]{1,0:T(8,128)(2,1)S(1)}, bf16[16,1280]{1,0:T(8,128)(2,1)S(1)}, u32[]{:S(2)}, u32[]{:S(2)}) %collective-permute-start.2) | collective-permute-done | bytes 40992 | tf_op jit(solution)/shard_map/ppermute | solution.py:512
  10.4 2.4 %collective-permute-done.3.m3 = bf16[16,1280]{1,0:T(8,128)(2,1)S(1)} collective-permute-done((bf16[16,1280]{1,0:T(8,128)(2,1)S(1)}, bf16[16,1280]{1,0:T(8,128)(2,1)S(1)}, u32[]{:S(2)}, u32[]{:S(2)}) %collective-permute-start.3) | collective-permute-done | bytes 40992 | tf_op jit(solution)/shard_map/ppermute | solution.py:512
  12.9 1.6 %collective-permute-start.4 = (bf16[16,1280]{1,0:T(8,128)(2,1)S(1)}, bf16[16,1280]{1,0:T(8,128)(2,1)S(1)}, u32[]{:S(2)}, u32[]{:S(2)}) collective-permute-start(bf16[16,1280]{1,0:T(8,128)(2,1)S(1)} %get-tuple-element.20), channel_id=1, source_target_pairs={{0,8},{2,10},{4,12},{6,14},{8,0},{10,2},{12,4},{14,6},{16,24},{18,... | collective-permute-start | bytes 122888 | tf_op jit(solution)/shard_map/ppermute | solution.py:512
  14.5 2.6 %collective-permute-start.5 = (bf16[16,1280]{1,0:T(8,128)(2,1)S(1)}, bf16[16,1280]{1,0:T(8,128)(2,1)S(1)}, u32[]{:S(2)}, u32[]{:S(2)}) collective-permute-start(bf16[16,1280]{1,0:T(8,128)(2,1)S(1)} %get-tuple-element.20), channel_id=1, source_target_pairs={{0,16},{2,18},{4,20},{6,22},{8,24},{10,26},{12,28},{14,30},{16,0},... | collective-permute-start | bytes 122888 | tf_op jit(solution)/shard_map/ppermute | solution.py:512
  17.3 0.7 copy-done.7
  18.0 0.7 copy-done.10
  18.7 1.2 %copy-done.13 = bf16[256,2048]{1,0:T(8,128)(2,1)S(1)} copy-done((bf16[256,2048]{1,0:T(8,128)(2,1)S(1)}, bf16[256,2048]{1,0:T(8,128)(2,1)}, u32[]{:S(2)}) %copy-start.13) | copy-done | bytes 1048600
  19.9 1.2 %copy-done.14 = bf16[256,2048]{1,0:T(8,128)(2,1)S(1)} copy-done((bf16[256,2048]{1,0:T(8,128)(2,1)S(1)}, bf16[256,2048]{1,0:T(8,128)(2,1)}, u32[]{:S(2)}) %copy-start.14) | copy-done | bytes 1048600
  21.1 1.0 %copy-done.15 = bf16[256,1024]{1,0:T(8,128)(2,1)S(1)} copy-done((bf16[256,1024]{1,0:T(8,128)(2,1)S(1)}, bf16[256,1024]{1,0:T(8,128)(2,1)}, u32[]{:S(2)}) %copy-start.15) | copy-done | bytes 524312
  22.2 1.1 %other.1 = (f32[24,1024]{1,0:T(8,128)S(1)}, f32[24,2048]{1,0:T(8,128)S(1)}, f32[24,2048]{1,0:T(8,128)S(1)}, f32[2,16,128]{2,1,0:T(8,128)S(1)}) custom-call(s32[16]{0:T(128)S(1)} %copy-done.10, bf16[16,128]{1,0:T(8,128)(2,1)S(1)} %copy-done.7, bf16[16,128]{1,0:T(8,128)(2,1)S(1)} %collective-permute-done.second, bf16[1,256]{1,0:T(2,128)(2,1)S(1)} %broadcast_in_dim.6.gain, ...), custom_call_target="tpu_custom_call" | custom-call | flops 1000000000 | bytes 4194304 | tf_op jit(solution)/shard_map/other/pallas_call | solution.py:516
  23.3 3.4 %copy-done = bf16[16,128,2048]{2,1,0:T(8,128)(2,1)S(1)} copy-done((bf16[16,128,2048]{2,1,0:T(8,128)(2,1)S(1)}, bf16[16,128,2048]{2,1,0:T(8,128)(2,1)}, u32[]{:S(2)}) %copy-start) | copy-done | bytes 8388632
  26.7 0.7 copy-done.11
  27.3 0.7 copy-done.12
  28.0 10.2 %attend.1 = bf16[16,16,512]{2,1,0:T(8,128)(2,1)S(1)} custom-call(s32[16]{0:T(128)S(1)} %copy-done.11, f32[16]{0:T(128)S(1)} %copy-done.12, f32[16,1280]{1,0:T(8,128)S(1)} %get-tuple-element.19.old, bf16[16,1280]{1,0:T(8,128)(2,1)S(1)} %collective-permute-done.4.m1, bf16[16,1280]{1,0:T(8,128)(2,1)S(1)} %collective-permute-done.5.m2, ...), custom_call_target="tpu_custom_call" | custom-call | tf_op jit(solution)/shard_map/attend/pallas_call | solution.py:540
  38.2 13.3 %all_to_all.20.pieces = bf16[16,16,512]{2,1,0:T(8,128)(2,1)S(1)} all-to-all(bf16[16,16,512]{2,1,0:T(8,128)(2,1)S(1)} %attend.1), channel_id=1, replica_groups=mesh['kv'=16,'tp'=2] {'kv'}, dimensions={0} | all-to-all | bytes 524288 | tf_op jit(solution)/shard_map/all_to_all | solution.py:556
  51.8 10.8 %all_to_all.21.gated = bf16[16,16,128]{2,1,0:T(8,128)(2,1)S(1)} all-to-all(bf16[16,16,128]{2,1,0:T(8,128)(2,1)S(1)} %gate.1), channel_id=1, replica_groups=mesh['kv'=16,'tp'=2] {'kv'}, dimensions={0} | all-to-all | bytes 131072 | tf_op jit(solution)/shard_map/all_to_all | solution.py:560
  62.9 1.2 %collective-permute-done.7.got = bf16[16,128]{1,0:T(8,128)(2,1)S(1)} collective-permute-done((bf16[16,128]{1,0:T(8,128)(2,1)S(1)}, bf16[16,128]{1,0:T(8,128)(2,1)S(1)}, u32[]{:S(2)}, u32[]{:S(2)}) %collective-permute-start.7) | collective-permute-done | bytes 4128 | tf_op jit(solution)/shard_map/ppermute | solution.py:564
  64.1 0.7 residual.1
  64.8 2.6 %all-to-all-start.2 = ((bf16[32,16,128]{2,1,0:T(8,128)(2,1)}), bf16[32,16,128]{2,1,0:T(8,128)(2,1)S(1)}, u32[]{:S(2)}, u32[]{:S(2)}) async-start(bf16[32,16,128]{2,1,0:T(8,128)(2,1)} %get-tuple-element.27), calls=%async_computation.2 | async-start | bytes 262144 | tf_op jit(solution)/shard_map/all_to_all | solution.py:572
  67.4 8.2 %all-to-all-done.2.residual = bf16[32,16,128]{2,1,0:T(8,128)(2,1)S(1)} async-done(((bf16[32,16,128]{2,1,0:T(8,128)(2,1)}), bf16[32,16,128]{2,1,0:T(8,128)(2,1)S(1)}, u32[]{:S(2)}, u32[]{:S(2)}) %all-to-all-start.2) | async-done | bytes 131104 | tf_op jit(solution)/shard_map/all_to_all | solution.py:572
  75.5 2.2 %copy-done.2 = bf16[4096,512]{1,0:T(8,128)(2,1)S(1)} copy-done((bf16[4096,512]{1,0:T(8,128)(2,1)S(1)}, bf16[4096,512]{1,0:T(8,128)(2,1)}, u32[]{:S(2)}) %copy-start.2) | copy-done | bytes 4194328
  77.7 2.2 %copy-done.3 = bf16[512,4096]{1,0:T(8,128)(2,1)S(1)} copy-done((bf16[512,4096]{1,0:T(8,128)(2,1)S(1)}, bf16[512,4096]{1,0:T(8,128)(2,1)}, u32[]{:S(2)}) %copy-start.3) | copy-done | bytes 4194328
  79.9 1.4 %mixer.1 = bf16[32,16,128]{2,1,0:T(8,128)(2,1)S(1)} custom-call(bf16[32,16,128]{2,1,0:T(8,128)(2,1)S(1)} %all-to-all-done.2.residual, bf16[1,4096]{1,0:T(2,128)(2,1)S(1)} %broadcast_in_dim.7.mlp_gain, bf16[4096,512]{1,0:T(8,128)(2,1)S(1)} %copy-done.2, bf16[512,4096]{1,0:T(8,128)(2,1)S(1)} %copy-done.3), custom_call_target="tpu_custom_call" | custom-call | tf_op jit(solution)/shard_map/mixer/pallas_call | solution.py:573
  81.4 9.9 %all_to_all.22.pieces = bf16[32,16,128]{2,1,0:T(8,128)(2,1)S(1)} all-to-all(bf16[32,16,128]{2,1,0:T(8,128)(2,1)S(1)} %mixer.1), channel_id=1, replica_groups=mesh['kv'=16,'tp'=2] {'kv','tp'}, dimensions={0} | all-to-all | bytes 262144 | tf_op jit(solution)/shard_map/all_to_all | solution.py:576
  91.3 0.6 final.1
  (34 shorter events, 1.4 us)
Async XLA Ops:
  0.0 23.3 %copy-start.1 = (bf16[16,128,1024]{2,1,0:T(8,128)(2,1)S(1)}, bf16[16,128,1024]{2,1,0:T(8,128)(2,1)}, u32[]{:S(2)}) copy-start(bf16[16,128,1024]{2,1,0:T(8,128)(2,1)} %keys.1) | copy-start | bytes 12582916
  0.0 1.5 %collective-permute-start = (bf16[16,128]{1,0:T(8,128)(2,1)}, bf16[16,128]{1,0:T(8,128)(2,1)S(1)}, u32[]{:S(2)}, u32[]{:S(2)}) collective-permute-start(bf16[16,128]{1,0:T(8,128)(2,1)} %tokens.1), channel_id=1, source_target_pairs={{0,1},{1,0},{2,3},{3,2},{4,5},{5,4},{6,7},{7,6},{8,9},{9,8},{10,11... | collective-permute-start | bytes 12296 | tf_op jit(solution)/shard_map/ppermute | solution.py:502
  1.5 1.0 %copy-start.5 = (bf16[256,1024]{1,0:T(8,128)(2,1)S(1)}, bf16[256,1024]{1,0:T(8,128)(2,1)}, u32[]{:S(2)}) copy-start(bf16[256,1024]{1,0:T(8,128)(2,1)} %w_query.1) | copy-start | bytes 1572868
  2.6 0.7 copy-start.6
  3.5 4.9 %collective-permute-start.1 = (bf16[16,1280]{1,0:T(8,128)(2,1)S(1)}, bf16[16,1280]{1,0:T(8,128)(2,1)S(1)}, u32[]{:S(2)}, u32[]{:S(2)}) collective-permute-start(bf16[16,1280]{1,0:T(8,128)(2,1)S(1)} %get-tuple-element.18), channel_id=1, source_target_pairs={{0,2},{2,0},{4,6},{6,4},{8,10},{10,8},{12,14},{14,12},{16,18},{18,... | collective-permute-start | bytes 122888 | tf_op jit(solution)/shard_map/ppermute | solution.py:512
  6.4 4.0 %collective-permute-start.2 = (bf16[16,1280]{1,0:T(8,128)(2,1)S(1)}, bf16[16,1280]{1,0:T(8,128)(2,1)S(1)}, u32[]{:S(2)}, u32[]{:S(2)}) collective-permute-start(bf16[16,1280]{1,0:T(8,128)(2,1)S(1)} %get-tuple-element.18), channel_id=1, source_target_pairs={{0,4},{2,6},{4,0},{6,2},{8,12},{10,14},{12,8},{14,10},{16,20},{18,... | collective-permute-start | bytes 122888 | tf_op jit(solution)/shard_map/ppermute | solution.py:512
  7.9 4.9 %collective-permute-start.3 = (bf16[16,1280]{1,0:T(8,128)(2,1)S(1)}, bf16[16,1280]{1,0:T(8,128)(2,1)S(1)}, u32[]{:S(2)}, u32[]{:S(2)}) collective-permute-start(bf16[16,1280]{1,0:T(8,128)(2,1)S(1)} %get-tuple-element.18), channel_id=1, source_target_pairs={{0,6},{2,4},{4,2},{6,0},{8,14},{10,12},{12,10},{14,8},{16,22},{18,... | collective-permute-start | bytes 122888 | tf_op jit(solution)/shard_map/ppermute | solution.py:512
  12.9 10.3 %collective-permute-start.4 = (bf16[16,1280]{1,0:T(8,128)(2,1)S(1)}, bf16[16,1280]{1,0:T(8,128)(2,1)S(1)}, u32[]{:S(2)}, u32[]{:S(2)}) collective-permute-start(bf16[16,1280]{1,0:T(8,128)(2,1)S(1)} %get-tuple-element.20), channel_id=1, source_target_pairs={{0,8},{2,10},{4,12},{6,14},{8,0},{10,2},{12,4},{14,6},{16,24},{18,... | collective-permute-start | bytes 122888 | tf_op jit(solution)/shard_map/ppermute | solution.py:512
  14.5 8.8 %collective-permute-start.5 = (bf16[16,1280]{1,0:T(8,128)(2,1)S(1)}, bf16[16,1280]{1,0:T(8,128)(2,1)S(1)}, u32[]{:S(2)}, u32[]{:S(2)}) collective-permute-start(bf16[16,1280]{1,0:T(8,128)(2,1)S(1)} %get-tuple-element.20), channel_id=1, source_target_pairs={{0,16},{2,18},{4,20},{6,22},{8,24},{10,26},{12,28},{14,30},{16,0},... | collective-permute-start | bytes 122888 | tf_op jit(solution)/shard_map/ppermute | solution.py:512
  17.1 6.2 %collective-permute-start.6 = (bf16[16,1280]{1,0:T(8,128)(2,1)S(1)}, bf16[16,1280]{1,0:T(8,128)(2,1)S(1)}, u32[]{:S(2)}, u32[]{:S(2)}) collective-permute-start(bf16[16,1280]{1,0:T(8,128)(2,1)S(1)} %get-tuple-element.20), channel_id=1, source_target_pairs={{0,24},{2,26},{4,28},{6,30},{8,16},{10,18},{12,20},{14,22},{16,8},... | collective-permute-start | bytes 122888 | tf_op jit(solution)/shard_map/ppermute | solution.py:512
  17.3 0.7 copy-start.7
  18.0 0.7 copy-start.10
  18.7 1.2 %copy-start.13 = (bf16[256,2048]{1,0:T(8,128)(2,1)S(1)}, bf16[256,2048]{1,0:T(8,128)(2,1)}, u32[]{:S(2)}) copy-start(bf16[256,2048]{1,0:T(8,128)(2,1)} %w_value.1) | copy-start | bytes 3145732
  19.9 1.2 %copy-start.14 = (bf16[256,2048]{1,0:T(8,128)(2,1)S(1)}, bf16[256,2048]{1,0:T(8,128)(2,1)}, u32[]{:S(2)}) copy-start(bf16[256,2048]{1,0:T(8,128)(2,1)} %w_gate.1) | copy-start | bytes 3145732
  21.1 1.0 %copy-start.15 = (bf16[256,1024]{1,0:T(8,128)(2,1)S(1)}, bf16[256,1024]{1,0:T(8,128)(2,1)}, u32[]{:S(2)}) copy-start(bf16[256,1024]{1,0:T(8,128)(2,1)} %w_key.1) | copy-start | bytes 1572868
  23.3 3.4 %copy-start = (bf16[16,128,2048]{2,1,0:T(8,128)(2,1)S(1)}, bf16[16,128,2048]{2,1,0:T(8,128)(2,1)}, u32[]{:S(2)}) copy-start(bf16[16,128,2048]{2,1,0:T(8,128)(2,1)} %values.1) | copy-start | bytes 25165828
  26.7 0.7 copy-start.11
  27.3 0.7 copy-start.12
  28.0 23.5 %copy-start.9 = (bf16[2048]{0:T(1024)(128)(2,1)S(1)}, bf16[2048]{0:T(1024)(128)(2,1)}, u32[]{:S(2)}) copy-start(bf16[2048]{0:T(1024)(128)(2,1)} %param.25) | copy-start | bytes 12292
  28.0 34.7 %copy-start.4 = (bf16[2048,256]{1,0:T(8,128)(2,1)S(1)}, bf16[2048,256]{1,0:T(8,128)(2,1)}, u32[]{:S(2)}) copy-start(bf16[2048,256]{1,0:T(8,128)(2,1)} %w_output.1) | copy-start | bytes 3145732
  28.0 36.1 %copy-start.8 = (bf16[16,128]{1,0:T(8,128)(2,1)S(1)}, bf16[16,128]{1,0:T(8,128)(2,1)}, u32[]{:S(2)}) copy-start(bf16[16,128]{1,0:T(8,128)(2,1)} %tokens.1) | copy-start | bytes 12292
  28.0 39.3 %copy-start.16 = (bf16[4096]{0:T(1024)(128)(2,1)S(1)}, bf16[4096]{0:T(1024)(128)(2,1)}, u32[]{:S(2)}) copy-start(bf16[4096]{0:T(1024)(128)(2,1)} %param.27) | copy-start | bytes 24580
  62.9 1.2 %collective-permute-start.7 = (bf16[16,128]{1,0:T(8,128)(2,1)S(1)}, bf16[16,128]{1,0:T(8,128)(2,1)S(1)}, u32[]{:S(2)}, u32[]{:S(2)}) collective-permute-start(bf16[16,128]{1,0:T(8,128)(2,1)S(1)} %get-tuple-element.26), channel_id=1, source_target_pairs={{0,1},{1,0},{2,3},{3,2},{4,5},{5,4},{6,7},{7,6},{8,9},{9,8},{10,11... | collective-permute-start | bytes 12296 | tf_op jit(solution)/shard_map/ppermute | solution.py:564
  64.8 10.8 %all-to-all-start.2 = ((bf16[32,16,128]{2,1,0:T(8,128)(2,1)}), bf16[32,16,128]{2,1,0:T(8,128)(2,1)S(1)}, u32[]{:S(2)}, u32[]{:S(2)}) async-start(bf16[32,16,128]{2,1,0:T(8,128)(2,1)} %get-tuple-element.27), calls=%async_computation.2 | async-start | bytes 262144 | tf_op jit(solution)/shard_map/all_to_all | solution.py:572
  75.5 2.2 %copy-start.2 = (bf16[4096,512]{1,0:T(8,128)(2,1)S(1)}, bf16[4096,512]{1,0:T(8,128)(2,1)}, u32[]{:S(2)}) copy-start(bf16[4096,512]{1,0:T(8,128)(2,1)} %w_up.1) | copy-start | bytes 12582916
  77.7 2.2 %copy-start.3 = (bf16[512,4096]{1,0:T(8,128)(2,1)S(1)}, bf16[512,4096]{1,0:T(8,128)(2,1)}, u32[]{:S(2)}) copy-start(bf16[512,4096]{1,0:T(8,128)(2,1)} %w_down.1) | copy-start | bytes 12582916

commit v3 on v2

--- a/solution.py
+++ b/solution.py
@@ -209,13 +209,19 @@
     return out
 
 
+def gain_row(gain, rows):
+    wide = gain[...].astype(F32)
+    return jnp.concatenate(
+        [jnp.broadcast_to(wide[i : i + 1], (rows, LANES)) for i in range(wide.shape[0])], 1
+    )
+
+
 def projection_rows(first, second, gain):
     t = lax.axis_index("tp")
     a, b = first[...].astype(F32), second[...].astype(F32)
     wide = jnp.concatenate([jnp.where(t == 0, a, b), jnp.where(t == 0, b, a)], 1)
-    row = gain[...]
-    scaled = (wide * row.astype(F32)).astype(BF)
-    return jnp.concatenate([scaled, jnp.broadcast_to(row, scaled.shape)], 0), wide
+    row = gain_row(gain, wide.shape[0])
+    return jnp.concatenate([(wide * row).astype(BF), row.astype(BF)], 0), wide
 
 
 def pack(q, csum, moments, message):
@@ -256,6 +262,50 @@
     state[:, columns + LANES :] = moments
 
 
+def first_load_kernel(
+    w_query,
+    tokens,
+    gain,
+    lengths,
+    decay,
+    w_out,
+    tokens_out,
+    gain_out,
+    length_out,
+    rate_out,
+    length_scalars,
+    decay_scalars,
+    sems,
+):
+    pairs = (
+        (lengths, length_scalars),
+        (decay, decay_scalars),
+        (tokens, tokens_out),
+        (gain, gain_out),
+        (w_query, w_out),
+    )
+    copies = [pltpu.make_async_copy(a, b, sems.at[i]) for i, (a, b) in enumerate(pairs)]
+    for copy in copies:
+        copy.start()
+    copies[0].wait()
+    length_out[...] = column_of(length_scalars, length_out.shape[0], jnp.int32)
+    copies[1].wait()
+    rate_out[...] = column_of(decay_scalars, rate_out.shape[0], F32)
+    for copy in copies[2:]:
+        copy.wait()
+
+
+def cache_load_kernel(after, keys, values, keys_out, values_out, sems):
+    copies = (
+        pltpu.make_async_copy(keys, keys_out, sems.at[0]),
+        pltpu.make_async_copy(values, values_out, sems.at[1]),
+    )
+    for copy in copies:
+        copy.start()
+    for copy in copies:
+        copy.wait()
+
+
 def query_kernel(first, second, gain, w_query, state, message):
     lhs, wide = projection_rows(first, second, gain)
     rows = wide.shape[0]
@@ -281,24 +331,57 @@
     pack(q, csum, moments, message)
 
 
-def other_kernel(lengths, first, second, gain, w_key, w_value, w_gate, k_out, v_out, g_out, turn):
+def other_kernel(
+    after,
+    lengths,
+    rates,
+    first,
+    second,
+    gain,
+    w_key,
+    w_value,
+    w_gate,
+    k_out,
+    v_out,
+    g_out,
+    turn,
+    weights,
+    key_buffer,
+    value_buffer,
+    gate_buffer,
+    sems,
+):
+    sources = (w_key, w_value, w_gate)
+    buffers = (key_buffer, value_buffer, gate_buffer)
+    copies = [
+        pltpu.make_async_copy(source, buffer, sems.at[i])
+        for i, (source, buffer) in enumerate(zip(sources, buffers))
+    ]
+    for copy in copies:
+        copy.start()
     lhs, wide = projection_rows(first, second, gain)
     rows = wide.shape[0]
-    for w, out in ((w_key, k_out), (w_value, v_out), (w_gate, g_out)):
-        product = jnp.dot(lhs, w[...], preferred_element_type=F32)
-        out[...] = product[: rows + 8]
     half = HEAD_KEY // 2
     entry = (lane_ids(rows) % half).astype(F32)
     inverse = jnp.exp(entry * (-math.log(THETA) / half))
-    angle = column_of(lengths, rows, F32) * inverse
+    angle = lengths[...].astype(F32) * inverse
     turn[0] = jnp.cos(angle)
     turn[1] = jnp.sin(angle)
+    heads = rates.shape[0]
+    places = lax.axis_index("kv") * LANES + lane_ids(heads)
+    rate = rates[...]
+    for s in range(rows):
+        distance = jnp.broadcast_to(lengths[s : s + 1, :], (heads, LANES)) - places
+        weight = jnp.exp(-rate * jnp.maximum(distance, 0).astype(F32)) * HEAD_KEY ** (-0.5)
+        weights[s] = jnp.where(distance > 0, weight, 0.0)
+    for copy, buffer, out in zip(copies, buffers, (k_out, v_out, g_out)):
+        copy.wait()
+        product = jnp.dot(lhs, buffer[...], preferred_element_type=F32)
+        out[...] = product[: rows + 8]
 
 
 def attend_kernel(
     width,
-    lengths,
-    decay,
     old,
     m1,
     m2,
@@ -307,35 +390,22 @@
     v_part,
     g_part,
     turn,
+    weights,
     keys,
     values,
     out,
-    key_buffer,
-    value_buffer,
     query_rows,
     cached,
-    key_sem,
-    value_sem,
 ):
     rows, span, key_columns = keys.shape
     heads = key_columns // HEAD_KEY
-
-    def copies(s):
-        return (
-            pltpu.make_async_copy(keys.at[s], key_buffer.at[s], key_sem.at[s]),
-            pltpu.make_async_copy(values.at[s], value_buffer.at[s], value_sem.at[s]),
-        )
-
-    for s in range(rows):
-        for copy in copies(s):
-            copy.start()
-
     q, csum, moments = unpack_sum(old, (m1, m2, m3))
     average = moments[:, 0:1] / width
     inverse = lax.rsqrt(moments[:, 1:2] / width - average * average + EPS)
     lanes = lane_ids(rows)
     in_first = lanes % HEAD_KEY < HEAD_KEY // 2
     low_head = lanes < HEAD_KEY
+    top = rows // 2
     cosine, sine = turn[0], turn[1]
     for i in range(key_columns // LANES):
         cut = slice(i * LANES, (i + 1) * LANES)
@@ -353,47 +423,48 @@
             picked = jnp.where(low_head == (j == 0), both, 0.0)
             score = jnp.sum(picked, 1, keepdims=True)
             high = score.astype(BF).astype(F32)
-            out[2 * i + j, :, 3 * LANES :] = jnp.where(low_head, high, score - high).astype(BF)
+            low = score - high
+            folded = jnp.where(
+                lanes[:top] < HEAD_KEY,
+                jnp.where(in_first[:top], high[:top], low[:top]),
+                jnp.where(in_first[:top], high[top:], low[top:]),
+            )
+            out[2 * i + j, 3 * rows :, :] = folded.astype(BF)
     for h in range(heads):
         cut = slice(h * LANES, (h + 1) * LANES)
         for place, part in ((1, v_part), (2, g_part)):
             normed = inverse * (part[:rows, cut] - average * part[rows : rows + 1, cut])
-            out[h, :, place * LANES : (place + 1) * LANES] = normed.astype(BF)
-
-    base = lax.axis_index("kv") * span
-    places = base + lax.broadcasted_iota(jnp.int32, (heads, span), 1)
-    rate = column_of(decay, heads, F32)
-    if span != LANES:
-        rate = jnp.broadcast_to(rate[:, :1], (heads, span))
+            out[h, place * rows : (place + 1) * rows, :] = normed.astype(BF)
+
     head_of_key = lax.broadcasted_iota(jnp.int32, (heads, key_columns), 1) // HEAD_KEY
     own_key = head_of_key == row_ids(heads, key_columns)
     value_columns = heads * HEAD_VALUE
     head_of_value = lax.broadcasted_iota(jnp.int32, (heads, value_columns), 1) // HEAD_VALUE
     own_value = head_of_value == row_ids(heads, value_columns)
     for s in range(rows):
-        for copy in copies(s):
-            copy.wait()
         spread = jnp.broadcast_to(query_rows[s : s + 1, :], (heads, key_columns))
         query = jnp.where(own_key, spread, 0.0).astype(BF)
         scores = lax.dot_general(
-            query, key_buffer[s], (((1,), (1,)), ((), ())), preferred_element_type=F32
-        )
-        distance = lengths[s] - places
-        weight = jnp.exp(-rate * jnp.maximum(distance, 0).astype(F32))
-        weight = jnp.where(distance > 0, weight, 0.0)
-        coefficients = (scores * HEAD_KEY ** (-0.5) * weight).astype(BF)
-        product = jnp.dot(coefficients, value_buffer[s], preferred_element_type=F32)
+            query, keys[s], (((1,), (1,)), ((), ())), preferred_element_type=F32
+        )
+        coefficients = (scores * weights[s]).astype(BF)
+        product = jnp.dot(coefficients, values[s], preferred_element_type=F32)
         cached[s : s + 1, :] = jnp.sum(
             jnp.where(own_value, product, 0.0), 0, keepdims=True
         )
     for h in range(heads):
-        out[h, :, :LANES] = cached[:, h * LANES : (h + 1) * LANES].astype(BF)
+        out[h, :rows, :] = cached[:, h * LANES : (h + 1) * LANES].astype(BF)
 
 
 def gate_kernel(pieces, head_gain, out):
+    rows = out.shape[1]
     total = jnp.sum(pieces[...].astype(F32), 0)
-    cached, value, gate, score = (total[:, i * LANES : (i + 1) * LANES] for i in range(4))
-    score = score[:, 0:1] + score[:, HEAD_KEY : HEAD_KEY + 1]
+    cached, value, gate = (total[i * rows : (i + 1) * rows] for i in range(3))
+    folded = total[3 * rows :]
+    half = HEAD_KEY // 2
+    score = jnp.concatenate(
+        [folded[:, i : i + 1] + folded[:, i + half : i + half + 1] for i in (0, HEAD_KEY)], 0
+    )
     retained = cached + score * value
     centered = retained - jnp.mean(retained, -1, keepdims=True)
     spread = lax.rsqrt(jnp.mean(centered * centered, -1, keepdims=True) + EPS)
@@ -428,15 +499,16 @@
     width = blocks * own
     first = jnp.zeros((rows, own), F32)
     second = jnp.zeros((rows, own), F32)
-    scaled = []
+    scaled, gain = [], []
+    gains = mlp_gain[...].astype(F32)
     for i in range(blocks):
         wide = residual[i].astype(F32)
         first = first + wide
         second = second + wide * wide
-        row = mlp_gain[:, i * own : (i + 1) * own]
-        scaled.append((wide * row.astype(F32)).astype(BF))
-    scaled = jnp.concatenate(scaled, 1)
-    lhs = jnp.concatenate([scaled, jnp.broadcast_to(mlp_gain[...], scaled.shape)], 0)
+        row = gains[i : i + 1]
+        scaled.append((wide * row).astype(BF))
+        gain.append(jnp.broadcast_to(row, wide.shape).astype(BF))
+    lhs = jnp.concatenate([jnp.concatenate(scaled, 1), jnp.concatenate(gain, 1)], 0)
     up = jnp.dot(lhs, w_up[...], preferred_element_type=F32)
     average = jnp.sum(first, 1, keepdims=True) / width
     inverse = lax.rsqrt(jnp.sum(second, 1, keepdims=True) / width - average * average + EPS)
@@ -453,8 +525,12 @@
 
 
 VMEM = pl.BlockSpec(memory_space=pltpu.VMEM)
-SMEM = pl.BlockSpec(memory_space=pltpu.SMEM)
+HBM = pl.BlockSpec(memory_space=pltpu.HBM)
 ANY = pl.BlockSpec(memory_space=pl.ANY)
+
+
+def in_hbm(*arrays):
+    return [pltpu.with_memory_space_constraint(x, pltpu.HBM) for x in arrays]
 
 
 def call(kernel, name, outs, in_specs, flops=0, bytes_accessed=0, scratch=(), limit=None):
@@ -500,11 +576,30 @@
         sds = jax.ShapeDtypeStruct
 
         other = lax.ppermute(tokens, "tp", swap)
-        gain = attn_gain[None, :]
+        gain = attn_gain.reshape(-1, LANES)
+        w_query, tokens, gain, length_rows, rates = call(
+            first_load_kernel,
+            "first_load",
+            (
+                sds(w_query.shape, BF),
+                sds(tokens.shape, BF),
+                sds(gain.shape, BF),
+                sds((S, LANES), jnp.int32),
+                sds((H, LANES), F32),
+            ),
+            [HBM] * 5,
+            flops=10**9,
+            scratch=[
+                pltpu.SMEM((S,), jnp.int32),
+                pltpu.SMEM((H,), F32),
+                pltpu.SemaphoreType.DMA((5,)),
+            ],
+            limit=2 * mib,
+        )(*in_hbm(w_query, tokens, gain, lengths, decay_rate))
         columns = qc + 2 * LANES
         message_types = (sds((S, columns), F32), sds((S, columns), BF))
         state, message = call(
-            query_kernel, "query", message_types, [VMEM] * 4, limit=4 * mib
+            query_kernel, "query", message_types, [VMEM] * 4, limit=2 * mib
         )(tokens, other, gain, w_query)
 
         def exchange(message, stride):
@@ -513,7 +608,8 @@
                 for j in range(1, 4)
             ]
 
-        k_part, v_part, g_part, turn = call(
+        got = exchange(message, 1)
+        k_part, v_part, g_part, turn, weights = call(
             other_kernel,
             "other",
             (
@@ -521,14 +617,15 @@
                 sds((S + 8, vc), F32),
                 sds((S + 8, vc), F32),
                 sds((2, S, LANES), F32),
+                sds((S, H, LANES), F32),
             ),
-            [SMEM] + [VMEM] * 6,
+            [ANY] + [VMEM] * 5 + [HBM] * 3,
             flops=10**9,
-            bytes_accessed=4 * mib,
-            limit=8 * mib,
-        )(lengths, tokens, other, gain, w_key, w_value, w_gate)
-
-        got = exchange(message, 1)
+            scratch=[pltpu.VMEM(w.shape, BF) for w in (w_key, w_value, w_gate)]
+            + [pltpu.SemaphoreType.DMA((3,))],
+            limit=6 * mib,
+        )(message, length_rows, rates, tokens, other, gain, *in_hbm(w_key, w_value, w_gate))
+
         stride = 4
         while stride < kv:
             state, message = call(
@@ -536,22 +633,24 @@
             )(state, *got)
             got = exchange(message, stride)
             stride *= 4
+        keys, values = call(
+            cache_load_kernel,
+            "cache_load",
+            (sds(key_cache.shape, BF), sds(value_cache.shape, BF)),
+            [ANY] + [HBM] * 2,
+            flops=10**9,
+            scratch=[pltpu.SemaphoreType.DMA((2,))],
+            limit=2 * mib,
+        )(message, *in_hbm(key_cache, value_cache))
 
         pieces = call(
             functools.partial(attend_kernel, width),
             "attend",
-            sds((H, S, 4 * LANES), BF),
-            [SMEM] * 2 + [VMEM] * 8 + [ANY] * 2,
-            scratch=[
-                pltpu.VMEM(key_cache.shape, BF),
-                pltpu.VMEM(value_cache.shape, BF),
-                pltpu.VMEM((S, qc), F32),
-                pltpu.VMEM((S, vc), F32),
-                pltpu.SemaphoreType.DMA((S,)),
-                pltpu.SemaphoreType.DMA((S,)),
-            ],
-            limit=20 * mib,
-        )(lengths, decay_rate, state, *got, k_part, v_part, g_part, turn, key_cache, value_cache)
+            sds((H, 3 * S + S // 2, LANES), BF),
+            [VMEM] * 11,
+            scratch=[pltpu.VMEM((S, qc), F32), pltpu.VMEM((S, vc), F32)],
+            limit=4 * mib,
+        )(state, *got, k_part, v_part, g_part, turn, weights, keys, values)
 
         pieces = lax.all_to_all(pieces, "kv", 0, 0, tiled=True)
         spread = call(gate_kernel, "gate", sds((kv, S, LANES), BF), [VMEM] * 2, limit=2 * mib)(
@@ -572,7 +671,7 @@
         spread = lax.all_to_all(spread, ("kv", "tp"), 0, 0, tiled=True)
         down = call(
             mixer_kernel, "mixer", sds((kv * tp, S, own), BF), [VMEM] * 4, limit=16 * mib
-        )(spread, mlp_gain[None, :], w_up, w_down)
+        )(spread, mlp_gain.reshape(-1, LANES), w_up, w_down)
         down = lax.all_to_all(down, ("kv", "tp"), 0, 0, tiled=True)
         return call(final_kernel, "final", sds((S, own), BF), [VMEM] * 2, limit=2 * mib)(
             down, residual
@@ -602,7 +701,8 @@
     kv, tp = mesh.shape["kv"], mesh.shape["tp"]
 
     def on_device(*arrays):
-        fits = tp == 2 and arrays[7].shape[0] == kv and arrays[0].shape[1] == LANES
+        fits = tp == 2 and arrays[7].shape[0] == kv
+        fits = fits and arrays[0].shape[1] == LANES == arrays[8].shape[1]
         make = make_kernels_on_device if fits else make_on_device
         return make(kv, tp)(*arrays)
 

time: 92.5 us -> 71 us (0.77)
  local copies, waits for them, and re-layouts: 16.6 us -> 0.03 us
  waiting for transfers between devices: 14.4 us -> 3.01 us
  blocking collectives: 34 us -> 44.5 us
  starting transfers between devices: 11.9 us -> 9.26 us
  Pallas kernels: 15 us -> 13.8 us
    unnamed x34 -> x10, local copies, waits for them, and re-layouts: 15.6 us -> 0.03 us
    all_to_all x0 -> x1, blocking collectives: none -> 9.91 us  [on_device(): spread = lax.all_to_all(spread, ('kv', 'tp'), 0, 0, tiled=True)]
    all_to_all x1 -> x0, waiting for transfers between devices: 8.17 us -> none  [on_device(): spread = lax.all_to_all(spread, ('kv', 'tp'), 0, 0, tiled=True)]
    ppermute x6, waiting for transfers between devices: 4.89 us -> 1.84 us  [exchange(): lax.ppermute(message, 'kv', [(i, i ^ j * stride) for i in range(kv)])]
    all_to_all x1 -> x0, starting transfers between devices: 2.57 us -> none  [on_device(): spread = lax.all_to_all(spread, ('kv', 'tp'), 0, 0, tiled=True)]
    pallas_call x2 -> x4, Pallas kernels: 10.4 us -> 8.88 us  [the longest x1 4.68 us: on_device(): call(cache_load_kernel, 'cache_load', (sds(key_cache.shape, BF), sds(valu...]
    pallas_call x1, Pallas kernels: 1.09 us -> 2.02 us  [on_device(): call(other_kernel, 'other', (sds((S + 8, qc), F32), sds((S + 8, vc), F32)...]
  transfers between devices with their start and end apart: 9 -> 8, of which waited for: 6 -> 3; matrix products, arithmetic and copies ran while one was open for 1% -> 0% of each run, Pallas kernels for 1% -> 11%
where the time goes in v3:
time: 71 us; the launch traced here: 70.8 us
  blocking collectives  44.5 us (63%)
  Pallas kernels  13.8 us (19%)
  starting transfers between devices  9.26 us (13%)
  waiting for transfers between devices  3.01 us (4%)
    all_to_all x1, blocking collectives, on_device(): pieces = lax.all_to_all(pieces, 'kv', 0, 0, tiled=True)  14.1 us
    all_to_all x1, blocking collectives, on_device(): gated = lax.all_to_all(spread, 'kv', 0, 0, tiled=True)  10.6 us
    all_to_all x1, blocking collectives, on_device(): spread = lax.all_to_all(spread, ('kv', 'tp'), 0, 0, tiled=True)  9.91 us
    all_to_all x1, blocking collectives, on_device(): down = lax.all_to_all(down, ('kv', 'tp'), 0, 0, tiled=True)  9.9 us
    ppermute x6, starting transfers between devices, exchange(): lax.ppermute(message, 'kv', [(i, i ^ j * stride) for i in range(kv)])  8.77 us
    pallas_call x1, Pallas kernels, on_device(): call(cache_load_kernel, 'cache_load', (sds(key_cache.shape, BF), sds(valu...  4.68 us
    pallas_call x1, Pallas kernels, on_device(): call(functools.partial(attend_kernel, width), 'attend', sds((H, 3 * S + S...  2.88 us
    pallas_call x1, Pallas kernels, on_device(): call(other_kernel, 'other', (sds((S + 8, qc), F32), sds((S + 8, vc), F32)...  2.02 us
  transfers between devices with their start and end apart: 8, of which 3 were waited for; matrix products, arithmetic and copies ran while one was open for 0% of the time, Pallas kernels for 11%

profile of v3, /device:TPU:0, one launch (start us, length us, event | category | flops | bytes accessed | tf_op | source)
XLA Modules:
  0.0 70.8 jit_solution(17387682155367221767)
XLA Ops:
  0.0 0.5 collective-permute-start
  0.5 1.1 %first_load.1 = (bf16[256,1024]{1,0:T(8,128)(2,1)S(1)}, bf16[16,128]{1,0:T(8,128)(2,1)S(1)}, bf16[2,128]{1,0:T(2,128)(2,1)S(1)}, s32[16,128]{1,0:T(8,128)S(1)}, f32[16,128]{1,0:T(8,128)S(1)}) custom-call(bf16[256,1024]{1,0:T(8,128)(2,1)} %w_query.1, bf16[16,128]{1,0:T(8,128)(2,1)} %tokens.1, bf16[2,128]{1,0:T(2,128)(2,1)} %bitcast.5, s32[16]{0:T(128)} %lengths.1, ...), custom_call_target="tpu_custom_call" | custom-call | flops 1000000000 | tf_op jit(solution)/shard_map/first_load/pallas_call | solution.py:580
  1.6 0.2 query.1
  1.8 3.7 %collective-permute-start.3 = (bf16[16,1280]{1,0:T(8,128)(2,1)S(1)}, bf16[16,1280]{1,0:T(8,128)(2,1)S(1)}, u32[]{:S(2)}, u32[]{:S(2)}) collective-permute-start(bf16[16,1280]{1,0:T(8,128)(2,1)S(1)} %get-tuple-element.29.after), channel_id=1, source_target_pairs={{0,6},{2,4},{4,2},{6,0},{8,14},{10,12},{12,10},{14,8},{16,22},{18,... | collective-permute-start | bytes 122888 | tf_op jit(solution)/shard_map/ppermute | solution.py:607
  5.6 0.5 collective-permute-start.2
  6.1 0.1 collective-permute-start.1
  6.2 2.0 %other.1 = (f32[24,1024]{1,0:T(8,128)S(1)}, f32[24,2048]{1,0:T(8,128)S(1)}, f32[24,2048]{1,0:T(8,128)S(1)}, f32[2,16,128]{2,1,0:T(8,128)S(1)}, f32[16,16,128]{2,1,0:T(8,128)S(1)}) custom-call(bf16[16,1280]{1,0:T(8,128)(2,1)S(1)} %get-tuple-element.29.after, s32[16,128]{1,0:T(8,128)S(1)} %get-tuple-element.32.lengths, f32[16,128]{1,0:T(8,128)S(1)} %get-tuple-element.33.rates, ...), custom_call_target="tpu_custom_call" | custom-call | flops 1000000000 | tf_op jit(solution)/shard_map/other/pallas_call | solution.py:612
  8.2 0.0 collective-permute-done.3.m3
  8.3 1.3 %collective-permute-done.2.m2 = bf16[16,1280]{1,0:T(8,128)(2,1)S(1)} collective-permute-done((bf16[16,1280]{1,0:T(8,128)(2,1)S(1)}, bf16[16,1280]{1,0:T(8,128)(2,1)S(1)}, u32[]{:S(2)}, u32[]{:S(2)}) %collective-permute-start.2) | collective-permute-done | bytes 40992 | tf_op jit(solution)/shard_map/ppermute | solution.py:607
  9.6 0.5 collective-permute-done.1.m1
  10.1 0.2 middle.1
  10.2 3.6 %collective-permute-start.6 = (bf16[16,1280]{1,0:T(8,128)(2,1)S(1)}, bf16[16,1280]{1,0:T(8,128)(2,1)S(1)}, u32[]{:S(2)}, u32[]{:S(2)}) collective-permute-start(bf16[16,1280]{1,0:T(8,128)(2,1)S(1)} %get-tuple-element.31.after), channel_id=1, source_target_pairs={{0,24},{2,26},{4,28},{6,30},{8,16},{10,18},{12,20},{14,22},{16,8},... | collective-permute-start | bytes 122888 | tf_op jit(solution)/shard_map/ppermute | solution.py:607
  13.8 0.8 %collective-permute-start.4 = (bf16[16,1280]{1,0:T(8,128)(2,1)S(1)}, bf16[16,1280]{1,0:T(8,128)(2,1)S(1)}, u32[]{:S(2)}, u32[]{:S(2)}) collective-permute-start(bf16[16,1280]{1,0:T(8,128)(2,1)S(1)} %get-tuple-element.31.after), channel_id=1, source_target_pairs={{0,8},{2,10},{4,12},{6,14},{8,0},{10,2},{12,4},{14,6},{16,24},{18,... | collective-permute-start | bytes 122888 | tf_op jit(solution)/shard_map/ppermute | solution.py:607
  14.6 4.7 %cache_load.1 = (bf16[16,128,1024]{2,1,0:T(8,128)(2,1)S(1)}, bf16[16,128,2048]{2,1,0:T(8,128)(2,1)S(1)}) custom-call(bf16[16,1280]{1,0:T(8,128)(2,1)S(1)} %get-tuple-element.31.after, bf16[16,128,1024]{2,1,0:T(8,128)(2,1)} %keys.1, bf16[16,128,2048]{2,1,0:T(8,128)(2,1)} %values.1), custom_call_target="tpu_custom_call" | custom-call | flops 1000000000 | tf_op jit(solution)/shard_map/cache_load/pallas_call | solution.py:636
  19.3 0.0 collective-permute-done.6.m3
  19.3 0.0 collective-permute-done.4.m1
  19.3 0.0 copy-start.4
  19.4 0.0 copy-start.2
  19.4 0.0 copy-start
  19.4 0.0 copy-start.1
  19.4 0.0 copy-start.3
  19.4 2.9 %attend.1 = bf16[16,56,128]{2,1,0:T(8,128)(2,1)S(1)} custom-call(f32[16,1280]{1,0:T(8,128)S(1)} %get-tuple-element.30.old, bf16[16,1280]{1,0:T(8,128)(2,1)S(1)} %collective-permute-done.4.m1, bf16[16,1280]{1,0:T(8,128)(2,1)S(1)} %collective-permute-done.5.m2, bf16[16,1280]{1,0:T(8,128)(2,1)S(1)} %collective-permute-done.6.m3, ...), custom_call_target="tpu_custom_call" | custom-call | tf_op jit(solution)/shard_map/attend/pallas_call | solution.py:646
  22.3 14.1 %all_to_all.20.pieces = bf16[16,56,128]{2,1,0:T(8,128)(2,1)S(1)} all-to-all(bf16[16,56,128]{2,1,0:T(8,128)(2,1)S(1)} %attend.1), channel_id=1, replica_groups=mesh['kv'=16,'tp'=2] {'kv'}, dimensions={0} | all-to-all | bytes 458752 | tf_op jit(solution)/shard_map/all_to_all | solution.py:655
  36.4 0.4 gate.1
  36.8 10.6 %all_to_all.21.gated = bf16[16,16,128]{2,1,0:T(8,128)(2,1)S(1)} all-to-all(bf16[16,16,128]{2,1,0:T(8,128)(2,1)S(1)} %gate.1), channel_id=1, replica_groups=mesh['kv'=16,'tp'=2] {'kv'}, dimensions={0} | all-to-all | bytes 131072 | tf_op jit(solution)/shard_map/all_to_all | solution.py:659
  47.4 0.2 output.1
  47.7 0.0 collective-permute-start.7
  47.7 1.2 %collective-permute-done.7.got = bf16[16,128]{1,0:T(8,128)(2,1)S(1)} collective-permute-done((bf16[16,128]{1,0:T(8,128)(2,1)S(1)}, bf16[16,128]{1,0:T(8,128)(2,1)S(1)}, u32[]{:S(2)}, u32[]{:S(2)}) %collective-permute-start.7) | collective-permute-done | bytes 4128 | tf_op jit(solution)/shard_map/ppermute | solution.py:663
  48.9 9.9 %all_to_all.22.residual = bf16[32,16,128]{2,1,0:T(8,128)(2,1)S(1)} all-to-all(bf16[32,16,128]{2,1,0:T(8,128)(2,1)S(1)} %get-tuple-element.43), channel_id=1, replica_groups=mesh['kv'=16,'tp'=2] {'kv','tp'}, dimensions={0} | all-to-all | bytes 262144 | tf_op jit(solution)/shard_map/all_to_all | solution.py:671
  58.8 1.5 %mixer.1 = bf16[32,16,128]{2,1,0:T(8,128)(2,1)S(1)} custom-call(bf16[32,16,128]{2,1,0:T(8,128)(2,1)S(1)} %all_to_all.22.residual, bf16[32,128]{1,0:T(8,128)(2,1)S(1)} %bitcast.3, bf16[4096,512]{1,0:T(8,128)(2,1)S(1)} %copy-done, bf16[512,4096]{1,0:T(8,128)(2,1)S(1)} %copy-done.1), custom_call_target="tpu_custom_call" | custom-call | tf_op jit(solution)/shard_map/mixer/pallas_call | solution.py:672
  60.2 9.9 %all_to_all.23.pieces = bf16[32,16,128]{2,1,0:T(8,128)(2,1)S(1)} all-to-all(bf16[32,16,128]{2,1,0:T(8,128)(2,1)S(1)} %mixer.1), channel_id=1, replica_groups=mesh['kv'=16,'tp'=2] {'kv','tp'}, dimensions={0} | all-to-all | bytes 262144 | tf_op jit(solution)/shard_map/all_to_all | solution.py:675
  70.1 0.6 final.1
  (9 shorter events, 0.0 us)
Async XLA Ops:
  0.0 1.6 %collective-permute-start = (bf16[16,128]{1,0:T(8,128)(2,1)}, bf16[16,128]{1,0:T(8,128)(2,1)S(1)}, u32[]{:S(2)}, u32[]{:S(2)}) collective-permute-start(bf16[16,128]{1,0:T(8,128)(2,1)} %tokens.1), channel_id=1, source_target_pairs={{0,1},{1,0},{2,3},{3,2},{4,5},{5,4},{6,7},{7,6},{8,9},{9,8},{10,11... | collective-permute-start | bytes 12296 | tf_op jit(solution)/shard_map/ppermute | solution.py:578
  1.8 6.4 %collective-permute-start.3 = (bf16[16,1280]{1,0:T(8,128)(2,1)S(1)}, bf16[16,1280]{1,0:T(8,128)(2,1)S(1)}, u32[]{:S(2)}, u32[]{:S(2)}) collective-permute-start(bf16[16,1280]{1,0:T(8,128)(2,1)S(1)} %get-tuple-element.29.after), channel_id=1, source_target_pairs={{0,6},{2,4},{4,2},{6,0},{8,14},{10,12},{12,10},{14,8},{16,22},{18,... | collective-permute-start | bytes 122888 | tf_op jit(solution)/shard_map/ppermute | solution.py:607
  5.6 4.0 %collective-permute-start.2 = (bf16[16,1280]{1,0:T(8,128)(2,1)S(1)}, bf16[16,1280]{1,0:T(8,128)(2,1)S(1)}, u32[]{:S(2)}, u32[]{:S(2)}) collective-permute-start(bf16[16,1280]{1,0:T(8,128)(2,1)S(1)} %get-tuple-element.29.after), channel_id=1, source_target_pairs={{0,4},{2,6},{4,0},{6,2},{8,12},{10,14},{12,8},{14,10},{16,20},{18,... | collective-permute-start | bytes 122888 | tf_op jit(solution)/shard_map/ppermute | solution.py:607
  6.1 4.0 %collective-permute-start.1 = (bf16[16,1280]{1,0:T(8,128)(2,1)S(1)}, bf16[16,1280]{1,0:T(8,128)(2,1)S(1)}, u32[]{:S(2)}, u32[]{:S(2)}) collective-permute-start(bf16[16,1280]{1,0:T(8,128)(2,1)S(1)} %get-tuple-element.29.after), channel_id=1, source_target_pairs={{0,2},{2,0},{4,6},{6,4},{8,10},{10,8},{12,14},{14,12},{16,18},{18,... | collective-permute-start | bytes 122888 | tf_op jit(solution)/shard_map/ppermute | solution.py:607
  10.2 9.1 %collective-permute-start.6 = (bf16[16,1280]{1,0:T(8,128)(2,1)S(1)}, bf16[16,1280]{1,0:T(8,128)(2,1)S(1)}, u32[]{:S(2)}, u32[]{:S(2)}) collective-permute-start(bf16[16,1280]{1,0:T(8,128)(2,1)S(1)} %get-tuple-element.31.after), channel_id=1, source_target_pairs={{0,24},{2,26},{4,28},{6,30},{8,16},{10,18},{12,20},{14,22},{16,8},... | collective-permute-start | bytes 122888 | tf_op jit(solution)/shard_map/ppermute | solution.py:607
  13.8 5.5 %collective-permute-start.5 = (bf16[16,1280]{1,0:T(8,128)(2,1)S(1)}, bf16[16,1280]{1,0:T(8,128)(2,1)S(1)}, u32[]{:S(2)}, u32[]{:S(2)}) collective-permute-start(bf16[16,1280]{1,0:T(8,128)(2,1)S(1)} %get-tuple-element.31.after), channel_id=1, source_target_pairs={{0,16},{2,18},{4,20},{6,22},{8,24},{10,26},{12,28},{14,30},{16,0},... | collective-permute-start | bytes 122888 | tf_op jit(solution)/shard_map/ppermute | solution.py:607
  13.8 5.5 %collective-permute-start.4 = (bf16[16,1280]{1,0:T(8,128)(2,1)S(1)}, bf16[16,1280]{1,0:T(8,128)(2,1)S(1)}, u32[]{:S(2)}, u32[]{:S(2)}) collective-permute-start(bf16[16,1280]{1,0:T(8,128)(2,1)S(1)} %get-tuple-element.31.after), channel_id=1, source_target_pairs={{0,8},{2,10},{4,12},{6,14},{8,0},{10,2},{12,4},{14,6},{16,24},{18,... | collective-permute-start | bytes 122888 | tf_op jit(solution)/shard_map/ppermute | solution.py:607
  19.3 17.0 %copy-start.4 = (bf16[2048]{0:T(1024)(128)(2,1)S(1)}, bf16[2048]{0:T(1024)(128)(2,1)}, u32[]{:S(2)}) copy-start(bf16[2048]{0:T(1024)(128)(2,1)} %param.25) | copy-start | bytes 12292
  19.4 28.1 %copy-start.2 = (bf16[2048,256]{1,0:T(8,128)(2,1)S(1)}, bf16[2048,256]{1,0:T(8,128)(2,1)}, u32[]{:S(2)}) copy-start(bf16[2048,256]{1,0:T(8,128)(2,1)} %w_output.1) | copy-start | bytes 3145732
  19.4 39.4 %copy-start = (bf16[4096,512]{1,0:T(8,128)(2,1)S(1)}, bf16[4096,512]{1,0:T(8,128)(2,1)}, u32[]{:S(2)}) copy-start(bf16[4096,512]{1,0:T(8,128)(2,1)} %w_up.1) | copy-start | bytes 12582916
  19.4 39.4 %copy-start.1 = (bf16[512,4096]{1,0:T(8,128)(2,1)S(1)}, bf16[512,4096]{1,0:T(8,128)(2,1)}, u32[]{:S(2)}) copy-start(bf16[512,4096]{1,0:T(8,128)(2,1)} %w_down.1) | copy-start | bytes 12582916
  19.4 39.4 %copy-start.3 = (bf16[4096]{0:T(1024)(128)(2,1)S(1)}, bf16[4096]{0:T(1024)(128)(2,1)}, u32[]{:S(2)}) copy-start(bf16[4096]{0:T(1024)(128)(2,1)} %param.27) | copy-start | bytes 24580
  47.7 1.2 %collective-permute-start.7 = (bf16[16,128]{1,0:T(8,128)(2,1)S(1)}, bf16[16,128]{1,0:T(8,128)(2,1)S(1)}, u32[]{:S(2)}, u32[]{:S(2)}) collective-permute-start(bf16[16,128]{1,0:T(8,128)(2,1)S(1)} %get-tuple-element.42), channel_id=1, source_target_pairs={{0,1},{1,0},{2,3},{3,2},{4,5},{5,4},{6,7},{7,6},{8,9},{9,8},{10,11... | collective-permute-start | bytes 12296 | tf_op jit(solution)/shard_map/ppermute | solution.py:663

commit v4 on v3

--- a/solution.py
+++ b/solution.py
@@ -7,6 +7,7 @@
 from jax.experimental import pallas as pl
 from jax.experimental.pallas import tpu as pltpu
 from jax.sharding import PartitionSpec as P
+
 
 HEAD_KEY = 64
 HEAD_VALUE = 128
@@ -295,15 +296,10 @@
         copy.wait()
 
 
-def cache_load_kernel(after, keys, values, keys_out, values_out, sems):
-    copies = (
-        pltpu.make_async_copy(keys, keys_out, sems.at[0]),
-        pltpu.make_async_copy(values, values_out, sems.at[1]),
-    )
-    for copy in copies:
-        copy.start()
-    for copy in copies:
-        copy.wait()
+def cache_load_kernel(after, values, values_out, sem):
+    copy = pltpu.make_async_copy(values, values_out, sem)
+    copy.start()
+    copy.wait()
 
 
 def query_kernel(first, second, gain, w_query, state, message):
@@ -341,22 +337,35 @@
     w_key,
     w_value,
     w_gate,
+    w_output,
+    keys,
     k_out,
     v_out,
     g_out,
     turn,
     weights,
+    w_keep,
+    w_send,
+    keys_out,
     key_buffer,
     value_buffer,
     gate_buffer,
     sems,
 ):
-    sources = (w_key, w_value, w_gate)
+    own = w_keep.shape[1]
+    t = lax.axis_index("tp")
+    kept = pl.ds(pl.multiple_of(t * own, own), own)
+    sent = pl.ds(pl.multiple_of((1 - t) * own, own), own)
     buffers = (key_buffer, value_buffer, gate_buffer)
-    copies = [
-        pltpu.make_async_copy(source, buffer, sems.at[i])
-        for i, (source, buffer) in enumerate(zip(sources, buffers))
-    ]
+    pairs = (
+        (w_key, key_buffer),
+        (w_value, value_buffer),
+        (w_gate, gate_buffer),
+        (w_output.at[:, sent], w_send),
+        (w_output.at[:, kept], w_keep),
+        (keys, keys_out),
+    )
+    copies = [pltpu.make_async_copy(a, b, sems.at[i]) for i, (a, b) in enumerate(pairs)]
     for copy in copies:
         copy.start()
     lhs, wide = projection_rows(first, second, gain)
@@ -378,10 +387,13 @@
         copy.wait()
         product = jnp.dot(lhs, buffer[...], preferred_element_type=F32)
         out[...] = product[: rows + 8]
+    for copy in copies[len(buffers) :]:
+        copy.wait()
 
 
 def attend_kernel(
     width,
+    after,
     old,
     m1,
     m2,
@@ -397,7 +409,7 @@
     query_rows,
     cached,
 ):
-    rows, span, key_columns = keys.shape
+    rows, _, key_columns = keys.shape
     heads = key_columns // HEAD_KEY
     q, csum, moments = unpack_sum(old, (m1, m2, m3))
     average = moments[:, 0:1] / width
@@ -476,19 +488,14 @@
     out[...] = jnp.broadcast_to(gated[None], out.shape)
 
 
-def output_kernel(gated, w_output, keep, send):
-    heads = gated.shape[0]
-    lhs = jnp.concatenate([gated[h] for h in range(heads)], 1)
-    part = jnp.dot(lhs, w_output[...], preferred_element_type=F32)
+def output_kernel(gated, w_keep, w_got, tokens, own, out):
+    heads = gated.shape[0] // 2
     t = lax.axis_index("tp")
-    half = keep.shape[1]
-    low, high = part[:, :half], part[:, half:]
-    keep[...] = jnp.where(t == 0, low, high).astype(BF)
-    send[...] = jnp.where(t == 0, high, low).astype(BF)
-
-
-def residual_kernel(tokens, keep, got, own, out):
-    branch = keep[...].astype(F32) + got[...].astype(F32)
+    branch = 0.0
+    for group, w in ((t, w_keep), (1 - t, w_got)):
+        lhs = jnp.concatenate([gated[2 * h + group] for h in range(heads)], 1)
+        part = jnp.dot(lhs, w[...], preferred_element_type=F32)
+        branch = branch + part.astype(BF).astype(F32)
     residual = (tokens[...].astype(F32) + branch).astype(BF)
     own[...] = residual
     out[...] = jnp.broadcast_to(residual[None], out.shape)
@@ -533,10 +540,9 @@
     return [pltpu.with_memory_space_constraint(x, pltpu.HBM) for x in arrays]
 
 
-def call(kernel, name, outs, in_specs, flops=0, bytes_accessed=0, scratch=(), limit=None):
+def call(kernel, outs, in_specs, flops=0, bytes_accessed=0, scratch=(), limit=None):
     return pl.pallas_call(
         kernel,
-        name=name,
         out_shape=outs,
         in_specs=in_specs,
         out_specs=jax.tree.map(lambda _: VMEM, outs),
@@ -568,7 +574,6 @@
     ):
         S, own = tokens.shape
         H = decay_rate.shape[0]
-        span = key_cache.shape[1]
         width = own * kv * tp
         qc, vc = H * HEAD_KEY, H * HEAD_VALUE
         swap = [(0, 1), (1, 0)]
@@ -579,7 +584,6 @@
         gain = attn_gain.reshape(-1, LANES)
         w_query, tokens, gain, length_rows, rates = call(
             first_load_kernel,
-            "first_load",
             (
                 sds(w_query.shape, BF),
                 sds(tokens.shape, BF),
@@ -599,7 +603,7 @@
         columns = qc + 2 * LANES
         message_types = (sds((S, columns), F32), sds((S, columns), BF))
         state, message = call(
-            query_kernel, "query", message_types, [VMEM] * 4, limit=2 * mib
+            query_kernel, message_types, [VMEM] * 4, limit=2 * mib
         )(tokens, other, gain, w_query)
 
         def exchange(message, stride):
@@ -609,73 +613,75 @@
             ]
 
         got = exchange(message, 1)
-        k_part, v_part, g_part, turn, weights = call(
+        k_part, v_part, g_part, turn, weights, w_keep, w_send, keys = call(
             other_kernel,
-            "other",
             (
                 sds((S + 8, qc), F32),
                 sds((S + 8, vc), F32),
                 sds((S + 8, vc), F32),
                 sds((2, S, LANES), F32),
                 sds((S, H, LANES), F32),
+                sds((w_output.shape[0], own), BF),
+                sds((w_output.shape[0], own), BF),
+                sds(key_cache.shape, BF),
             ),
-            [ANY] + [VMEM] * 5 + [HBM] * 3,
+            [ANY] + [VMEM] * 5 + [HBM] * 5,
             flops=10**9,
             scratch=[pltpu.VMEM(w.shape, BF) for w in (w_key, w_value, w_gate)]
-            + [pltpu.SemaphoreType.DMA((3,))],
+            + [pltpu.SemaphoreType.DMA((6,))],
             limit=6 * mib,
-        )(message, length_rows, rates, tokens, other, gain, *in_hbm(w_key, w_value, w_gate))
+        )(
+            message,
+            length_rows,
+            rates,
+            tokens,
+            other,
+            gain,
+            *in_hbm(w_key, w_value, w_gate, w_output, key_cache),
+        )
+        w_got = lax.ppermute(w_send, "tp", swap)
 
         stride = 4
         while stride < kv:
             state, message = call(
-                middle_kernel, "middle", message_types, [VMEM] * 4, limit=2 * mib
+                middle_kernel, message_types, [VMEM] * 4, limit=2 * mib
             )(state, *got)
             got = exchange(message, stride)
             stride *= 4
-        keys, values = call(
+        values = call(
             cache_load_kernel,
-            "cache_load",
-            (sds(key_cache.shape, BF), sds(value_cache.shape, BF)),
-            [ANY] + [HBM] * 2,
+            sds(value_cache.shape, BF),
+            [ANY, HBM],
             flops=10**9,
-            scratch=[pltpu.SemaphoreType.DMA((2,))],
+            scratch=[pltpu.SemaphoreType.DMA],
             limit=2 * mib,
-        )(message, *in_hbm(key_cache, value_cache))
+        )(message, *in_hbm(value_cache))
 
         pieces = call(
             functools.partial(attend_kernel, width),
-            "attend",
             sds((H, 3 * S + S // 2, LANES), BF),
-            [VMEM] * 11,
+            [ANY] + [VMEM] * 11,
             scratch=[pltpu.VMEM((S, qc), F32), pltpu.VMEM((S, vc), F32)],
             limit=4 * mib,
-        )(state, *got, k_part, v_part, g_part, turn, weights, keys, values)
+        )(w_got, state, *got, k_part, v_part, g_part, turn, weights, keys, values)
 
         pieces = lax.all_to_all(pieces, "kv", 0, 0, tiled=True)
-        spread = call(gate_kernel, "gate", sds((kv, S, LANES), BF), [VMEM] * 2, limit=2 * mib)(
-            pieces, head_gain.reshape(H, HEAD_VALUE)
-        )
-        gated = lax.all_to_all(spread, "kv", 0, 0, tiled=True)
-        keep, send = call(
-            output_kernel, "output", (sds((S, own), BF),) * 2, [VMEM] * 2, limit=4 * mib
-        )(gated, w_output)
-        got = lax.ppermute(send, "tp", swap)
+        gated = call(
+            gate_kernel, sds((kv * tp, S, LANES), BF), [VMEM] * 2, limit=2 * mib
+        )(pieces, head_gain.reshape(H, HEAD_VALUE))
+        gated = lax.all_to_all(gated, ("kv", "tp"), 0, 0, tiled=True)
         residual, spread = call(
-            residual_kernel,
-            "residual",
+            output_kernel,
             (sds((S, own), BF), sds((kv * tp, S, own), BF)),
-            [VMEM] * 3,
-            limit=2 * mib,
-        )(tokens, keep, got)
+            [VMEM] * 4,
+            limit=4 * mib,
+        )(gated, w_keep, w_got, tokens)
         spread = lax.all_to_all(spread, ("kv", "tp"), 0, 0, tiled=True)
         down = call(
-            mixer_kernel, "mixer", sds((kv * tp, S, own), BF), [VMEM] * 4, limit=16 * mib
+            mixer_kernel, sds((kv * tp, S, own), BF), [VMEM] * 4, limit=16 * mib
         )(spread, mlp_gain.reshape(-1, LANES), w_up, w_down)
         down = lax.all_to_all(down, ("kv", "tp"), 0, 0, tiled=True)
-        return call(final_kernel, "final", sds((S, own), BF), [VMEM] * 2, limit=2 * mib)(
-            down, residual
-        )
+        return call(final_kernel, sds((S, own), BF), [VMEM] * 2, limit=2 * mib)(down, residual)
 
     return on_device
 

time: 71 us -> 72.1 us (1.015)
  waiting for transfers between devices: 3.01 us -> 4.66 us
  blocking collectives: 44.5 us -> 43.7 us
    ppermute x6, waiting for transfers between devices: 1.84 us -> 4.65 us  [exchange(): lax.ppermute(message, 'kv', [(i, i ^ j * stride) for i in range(kv)])]
    ppermute x1, waiting for transfers between devices: 1.17 us -> 0.01 us  [on_device(): w_got = lax.ppermute(w_send, 'tp', swap)]
    pallas_call x11 -> x10, Pallas kernels: 13.8 us -> 13.9 us  [the longest x1 3.39 us: on_device(): call(cache_load_kernel, sds(value_cache.shape, BF), [ANY, HBM], flops=10...]
  transfers between devices with their start and end apart: 8 -> 8, of which waited for: 3 -> 4; matrix products, arithmetic and copies ran while one was open for 0% -> 0% of each run, Pallas kernels for 11% -> 6%
where the time goes in v4:
time: 72.1 us; the launch traced here: 71.8 us
  blocking collectives  43.7 us (61%)
  Pallas kernels  13.9 us (19%)
  starting transfers between devices  9.45 us (13%)
  waiting for transfers between devices  4.66 us (6%)
    all_to_all x1, blocking collectives, on_device(): pieces = lax.all_to_all(pieces, 'kv', 0, 0, tiled=True)  13.4 us
    all_to_all x1, blocking collectives, on_device(): gated = lax.all_to_all(gated, ('kv', 'tp'), 0, 0, tiled=True)  10.3 us
    all_to_all x1, blocking collectives, on_device(): down = lax.all_to_all(down, ('kv', 'tp'), 0, 0, tiled=True)  9.97 us
    all_to_all x1, blocking collectives, on_device(): spread = lax.all_to_all(spread, ('kv', 'tp'), 0, 0, tiled=True)  9.97 us
    ppermute x6, starting transfers between devices, exchange(): lax.ppermute(message, 'kv', [(i, i ^ j * stride) for i in range(kv)])  8.65 us
    ppermute x6, waiting for transfers between devices, exchange(): lax.ppermute(message, 'kv', [(i, i ^ j * stride) for i in range(kv)])  4.65 us
    pallas_call x1, Pallas kernels, on_device(): call(cache_load_kernel, sds(value_cache.shape, BF), [ANY, HBM], flops=10...  3.39 us
    pallas_call x1, Pallas kernels, on_device(): call(other_kernel, (sds((S + 8, qc), F32), sds((S + 8, vc), F32), sds((S...  3.39 us
  transfers between devices with their start and end apart: 8, of which 4 were waited for; matrix products, arithmetic and copies ran while one was open for 0% of the time, Pallas kernels for 6%

profile of v4, /device:TPU:0, one launch (start us, length us, event | category | flops | bytes accessed | tf_op | source)
XLA Modules:
  0.0 71.8 jit_solution(12446860745445121481)
XLA Ops:
  0.0 0.5 collective-permute-start
  0.5 1.1 %shard_map.145 = (bf16[256,1024]{1,0:T(8,128)(2,1)S(1)}, bf16[16,128]{1,0:T(8,128)(2,1)S(1)}, bf16[2,128]{1,0:T(2,128)(2,1)S(1)}, s32[16,128]{1,0:T(8,128)S(1)}, f32[16,128]{1,0:T(8,128)S(1)}) custom-call(bf16[256,1024]{1,0:T(8,128)(2,1)} %w_query.1, bf16[16,128]{1,0:T(8,128)(2,1)} %tokens.1, bf16[2,128]{1,0:T(2,128)(2,1)} %bitcast.5, s32[16]{0:T(128)} %lengths.1, ...), custom_call_target="tpu_custom_call" | custom-call | flops 1000000000 | tf_op jit(solution)/shard_map/pallas_call | solution.py:585
  1.6 0.0 collective-permute-done.second
  1.6 0.2 shard_map.146
  1.8 3.4 %shard_map.147 = (f32[24,1024]{1,0:T(8,128)S(1)}, f32[24,2048]{1,0:T(8,128)S(1)}, f32[24,2048]{1,0:T(8,128)S(1)}, f32[2,16,128]{2,1,0:T(8,128)S(1)}, f32[16,16,1...) custom-call(bf16[16,1280]{1,0:T(8,128)(2,1)S(1)} %get-tuple-element., ...), custom_call_target="tpu_custom_call" | custom-call | flops 1000000000 | tf_op jit(solution)/shard_map/pallas_call | solution.py:616
  5.2 0.3 collective-permute-start.1
  5.5 3.7 %collective-permute-start.4 = (bf16[16,1280]{1,0:T(8,128)(2,1)S(1)}, bf16[16,1280]{1,0:T(8,128)(2,1)S(1)}, u32[]{:S(2)}, u32[]{:S(2)}) collective-permute-start(bf16[16,1280]{1,0:T(8,128)(2,1)S(1)} %get-tuple-element.27.after), channel_id=1, source_target_pairs={{0,6},{2,4},{4,2},{6,0},{8,14},{10,12},{12,10},{14,8},{16,22},{18,... | collective-permute-start | bytes 122888 | tf_op jit(solution)/shard_map/ppermute | solution.py:611
  9.2 0.5 collective-permute-start.3
  9.7 0.1 collective-permute-start.2
  9.8 1.4 %collective-permute-done.4.m3 = bf16[16,1280]{1,0:T(8,128)(2,1)S(1)} collective-permute-done((bf16[16,1280]{1,0:T(8,128)(2,1)S(1)}, bf16[16,1280]{1,0:T(8,128)(2,1)S(1)}, u32[]{:S(2)}, u32[]{:S(2)}) %collective-permute-start.4) | collective-permute-done | bytes 40992 | tf_op jit(solution)/shard_map/ppermute | solution.py:611
  11.2 2.0 %collective-permute-done.3.m2 = bf16[16,1280]{1,0:T(8,128)(2,1)S(1)} collective-permute-done((bf16[16,1280]{1,0:T(8,128)(2,1)S(1)}, bf16[16,1280]{1,0:T(8,128)(2,1)S(1)}, u32[]{:S(2)}, u32[]{:S(2)}) %collective-permute-start.3) | collective-permute-done | bytes 40992 | tf_op jit(solution)/shard_map/ppermute | solution.py:611
  13.2 0.5 collective-permute-done.2.m1
  13.7 0.2 shard_map.148
  13.9 3.6 %collective-permute-start.7 = (bf16[16,1280]{1,0:T(8,128)(2,1)S(1)}, bf16[16,1280]{1,0:T(8,128)(2,1)S(1)}, u32[]{:S(2)}, u32[]{:S(2)}) collective-permute-start(bf16[16,1280]{1,0:T(8,128)(2,1)S(1)} %get-tuple-element.33.after), channel_id=1, source_target_pairs={{0,24},{2,26},{4,28},{6,30},{8,16},{10,18},{12,20},{14,22},{16,8},... | collective-permute-start | bytes 122888 | tf_op jit(solution)/shard_map/ppermute | solution.py:611
  17.5 0.0 collective-permute-start.6
  17.5 0.8 %collective-permute-start.5 = (bf16[16,1280]{1,0:T(8,128)(2,1)S(1)}, bf16[16,1280]{1,0:T(8,128)(2,1)S(1)}, u32[]{:S(2)}, u32[]{:S(2)}) collective-permute-start(bf16[16,1280]{1,0:T(8,128)(2,1)S(1)} %get-tuple-element.33.after), channel_id=1, source_target_pairs={{0,8},{2,10},{4,12},{6,14},{8,0},{10,2},{12,4},{14,6},{16,24},{18,... | collective-permute-start | bytes 122888 | tf_op jit(solution)/shard_map/ppermute | solution.py:611
  18.3 3.4 %shard_map.149.values = bf16[16,128,2048]{2,1,0:T(8,128)(2,1)S(1)} custom-call(bf16[16,1280]{1,0:T(8,128)(2,1)S(1)} %get-tuple-element.33.after, bf16[16,128,2048]{2,1,0:T(8,128)(2,1)} %values.1), custom_call_target="tpu_custom_call" | custom-call | flops 1000000000 | tf_op jit(solution)/shard_map/pallas_call | solution.py:651
  21.7 0.0 collective-permute-done.7.m3
  21.7 0.7 collective-permute-done.6.m2
  22.4 0.0 collective-permute-done.5.m1
  22.4 0.0 copy-start
  22.4 0.0 copy-start.1
  22.4 0.0 copy-start.2
  22.5 3.0 %shard_map.150 = bf16[16,56,128]{2,1,0:T(8,128)(2,1)S(1)} custom-call(bf16[2048,128]{1,0:T(8,128)(2,1)S(1)} %collective-permute-done.1.after.w_got, f32[16,1280]{1,0:T(8,128)S(1)} %get-tuple-element.32.old, bf16[16,1280]{1,0:T(8,128)(2,1)S(1)} %collective-permute-done.5.m1, bf16[16,1280]{1,0:T(8,128)(2,1)S(1)} %collective-permute-done.6.m2, ...), custom_call_target="tpu_custom_call" | custom-call | tf_op jit(solution)/shard_map/pallas_call | solution.py:660
  25.4 13.4 %all_to_all.20.pieces = bf16[16,56,128]{2,1,0:T(8,128)(2,1)S(1)} all-to-all(bf16[16,56,128]{2,1,0:T(8,128)(2,1)S(1)} %shard_map.150), channel_id=1, replica_groups=mesh['kv'=16,'tp'=2] {'kv'}, dimensions={0} | all-to-all | bytes 458752 | tf_op jit(solution)/shard_map/all_to_all | solution.py:668
  38.8 0.4 shard_map.151
  39.2 10.3 %all_to_all.21.gated = bf16[32,16,128]{2,1,0:T(8,128)(2,1)S(1)} all-to-all(bf16[32,16,128]{2,1,0:T(8,128)(2,1)S(1)} %shard_map.151), channel_id=1, replica_groups=mesh['kv'=16,'tp'=2] {'kv','tp'}, dimensions={0} | all-to-all | bytes 262144 | tf_op jit(solution)/shard_map/all_to_all | solution.py:672
  49.5 0.3 shard_map.152
  49.8 10.0 %all_to_all.22.residual = bf16[32,16,128]{2,1,0:T(8,128)(2,1)S(1)} all-to-all(bf16[32,16,128]{2,1,0:T(8,128)(2,1)S(1)} %get-tuple-element.41), channel_id=1, replica_groups=mesh['kv'=16,'tp'=2] {'kv','tp'}, dimensions={0} | all-to-all | bytes 262144 | tf_op jit(solution)/shard_map/all_to_all | solution.py:679
  59.8 1.5 %shard_map.153 = bf16[32,16,128]{2,1,0:T(8,128)(2,1)S(1)} custom-call(bf16[32,16,128]{2,1,0:T(8,128)(2,1)S(1)} %all_to_all.22.residual, bf16[32,128]{1,0:T(8,128)(2,1)S(1)} %bitcast.3, bf16[4096,512]{1,0:T(8,128)(2,1)S(1)} %copy-done, bf16[512,4096]{1,0:T(8,128)(2,1)S(1)} %copy-done.1), custom_call_target="tpu_custom_call" | custom-call | tf_op jit(solution)/shard_map/pallas_call | solution.py:680
  61.2 10.0 %all_to_all.23.pieces = bf16[32,16,128]{2,1,0:T(8,128)(2,1)S(1)} all-to-all(bf16[32,16,128]{2,1,0:T(8,128)(2,1)S(1)} %shard_map.153), channel_id=1, replica_groups=mesh['kv'=16,'tp'=2] {'kv','tp'}, dimensions={0} | all-to-all | bytes 262144 | tf_op jit(solution)/shard_map/all_to_all | solution.py:683
  71.2 0.6 shard_map.154
  (6 shorter events, 0.0 us)
Async XLA Ops:
  0.0 1.6 %collective-permute-start = (bf16[16,128]{1,0:T(8,128)(2,1)}, bf16[16,128]{1,0:T(8,128)(2,1)S(1)}, u32[]{:S(2)}, u32[]{:S(2)}) collective-permute-start(bf16[16,128]{1,0:T(8,128)(2,1)} %tokens.1), channel_id=1, source_target_pairs={{0,1},{1,0},{2,3},{3,2},{4,5},{5,4},{6,7},{7,6},{8,9},{9,8},{10,11... | collective-permute-start | bytes 12296 | tf_op jit(solution)/shard_map/ppermute | solution.py:583
  5.2 17.2 %collective-permute-start.1 = (bf16[2048,128]{1,0:T(8,128)(2,1)S(1)}, bf16[2048,128]{1,0:T(8,128)(2,1)S(1)}, u32[]{:S(2)}, u32[]{:S(2)}) collective-permute-start(bf16[2048,128]{1,0:T(8,128)(2,1)S(1)} %get-tuple-element.30), channel_id=1, source_target_pairs={{0,1},{1,0},{2,3},{3,2},{4,5},{5,4},{6,7},{7,6},{8,9},{9,8},{10,11... | collective-permute-start | bytes 1572872 | tf_op jit(solution)/shard_map/ppermute | solution.py:642
  5.5 5.7 %collective-permute-start.4 = (bf16[16,1280]{1,0:T(8,128)(2,1)S(1)}, bf16[16,1280]{1,0:T(8,128)(2,1)S(1)}, u32[]{:S(2)}, u32[]{:S(2)}) collective-permute-start(bf16[16,1280]{1,0:T(8,128)(2,1)S(1)} %get-tuple-element.27.after), channel_id=1, source_target_pairs={{0,6},{2,4},{4,2},{6,0},{8,14},{10,12},{12,10},{14,8},{16,22},{18,... | collective-permute-start | bytes 122888 | tf_op jit(solution)/shard_map/ppermute | solution.py:611
  9.2 4.0 %collective-permute-start.3 = (bf16[16,1280]{1,0:T(8,128)(2,1)S(1)}, bf16[16,1280]{1,0:T(8,128)(2,1)S(1)}, u32[]{:S(2)}, u32[]{:S(2)}) collective-permute-start(bf16[16,1280]{1,0:T(8,128)(2,1)S(1)} %get-tuple-element.27.after), channel_id=1, source_target_pairs={{0,4},{2,6},{4,0},{6,2},{8,12},{10,14},{12,8},{14,10},{16,20},{18,... | collective-permute-start | bytes 122888 | tf_op jit(solution)/shard_map/ppermute | solution.py:611
  9.7 4.0 %collective-permute-start.2 = (bf16[16,1280]{1,0:T(8,128)(2,1)S(1)}, bf16[16,1280]{1,0:T(8,128)(2,1)S(1)}, u32[]{:S(2)}, u32[]{:S(2)}) collective-permute-start(bf16[16,1280]{1,0:T(8,128)(2,1)S(1)} %get-tuple-element.27.after), channel_id=1, source_target_pairs={{0,2},{2,0},{4,6},{6,4},{8,10},{10,8},{12,14},{14,12},{16,18},{18,... | collective-permute-start | bytes 122888 | tf_op jit(solution)/shard_map/ppermute | solution.py:611
  13.9 7.8 %collective-permute-start.7 = (bf16[16,1280]{1,0:T(8,128)(2,1)S(1)}, bf16[16,1280]{1,0:T(8,128)(2,1)S(1)}, u32[]{:S(2)}, u32[]{:S(2)}) collective-permute-start(bf16[16,1280]{1,0:T(8,128)(2,1)S(1)} %get-tuple-element.33.after), channel_id=1, source_target_pairs={{0,24},{2,26},{4,28},{6,30},{8,16},{10,18},{12,20},{14,22},{16,8},... | collective-permute-start | bytes 122888 | tf_op jit(solution)/shard_map/ppermute | solution.py:611
  17.5 4.9 %collective-permute-start.6 = (bf16[16,1280]{1,0:T(8,128)(2,1)S(1)}, bf16[16,1280]{1,0:T(8,128)(2,1)S(1)}, u32[]{:S(2)}, u32[]{:S(2)}) collective-permute-start(bf16[16,1280]{1,0:T(8,128)(2,1)S(1)} %get-tuple-element.33.after), channel_id=1, source_target_pairs={{0,16},{2,18},{4,20},{6,22},{8,24},{10,26},{12,28},{14,30},{16,0},... | collective-permute-start | bytes 122888 | tf_op jit(solution)/shard_map/ppermute | solution.py:611
  17.5 4.9 %collective-permute-start.5 = (bf16[16,1280]{1,0:T(8,128)(2,1)S(1)}, bf16[16,1280]{1,0:T(8,128)(2,1)S(1)}, u32[]{:S(2)}, u32[]{:S(2)}) collective-permute-start(bf16[16,1280]{1,0:T(8,128)(2,1)S(1)} %get-tuple-element.33.after), channel_id=1, source_target_pairs={{0,8},{2,10},{4,12},{6,14},{8,0},{10,2},{12,4},{14,6},{16,24},{18,... | collective-permute-start | bytes 122888 | tf_op jit(solution)/shard_map/ppermute | solution.py:611
  22.4 16.4 %copy-start.3 = (bf16[2048]{0:T(1024)(128)(2,1)S(1)}, bf16[2048]{0:T(1024)(128)(2,1)}, u32[]{:S(2)}) copy-start(bf16[2048]{0:T(1024)(128)(2,1)} %param.25) | copy-start | bytes 12292
  22.4 37.4 %copy-start = (bf16[4096,512]{1,0:T(8,128)(2,1)S(1)}, bf16[4096,512]{1,0:T(8,128)(2,1)}, u32[]{:S(2)}) copy-start(bf16[4096,512]{1,0:T(8,128)(2,1)} %w_up.1) | copy-start | bytes 12582916
  22.4 37.4 %copy-start.1 = (bf16[512,4096]{1,0:T(8,128)(2,1)S(1)}, bf16[512,4096]{1,0:T(8,128)(2,1)}, u32[]{:S(2)}) copy-start(bf16[512,4096]{1,0:T(8,128)(2,1)} %w_down.1) | copy-start | bytes 12582916
  22.4 37.3 %copy-start.2 = (bf16[4096]{0:T(1024)(128)(2,1)S(1)}, bf16[4096]{0:T(1024)(128)(2,1)}, u32[]{:S(2)}) copy-start(bf16[4096]{0:T(1024)(128)(2,1)} %param.27) | copy-start | bytes 24580

commit v5 on v4

--- a/solution.py
+++ b/solution.py
@@ -296,10 +296,35 @@
         copy.wait()
 
 
-def cache_load_kernel(after, values, values_out, sem):
-    copy = pltpu.make_async_copy(values, values_out, sem)
-    copy.start()
-    copy.wait()
+def live_scalars(lengths, base):
+    values = lengths[...]
+    return [values[s, 0] > base for s in range(values.shape[0])]
+
+
+def cache_load_kernel(
+    after, lengths, keys, values, keys_out, values_out, key_sems, value_sems
+):
+    live = live_scalars(lengths, lax.axis_index("kv") * keys.shape[1])
+
+    def copies(s):
+        return (
+            pltpu.make_async_copy(keys.at[s], keys_out.at[s], key_sems.at[s]),
+            pltpu.make_async_copy(values.at[s], values_out.at[s], value_sems.at[s]),
+        )
+
+    for s in range(keys.shape[0]):
+
+        @pl.when(live[s])
+        def _():
+            for copy in copies(s):
+                copy.start()
+
+    for s in range(keys.shape[0]):
+
+        @pl.when(live[s])
+        def _():
+            for copy in copies(s):
+                copy.wait()
 
 
 def query_kernel(first, second, gain, w_query, state, message):
@@ -338,7 +363,6 @@
     w_value,
     w_gate,
     w_output,
-    keys,
     k_out,
     v_out,
     g_out,
@@ -346,7 +370,6 @@
     weights,
     w_keep,
     w_send,
-    keys_out,
     key_buffer,
     value_buffer,
     gate_buffer,
@@ -363,7 +386,6 @@
         (w_gate, gate_buffer),
         (w_output.at[:, sent], w_send),
         (w_output.at[:, kept], w_keep),
-        (keys, keys_out),
     )
     copies = [pltpu.make_async_copy(a, b, sems.at[i]) for i, (a, b) in enumerate(pairs)]
     for copy in copies:
@@ -394,6 +416,7 @@
 def attend_kernel(
     width,
     after,
+    lengths,
     old,
     m1,
     m2,
@@ -408,8 +431,9 @@
     out,
     query_rows,
     cached,
+    order,
 ):
-    rows, _, key_columns = keys.shape
+    rows, span, key_columns = keys.shape
     heads = key_columns // HEAD_KEY
     q, csum, moments = unpack_sum(old, (m1, m2, m3))
     average = moments[:, 0:1] / width
@@ -453,17 +477,38 @@
     value_columns = heads * HEAD_VALUE
     head_of_value = lax.broadcasted_iota(jnp.int32, (heads, value_columns), 1) // HEAD_VALUE
     own_value = head_of_value == row_ids(heads, value_columns)
+    live = live_scalars(lengths, lax.axis_index("kv") * span)
+    count = jnp.int32(0)
     for s in range(rows):
-        spread = jnp.broadcast_to(query_rows[s : s + 1, :], (heads, key_columns))
+        order[count] = s
+        count = count + live[s].astype(jnp.int32)
+
+    def one(s, is_live):
+        row = pl.ds(s, 1)
+        spread = jnp.broadcast_to(query_rows[row, :], (heads, key_columns))
         query = jnp.where(own_key, spread, 0.0).astype(BF)
         scores = lax.dot_general(
             query, keys[s], (((1,), (1,)), ((), ())), preferred_element_type=F32
         )
-        coefficients = (scores * weights[s]).astype(BF)
+        weight = weights[s]
+        coefficients = jnp.where(weight > 0.0, scores * weight, 0.0).astype(BF)
         product = jnp.dot(coefficients, values[s], preferred_element_type=F32)
-        cached[s : s + 1, :] = jnp.sum(
-            jnp.where(own_value, product, 0.0), 0, keepdims=True
-        )
+        kept = jnp.logical_and(own_value, is_live)
+        cached[row, :] = jnp.sum(jnp.where(kept, product, 0.0), 0, keepdims=True)
+
+    steps = [n for n in (4, 8) if n < rows] + [rows]
+    for least, most in zip([-1] + steps[:-1], steps):
+
+        @pl.when(jnp.logical_and(count > least, count <= most))
+        def _():
+            if most == rows:
+                for s in range(rows):
+                    one(s, live[s])
+            else:
+                cached[...] = jnp.zeros_like(cached)
+                for i in range(most):
+                    one(order[jnp.minimum(i, jnp.maximum(count - 1, 0))], count > 0)
+
     for h in range(heads):
         out[h, :rows, :] = cached[:, h * LANES : (h + 1) * LANES].astype(BF)
 
@@ -613,7 +658,7 @@
             ]
 
         got = exchange(message, 1)
-        k_part, v_part, g_part, turn, weights, w_keep, w_send, keys = call(
+        k_part, v_part, g_part, turn, weights, w_keep, w_send = call(
             other_kernel,
             (
                 sds((S + 8, qc), F32),
@@ -623,12 +668,11 @@
                 sds((S, H, LANES), F32),
                 sds((w_output.shape[0], own), BF),
                 sds((w_output.shape[0], own), BF),
-                sds(key_cache.shape, BF),
             ),
-            [ANY] + [VMEM] * 5 + [HBM] * 5,
+            [ANY] + [VMEM] * 5 + [HBM] * 4,
             flops=10**9,
             scratch=[pltpu.VMEM(w.shape, BF) for w in (w_key, w_value, w_gate)]
-            + [pltpu.SemaphoreType.DMA((6,))],
+            + [pltpu.SemaphoreType.DMA((5,))],
             limit=6 * mib,
         )(
             message,
@@ -637,7 +681,7 @@
             tokens,
             other,
             gain,
-            *in_hbm(w_key, w_value, w_gate, w_output, key_cache),
+            *in_hbm(w_key, w_value, w_gate, w_output),
         )
         w_got = lax.ppermute(w_send, "tp", swap)
 
@@ -648,22 +692,26 @@
             )(state, *got)
             got = exchange(message, stride)
             stride *= 4
-        values = call(
+        keys, values = call(
             cache_load_kernel,
-            sds(value_cache.shape, BF),
-            [ANY, HBM],
+            (sds(key_cache.shape, BF), sds(value_cache.shape, BF)),
+            [ANY, VMEM] + [HBM] * 2,
             flops=10**9,
-            scratch=[pltpu.SemaphoreType.DMA],
+            scratch=[pltpu.SemaphoreType.DMA((S,))] * 2,
             limit=2 * mib,
-        )(message, *in_hbm(value_cache))
+        )(message, length_rows, *in_hbm(key_cache, value_cache))
 
         pieces = call(
             functools.partial(attend_kernel, width),
             sds((H, 3 * S + S // 2, LANES), BF),
-            [ANY] + [VMEM] * 11,
-            scratch=[pltpu.VMEM((S, qc), F32), pltpu.VMEM((S, vc), F32)],
+            [ANY] + [VMEM] * 12,
+            scratch=[
+                pltpu.VMEM((S, qc), F32),
+                pltpu.VMEM((S, vc), F32),
+                pltpu.SMEM((S,), jnp.int32),
+            ],
             limit=4 * mib,
-        )(w_got, state, *got, k_part, v_part, g_part, turn, weights, keys, values)
+        )(w_got, length_rows, state, *got, k_part, v_part, g_part, turn, weights, keys, values)
 
         pieces = lax.all_to_all(pieces, "kv", 0, 0, tiled=True)
         gated = call(

time: 72.1 us -> 69.1 us (0.958)
  blocking collectives: 43.7 us -> 41.1 us
    all_to_all x1, blocking collectives: 13.4 us -> 10.9 us  [on_device(): pieces = lax.all_to_all(pieces, 'kv', 0, 0, tiled=True)]
    pallas_call x1, Pallas kernels: 3.39 us -> 4.89 us  [on_device(): call(cache_load_kernel, (sds(key_cache.shape, BF), sds(value_cache.shape,...]
    pallas_call x1, Pallas kernels: 3.39 us -> 2.05 us  [on_device(): call(other_kernel, (sds((S + 8, qc), F32), sds((S + 8, vc), F32), sds((S...]
  transfers between devices with their start and end apart: 8 -> 8, of which waited for: 4 -> 3; matrix products, arithmetic and copies ran while one was open for 0% -> 0% of each run, Pallas kernels for 6% -> 9%
where the time goes in v5:
time: 69.1 us; the launch traced here: 68.8 us
  blocking collectives  41.1 us (59%)
  Pallas kernels  14.1 us (20%)
  starting transfers between devices  9.45 us (14%)
  waiting for transfers between devices  3.95 us (6%)
    all_to_all x1, blocking collectives, on_device(): pieces = lax.all_to_all(pieces, 'kv', 0, 0, tiled=True)  10.9 us
    all_to_all x1, blocking collectives, on_device(): gated = lax.all_to_all(gated, ('kv', 'tp'), 0, 0, tiled=True)  10.3 us
    all_to_all x1, blocking collectives, on_device(): down = lax.all_to_all(down, ('kv', 'tp'), 0, 0, tiled=True)  9.97 us
    all_to_all x1, blocking collectives, on_device(): spread = lax.all_to_all(spread, ('kv', 'tp'), 0, 0, tiled=True)  9.97 us
    ppermute x6, starting transfers between devices, exchange(): lax.ppermute(message, 'kv', [(i, i ^ j * stride) for i in range(kv)])  8.65 us
    pallas_call x1, Pallas kernels, on_device(): call(cache_load_kernel, (sds(key_cache.shape, BF), sds(value_cache.shape,...  4.89 us
    ppermute x6, waiting for transfers between devices, exchange(): lax.ppermute(message, 'kv', [(i, i ^ j * stride) for i in range(kv)])  3.95 us
    pallas_call x1, Pallas kernels, on_device(): call(functools.partial(attend_kernel, width), sds((H, 3 * S + S // 2, LAN...  2.99 us
  transfers between devices with their start and end apart: 8, of which 3 were waited for; matrix products, arithmetic and copies ran while one was open for 0% of the time, Pallas kernels for 9%

profile of v5, /device:TPU:0, one launch (start us, length us, event | category | flops | bytes accessed | tf_op | source)
XLA Modules:
  0.0 68.8 jit_solution(5436990422593735764)
XLA Ops:
  0.0 0.5 collective-permute-start
  0.5 1.1 %shard_map.145 = (bf16[256,1024]{1,0:T(8,128)(2,1)S(1)}, bf16[16,128]{1,0:T(8,128)(2,1)S(1)}, bf16[2,128]{1,0:T(2,128)(2,1)S(1)}, s32[16,128]{1,0:T(8,128)S(1)}, f32[16,128]{1,0:T(8,128)S(1)}) custom-call(bf16[256,1024]{1,0:T(8,128)(2,1)} %w_query.1, bf16[16,128]{1,0:T(8,128)(2,1)} %tokens.1, bf16[2,128]{1,0:T(2,128)(2,1)} %bitcast.5, s32[16]{0:T(128)} %lengths.1, ...), custom_call_target="tpu_custom_call" | custom-call | flops 1000000000 | tf_op jit(solution)/shard_map/pallas_call | solution.py:630
  1.6 0.0 collective-permute-done.second
  1.6 0.2 shard_map.146
  1.8 2.0 %shard_map.147 = (f32[24,1024]{1,0:T(8,128)S(1)}, f32[24,2048]{1,0:T(8,128)S(1)}, f32[24,2048]{1,0:T(8,128)S(1)}, f32[2,16,128]{2,1,0:T(8,128)S(1)}, f32[16,16,1...) custom-call(bf16[16,1280]{1,0:T(8,128)(2,1)S(1)} %get-tuple-element.28.after, ...), custom_call_target="tpu_custom_call" | custom-call | flops 1000000000 | tf_op jit(solution)/shard_map/pallas_call | solution.py:661
  3.9 0.3 collective-permute-start.1
  4.2 3.7 %collective-permute-start.4 = (bf16[16,1280]{1,0:T(8,128)(2,1)S(1)}, bf16[16,1280]{1,0:T(8,128)(2,1)S(1)}, u32[]{:S(2)}, u32[]{:S(2)}) collective-permute-start(bf16[16,1280]{1,0:T(8,128)(2,1)S(1)} %get-tuple-element.28.after), channel_id=1, source_target_pairs={{0,6},{2,4},{4,2},{6,0},{8,14},{10,12},{12,10},{14,8},{16,22},{18,... | collective-permute-start | bytes 122888 | tf_op jit(solution)/shard_map/ppermute | solution.py:656
  7.9 0.5 collective-permute-start.3
  8.4 0.1 collective-permute-start.2
  8.5 1.4 %collective-permute-done.4.m3 = bf16[16,1280]{1,0:T(8,128)(2,1)S(1)} collective-permute-done((bf16[16,1280]{1,0:T(8,128)(2,1)S(1)}, bf16[16,1280]{1,0:T(8,128)(2,1)S(1)}, u32[]{:S(2)}, u32[]{:S(2)}) %collective-permute-start.4) | collective-permute-done | bytes 40992 | tf_op jit(solution)/shard_map/ppermute | solution.py:656
  9.9 2.0 %collective-permute-done.3.m2 = bf16[16,1280]{1,0:T(8,128)(2,1)S(1)} collective-permute-done((bf16[16,1280]{1,0:T(8,128)(2,1)S(1)}, bf16[16,1280]{1,0:T(8,128)(2,1)S(1)}, u32[]{:S(2)}, u32[]{:S(2)}) %collective-permute-start.3) | collective-permute-done | bytes 40992 | tf_op jit(solution)/shard_map/ppermute | solution.py:656
  11.9 0.5 collective-permute-done.2.m1
  12.4 0.2 shard_map.148
  12.6 3.6 %collective-permute-start.7 = (bf16[16,1280]{1,0:T(8,128)(2,1)S(1)}, bf16[16,1280]{1,0:T(8,128)(2,1)S(1)}, u32[]{:S(2)}, u32[]{:S(2)}) collective-permute-start(bf16[16,1280]{1,0:T(8,128)(2,1)S(1)} %get-tuple-element.34.after), channel_id=1, source_target_pairs={{0,24},{2,26},{4,28},{6,30},{8,16},{10,18},{12,20},{14,22},{16,8},... | collective-permute-start | bytes 122888 | tf_op jit(solution)/shard_map/ppermute | solution.py:656
  16.2 0.0 collective-permute-start.6
  16.2 0.8 %collective-permute-start.5 = (bf16[16,1280]{1,0:T(8,128)(2,1)S(1)}, bf16[16,1280]{1,0:T(8,128)(2,1)S(1)}, u32[]{:S(2)}, u32[]{:S(2)}) collective-permute-start(bf16[16,1280]{1,0:T(8,128)(2,1)S(1)} %get-tuple-element.34.after), channel_id=1, source_target_pairs={{0,8},{2,10},{4,12},{6,14},{8,0},{10,2},{12,4},{14,6},{16,24},{18,... | collective-permute-start | bytes 122888 | tf_op jit(solution)/shard_map/ppermute | solution.py:656
  17.0 4.9 %shard_map.149 = (bf16[16,128,1024]{2,1,0:T(8,128)(2,1)S(1)}, bf16[16,128,2048]{2,1,0:T(8,128)(2,1)S(1)}) custom-call(bf16[16,1280]{1,0:T(8,128)(2,1)S(1)} %get-tuple-element.34.after, s32[16,128]{1,0:T(8,128)S(1)} %get-tuple-element.29.lengths, bf16[16,128,1024]{2,1,0:T(8,128)(2,1)} %keys.1, bf16[16,128,2048]{2,1,0:T(8,128)(2,1)} %values.1), custom_call_target="tpu_custom_call" | custom-call | flops 1000000000 | tf_op jit(solution)/shard_map/pallas_call | solution.py:695
  21.9 0.0 collective-permute-done.7.m3
  21.9 0.0 collective-permute-done.1.after.w_got
  21.9 0.0 copy-start.3
  21.9 0.0 copy-start
  21.9 0.0 copy-start.1
  21.9 0.0 copy-start.2
  21.9 3.0 %shard_map.150 = bf16[16,56,128]{2,1,0:T(8,128)(2,1)S(1)} custom-call(bf16[2048,128]{1,0:T(8,128)(2,1)S(1)} %collective-permute-done.1.after.w_got, s32[16,128]{1,0:T(8,128)S(1)} %get-tuple-element.29.lengths, f32[16,1280]{1,0:T(8,128)S(1)} %get-tuple-element.33.old, bf16[16,1280]{1,0:T(8,128)(2,1)S(1)} %collective-permute-done.5.m1, ...), custom_call_target="tpu_custom_call" | custom-call | tf_op jit(solution)/shard_map/pallas_call | solution.py:704
  24.9 10.9 %all_to_all.20.pieces = bf16[16,56,128]{2,1,0:T(8,128)(2,1)S(1)} all-to-all(bf16[16,56,128]{2,1,0:T(8,128)(2,1)S(1)} %shard_map.150), channel_id=1, replica_groups=mesh['kv'=16,'tp'=2] {'kv'}, dimensions={0} | all-to-all | bytes 458752 | tf_op jit(solution)/shard_map/all_to_all | solution.py:716
  35.9 0.4 shard_map.151
  36.3 10.3 %all_to_all.21.gated = bf16[32,16,128]{2,1,0:T(8,128)(2,1)S(1)} all-to-all(bf16[32,16,128]{2,1,0:T(8,128)(2,1)S(1)} %shard_map.151), channel_id=1, replica_groups=mesh['kv'=16,'tp'=2] {'kv','tp'}, dimensions={0} | all-to-all | bytes 262144 | tf_op jit(solution)/shard_map/all_to_all | solution.py:720
  46.5 0.3 shard_map.152
  46.8 10.0 %all_to_all.22.residual = bf16[32,16,128]{2,1,0:T(8,128)(2,1)S(1)} all-to-all(bf16[32,16,128]{2,1,0:T(8,128)(2,1)S(1)} %get-tuple-element.43), channel_id=1, replica_groups=mesh['kv'=16,'tp'=2] {'kv','tp'}, dimensions={0} | all-to-all | bytes 262144 | tf_op jit(solution)/shard_map/all_to_all | solution.py:727
  56.8 1.5 %shard_map.153 = bf16[32,16,128]{2,1,0:T(8,128)(2,1)S(1)} custom-call(bf16[32,16,128]{2,1,0:T(8,128)(2,1)S(1)} %all_to_all.22.residual, bf16[32,128]{1,0:T(8,128)(2,1)S(1)} %bitcast.3, bf16[4096,512]{1,0:T(8,128)(2,1)S(1)} %copy-done, bf16[512,4096]{1,0:T(8,128)(2,1)S(1)} %copy-done.1), custom_call_target="tpu_custom_call" | custom-call | tf_op jit(solution)/shard_map/pallas_call | solution.py:728
  58.2 10.0 %all_to_all.23.pieces = bf16[32,16,128]{2,1,0:T(8,128)(2,1)S(1)} all-to-all(bf16[32,16,128]{2,1,0:T(8,128)(2,1)S(1)} %shard_map.153), channel_id=1, replica_groups=mesh['kv'=16,'tp'=2] {'kv','tp'}, dimensions={0} | all-to-all | bytes 262144 | tf_op jit(solution)/shard_map/all_to_all | solution.py:731
  68.2 0.6 shard_map.154
  (6 shorter events, 0.0 us)
Async XLA Ops:
  0.0 1.6 %collective-permute-start = (bf16[16,128]{1,0:T(8,128)(2,1)}, bf16[16,128]{1,0:T(8,128)(2,1)S(1)}, u32[]{:S(2)}, u32[]{:S(2)}) collective-permute-start(bf16[16,128]{1,0:T(8,128)(2,1)} %tokens.1), channel_id=1, source_target_pairs={{0,1},{1,0},{2,3},{3,2},{4,5},{5,4},{6,7},{7,6},{8,9},{9,8},{10,11... | collective-permute-start | bytes 12296 | tf_op jit(solution)/shard_map/ppermute | solution.py:628
  3.9 18.0 %collective-permute-start.1 = (bf16[2048,128]{1,0:T(8,128)(2,1)S(1)}, bf16[2048,128]{1,0:T(8,128)(2,1)S(1)}, u32[]{:S(2)}, u32[]{:S(2)}) collective-permute-start(bf16[2048,128]{1,0:T(8,128)(2,1)S(1)} %get-tuple-element.31), channel_id=1, source_target_pairs={{0,1},{1,0},{2,3},{3,2},{4,5},{5,4},{6,7},{7,6},{8,9},{9,8},{10,11... | collective-permute-start | bytes 1572872 | tf_op jit(solution)/shard_map/ppermute | solution.py:686
  4.2 5.7 %collective-permute-start.4 = (bf16[16,1280]{1,0:T(8,128)(2,1)S(1)}, bf16[16,1280]{1,0:T(8,128)(2,1)S(1)}, u32[]{:S(2)}, u32[]{:S(2)}) collective-permute-start(bf16[16,1280]{1,0:T(8,128)(2,1)S(1)} %get-tuple-element.28.after), channel_id=1, source_target_pairs={{0,6},{2,4},{4,2},{6,0},{8,14},{10,12},{12,10},{14,8},{16,22},{18,... | collective-permute-start | bytes 122888 | tf_op jit(solution)/shard_map/ppermute | solution.py:656
  7.9 4.0 %collective-permute-start.3 = (bf16[16,1280]{1,0:T(8,128)(2,1)S(1)}, bf16[16,1280]{1,0:T(8,128)(2,1)S(1)}, u32[]{:S(2)}, u32[]{:S(2)}) collective-permute-start(bf16[16,1280]{1,0:T(8,128)(2,1)S(1)} %get-tuple-element.28.after), channel_id=1, source_target_pairs={{0,4},{2,6},{4,0},{6,2},{8,12},{10,14},{12,8},{14,10},{16,20},{18,... | collective-permute-start | bytes 122888 | tf_op jit(solution)/shard_map/ppermute | solution.py:656
  8.4 4.0 %collective-permute-start.2 = (bf16[16,1280]{1,0:T(8,128)(2,1)S(1)}, bf16[16,1280]{1,0:T(8,128)(2,1)S(1)}, u32[]{:S(2)}, u32[]{:S(2)}) collective-permute-start(bf16[16,1280]{1,0:T(8,128)(2,1)S(1)} %get-tuple-element.28.after), channel_id=1, source_target_pairs={{0,2},{2,0},{4,6},{6,4},{8,10},{10,8},{12,14},{14,12},{16,18},{18,... | collective-permute-start | bytes 122888 | tf_op jit(solution)/shard_map/ppermute | solution.py:656
  12.6 9.3 %collective-permute-start.7 = (bf16[16,1280]{1,0:T(8,128)(2,1)S(1)}, bf16[16,1280]{1,0:T(8,128)(2,1)S(1)}, u32[]{:S(2)}, u32[]{:S(2)}) collective-permute-start(bf16[16,1280]{1,0:T(8,128)(2,1)S(1)} %get-tuple-element.34.after), channel_id=1, source_target_pairs={{0,24},{2,26},{4,28},{6,30},{8,16},{10,18},{12,20},{14,22},{16,8},... | collective-permute-start | bytes 122888 | tf_op jit(solution)/shard_map/ppermute | solution.py:656
  16.2 5.7 %collective-permute-start.6 = (bf16[16,1280]{1,0:T(8,128)(2,1)S(1)}, bf16[16,1280]{1,0:T(8,128)(2,1)S(1)}, u32[]{:S(2)}, u32[]{:S(2)}) collective-permute-start(bf16[16,1280]{1,0:T(8,128)(2,1)S(1)} %get-tuple-element.34.after), channel_id=1, source_target_pairs={{0,16},{2,18},{4,20},{6,22},{8,24},{10,26},{12,28},{14,30},{16,0},... | collective-permute-start | bytes 122888 | tf_op jit(solution)/shard_map/ppermute | solution.py:656
  16.2 5.7 %collective-permute-start.5 = (bf16[16,1280]{1,0:T(8,128)(2,1)S(1)}, bf16[16,1280]{1,0:T(8,128)(2,1)S(1)}, u32[]{:S(2)}, u32[]{:S(2)}) collective-permute-start(bf16[16,1280]{1,0:T(8,128)(2,1)S(1)} %get-tuple-element.34.after), channel_id=1, source_target_pairs={{0,8},{2,10},{4,12},{6,14},{8,0},{10,2},{12,4},{14,6},{16,24},{18,... | collective-permute-start | bytes 122888 | tf_op jit(solution)/shard_map/ppermute | solution.py:656
  21.9 14.0 %copy-start.3 = (bf16[2048]{0:T(1024)(128)(2,1)S(1)}, bf16[2048]{0:T(1024)(128)(2,1)}, u32[]{:S(2)}) copy-start(bf16[2048]{0:T(1024)(128)(2,1)} %param.25) | copy-start | bytes 12292
  21.9 34.9 %copy-start = (bf16[4096,512]{1,0:T(8,128)(2,1)S(1)}, bf16[4096,512]{1,0:T(8,128)(2,1)}, u32[]{:S(2)}) copy-start(bf16[4096,512]{1,0:T(8,128)(2,1)} %w_up.1) | copy-start | bytes 12582916
  21.9 34.9 %copy-start.1 = (bf16[512,4096]{1,0:T(8,128)(2,1)S(1)}, bf16[512,4096]{1,0:T(8,128)(2,1)}, u32[]{:S(2)}) copy-start(bf16[512,4096]{1,0:T(8,128)(2,1)} %w_down.1) | copy-start | bytes 12582916
  21.9 34.9 %copy-start.2 = (bf16[4096]{0:T(1024)(128)(2,1)S(1)}, bf16[4096]{0:T(1024)(128)(2,1)}, u32[]{:S(2)}) copy-start(bf16[4096]{0:T(1024)(128)(2,1)} %param.27) | copy-start | bytes 24580

commit v6 on v5

--- a/solution.py
+++ b/solution.py
@@ -298,33 +298,48 @@
 
 def live_scalars(lengths, base):
     values = lengths[...]
-    return [values[s, 0] > base for s in range(values.shape[0])]
+    live = [values[s, 0] > base for s in range(values.shape[0])]
+    count = jnp.int32(0)
+    for flag in live:
+        count = count + flag.astype(jnp.int32)
+    return live, count
+
+
+def few_rows(rows):
+    return rows // 2
+
+
+def late_rows(rows):
+    return rows * 3 // 8
 
 
 def cache_load_kernel(
     after, lengths, keys, values, keys_out, values_out, key_sems, value_sems
 ):
-    live = live_scalars(lengths, lax.axis_index("kv") * keys.shape[1])
-
-    def copies(s):
-        return (
-            pltpu.make_async_copy(keys.at[s], keys_out.at[s], key_sems.at[s]),
-            pltpu.make_async_copy(values.at[s], values_out.at[s], value_sems.at[s]),
-        )
-
-    for s in range(keys.shape[0]):
-
-        @pl.when(live[s])
-        def _():
-            for copy in copies(s):
-                copy.start()
-
-    for s in range(keys.shape[0]):
-
-        @pl.when(live[s])
-        def _():
-            for copy in copies(s):
-                copy.wait()
+    rows = keys.shape[0]
+    live, count = live_scalars(lengths, lax.axis_index("kv") * keys.shape[1])
+    few = count <= few_rows(rows)
+
+    def each_copy(act):
+        for s in range(rows):
+            key = pltpu.make_async_copy(keys.at[s], keys_out.at[s], key_sems.at[s])
+            value = pltpu.make_async_copy(values.at[s], values_out.at[s], value_sems.at[s])
+            late = s >= rows - late_rows(rows)
+
+            @pl.when(live[s])
+            def _():
+                act(key)
+                if not late:
+                    act(value)
+
+            if late:
+
+                @pl.when(jnp.logical_and(live[s], few))
+                def _():
+                    act(value)
+
+    each_copy(lambda copy: copy.start())
+    each_copy(lambda copy: copy.wait())
 
 
 def query_kernel(first, second, gain, w_query, state, message):
@@ -428,13 +443,28 @@
     weights,
     keys,
     values,
+    values_far,
     out,
     query_rows,
     cached,
     order,
+    late_values,
+    late_sems,
 ):
     rows, span, key_columns = keys.shape
     heads = key_columns // HEAD_KEY
+    live, live_count = live_scalars(lengths, lax.axis_index("kv") * span)
+    late = late_values.shape[0]
+    late_copies = [
+        pltpu.make_async_copy(values_far.at[rows - late + i], late_values.at[i], late_sems.at[i])
+        for i in range(late)
+    ]
+
+    @pl.when(live_count > few_rows(rows))
+    def _():
+        for copy in late_copies:
+            copy.start()
+
     q, csum, moments = unpack_sum(old, (m1, m2, m3))
     average = moments[:, 0:1] / width
     inverse = lax.rsqrt(moments[:, 1:2] / width - average * average + EPS)
@@ -477,13 +507,12 @@
     value_columns = heads * HEAD_VALUE
     head_of_value = lax.broadcasted_iota(jnp.int32, (heads, value_columns), 1) // HEAD_VALUE
     own_value = head_of_value == row_ids(heads, value_columns)
-    live = live_scalars(lengths, lax.axis_index("kv") * span)
     count = jnp.int32(0)
     for s in range(rows):
         order[count] = s
         count = count + live[s].astype(jnp.int32)
 
-    def one(s, is_live):
+    def one(s, is_live, value=None):
         row = pl.ds(s, 1)
         spread = jnp.broadcast_to(query_rows[row, :], (heads, key_columns))
         query = jnp.where(own_key, spread, 0.0).astype(BF)
@@ -492,18 +521,23 @@
         )
         weight = weights[s]
         coefficients = jnp.where(weight > 0.0, scores * weight, 0.0).astype(BF)
-        product = jnp.dot(coefficients, values[s], preferred_element_type=F32)
+        value = values[s] if value is None else value
+        product = jnp.dot(coefficients, value, preferred_element_type=F32)
         kept = jnp.logical_and(own_value, is_live)
         cached[row, :] = jnp.sum(jnp.where(kept, product, 0.0), 0, keepdims=True)
 
-    steps = [n for n in (4, 8) if n < rows] + [rows]
+    steps = [few_rows(rows) // 2, few_rows(rows), rows]
     for least, most in zip([-1] + steps[:-1], steps):
 
         @pl.when(jnp.logical_and(count > least, count <= most))
         def _():
             if most == rows:
-                for s in range(rows):
+                for s in range(rows - late):
                     one(s, live[s])
+                for copy in late_copies:
+                    copy.wait()
+                for i in range(late):
+                    one(rows - late + i, live[rows - late + i], late_values[i])
             else:
                 cached[...] = jnp.zeros_like(cached)
                 for i in range(most):
@@ -704,14 +738,29 @@
         pieces = call(
             functools.partial(attend_kernel, width),
             sds((H, 3 * S + S // 2, LANES), BF),
-            [ANY] + [VMEM] * 12,
+            [ANY] + [VMEM] * 12 + [HBM],
             scratch=[
                 pltpu.VMEM((S, qc), F32),
                 pltpu.VMEM((S, vc), F32),
                 pltpu.SMEM((S,), jnp.int32),
+                pltpu.VMEM((late_rows(S),) + value_cache.shape[1:], BF),
+                pltpu.SemaphoreType.DMA((late_rows(S),)),
             ],
-            limit=4 * mib,
-        )(w_got, length_rows, state, *got, k_part, v_part, g_part, turn, weights, keys, values)
+            limit=8 * mib,
+        )(
+            w_got,
+            length_rows,
+            state,
+            *got,
+            k_part,
+            v_part,
+            g_part,
+            turn,
+            weights,
+            keys,
+            values,
+            *in_hbm(value_cache),
+        )
 
         pieces = lax.all_to_all(pieces, "kv", 0, 0, tiled=True)
         gated = call(

time: 69.1 us -> 69.1 us (level)
    pallas_call x1, Pallas kernels: 4.89 us -> 3.98 us  [on_device(): call(cache_load_kernel, (sds(key_cache.shape, BF), sds(value_cache.shape,...]
  transfers between devices with their start and end apart: 8 -> 8, of which waited for: 3 -> 4; matrix products, arithmetic and copies ran while one was open for 0% -> 0% of each run, Pallas kernels for 9% -> 8%
where the time goes in v6:
time: 69.1 us; the launch traced here: 68.9 us
  blocking collectives  41.3 us (60%)
  Pallas kernels  13.9 us (20%)
  starting transfers between devices  9.45 us (14%)
  waiting for transfers between devices  4.07 us (6%)
    all_to_all x1, blocking collectives, on_device(): pieces = lax.all_to_all(pieces, 'kv', 0, 0, tiled=True)  11.1 us
    all_to_all x1, blocking collectives, on_device(): gated = lax.all_to_all(gated, ('kv', 'tp'), 0, 0, tiled=True)  10.3 us
    all_to_all x1, blocking collectives, on_device(): spread = lax.all_to_all(spread, ('kv', 'tp'), 0, 0, tiled=True)  9.97 us
    all_to_all x1, blocking collectives, on_device(): down = lax.all_to_all(down, ('kv', 'tp'), 0, 0, tiled=True)  9.97 us
    ppermute x6, starting transfers between devices, exchange(): lax.ppermute(message, 'kv', [(i, i ^ j * stride) for i in range(kv)])  8.65 us
    ppermute x6, waiting for transfers between devices, exchange(): lax.ppermute(message, 'kv', [(i, i ^ j * stride) for i in range(kv)])  4.06 us
    pallas_call x1, Pallas kernels, on_device(): call(cache_load_kernel, (sds(key_cache.shape, BF), sds(value_cache.shape,...  3.98 us
    pallas_call x1, Pallas kernels, on_device(): call(functools.partial(attend_kernel, width), sds((H, 3 * S + S // 2, LAN...  3.67 us
  transfers between devices with their start and end apart: 8, of which 4 were waited for; matrix products, arithmetic and copies ran while one was open for 0% of the time, Pallas kernels for 8%

profile of v6, /device:TPU:0, one launch (start us, length us, event | category | flops | bytes accessed | tf_op | source)
XLA Modules:
  0.0 68.9 jit_solution(10453195281551519458)
XLA Ops:
  0.0 0.5 collective-permute-start
  0.5 1.1 %shard_map.145 = (bf16[256,1024]{1,0:T(8,128)(2,1)S(1)}, bf16[16,128]{1,0:T(8,128)(2,1)S(1)}, bf16[2,128]{1,0:T(2,128)(2,1)S(1)}, s32[16,128]{1,0:T(8,128)S(1)}, f32[16,128]{1,0:T(8,128)S(1)}) custom-call(bf16[256,1024]{1,0:T(8,128)(2,1)} %w_query.1, bf16[16,128]{1,0:T(8,128)(2,1)} %tokens.1, bf16[2,128]{1,0:T(2,128)(2,1)} %bitcast.5, s32[16]{0:T(128)} %lengths.1, ...), custom_call_target="tpu_custom_call" | custom-call | flops 1000000000 | tf_op jit(solution)/shard_map/pallas_call | solution.py:664
  1.6 0.0 collective-permute-done.second
  1.6 0.2 shard_map.146
  1.8 2.0 %shard_map.147 = (f32[24,1024]{1,0:T(8,128)S(1)}, f32[24,2048]{1,0:T(8,128)S(1)}, f32[24,2048]{1,0:T(8,128)S(1)}, f32[2,16,128]{2,1,0:T(8,128)S(1)}, f32[16,16,1...) custom-call(bf16[16,1280]{1,0:T(8,128)(2,1)S(1)} %get-tuple-element.28.after, ...), custom_call_target="tpu_custom_call" | custom-call | flops 1000000000 | tf_op jit(solution)/shard_map/pallas_call | solution.py:695
  3.9 0.3 collective-permute-start.1
  4.2 3.7 %collective-permute-start.4 = (bf16[16,1280]{1,0:T(8,128)(2,1)S(1)}, bf16[16,1280]{1,0:T(8,128)(2,1)S(1)}, u32[]{:S(2)}, u32[]{:S(2)}) collective-permute-start(bf16[16,1280]{1,0:T(8,128)(2,1)S(1)} %get-tuple-element.28.after), channel_id=1, source_target_pairs={{0,6},{2,4},{4,2},{6,0},{8,14},{10,12},{12,10},{14,8},{16,22},{18,... | collective-permute-start | bytes 122888 | tf_op jit(solution)/shard_map/ppermute | solution.py:690
  7.9 0.5 collective-permute-start.3
  8.4 0.1 collective-permute-start.2
  8.5 1.4 %collective-permute-done.4.m3 = bf16[16,1280]{1,0:T(8,128)(2,1)S(1)} collective-permute-done((bf16[16,1280]{1,0:T(8,128)(2,1)S(1)}, bf16[16,1280]{1,0:T(8,128)(2,1)S(1)}, u32[]{:S(2)}, u32[]{:S(2)}) %collective-permute-start.4) | collective-permute-done | bytes 40992 | tf_op jit(solution)/shard_map/ppermute | solution.py:690
  9.9 2.0 %collective-permute-done.3.m2 = bf16[16,1280]{1,0:T(8,128)(2,1)S(1)} collective-permute-done((bf16[16,1280]{1,0:T(8,128)(2,1)S(1)}, bf16[16,1280]{1,0:T(8,128)(2,1)S(1)}, u32[]{:S(2)}, u32[]{:S(2)}) %collective-permute-start.3) | collective-permute-done | bytes 40992 | tf_op jit(solution)/shard_map/ppermute | solution.py:690
  11.9 0.5 collective-permute-done.2.m1
  12.4 0.2 shard_map.148
  12.6 3.6 %collective-permute-start.7 = (bf16[16,1280]{1,0:T(8,128)(2,1)S(1)}, bf16[16,1280]{1,0:T(8,128)(2,1)S(1)}, u32[]{:S(2)}, u32[]{:S(2)}) collective-permute-start(bf16[16,1280]{1,0:T(8,128)(2,1)S(1)} %get-tuple-element.34.after), channel_id=1, source_target_pairs={{0,24},{2,26},{4,28},{6,30},{8,16},{10,18},{12,20},{14,22},{16,8},... | collective-permute-start | bytes 122888 | tf_op jit(solution)/shard_map/ppermute | solution.py:690
  16.2 0.0 collective-permute-start.6
  16.2 0.8 %collective-permute-start.5 = (bf16[16,1280]{1,0:T(8,128)(2,1)S(1)}, bf16[16,1280]{1,0:T(8,128)(2,1)S(1)}, u32[]{:S(2)}, u32[]{:S(2)}) collective-permute-start(bf16[16,1280]{1,0:T(8,128)(2,1)S(1)} %get-tuple-element.34.after), channel_id=1, source_target_pairs={{0,8},{2,10},{4,12},{6,14},{8,0},{10,2},{12,4},{14,6},{16,24},{18,... | collective-permute-start | bytes 122888 | tf_op jit(solution)/shard_map/ppermute | solution.py:690
  17.0 4.0 %shard_map.149 = (bf16[16,128,1024]{2,1,0:T(8,128)(2,1)S(1)}, bf16[16,128,2048]{2,1,0:T(8,128)(2,1)S(1)}) custom-call(bf16[16,1280]{1,0:T(8,128)(2,1)S(1)} %get-tuple-element.34.after, s32[16,128]{1,0:T(8,128)S(1)} %get-tuple-element.29.lengths, bf16[16,128,1024]{2,1,0:T(8,128)(2,1)} %keys.1, bf16[16,128,2048]{2,1,0:T(8,128)(2,1)} %values_far.1), custom_call_target="tpu_custom_call" | custom-call | flops 1000000000 | tf_op jit(solution)/shard_map/pallas_call | solution.py:729
  20.9 0.0 collective-permute-done.7.m3
  21.0 0.1 collective-permute-done.6.m2
  21.1 0.0 collective-permute-done.5.m1
  21.1 0.0 copy-start
  21.1 0.0 copy-start.1
  21.1 0.0 copy-start.2
  21.1 3.7 %shard_map.150 = bf16[16,56,128]{2,1,0:T(8,128)(2,1)S(1)} custom-call(bf16[2048,128]{1,0:T(8,128)(2,1)S(1)} %collective-permute-done.1.after.w_got, s32[16,128]{1,0:T(8,128)S(1)} %get-tuple-element.29.lengths, f32[16,1280]{1,0:T(8,128)S(1)} %get-tuple-element.33.old, bf16[16,1280]{1,0:T(8,128)(2,1)S(1)} %collective-permute-done.5.m1, ...), custom_call_target="tpu_custom_call" | custom-call | tf_op jit(solution)/shard_map/pallas_call | solution.py:738
  24.8 11.1 %all_to_all.20.pieces = bf16[16,56,128]{2,1,0:T(8,128)(2,1)S(1)} all-to-all(bf16[16,56,128]{2,1,0:T(8,128)(2,1)S(1)} %shard_map.150), channel_id=1, replica_groups=mesh['kv'=16,'tp'=2] {'kv'}, dimensions={0} | all-to-all | bytes 458752 | tf_op jit(solution)/shard_map/all_to_all | solution.py:765
  35.9 0.4 shard_map.151
  36.3 10.3 %all_to_all.21.gated = bf16[32,16,128]{2,1,0:T(8,128)(2,1)S(1)} all-to-all(bf16[32,16,128]{2,1,0:T(8,128)(2,1)S(1)} %shard_map.151), channel_id=1, replica_groups=mesh['kv'=16,'tp'=2] {'kv','tp'}, dimensions={0} | all-to-all | bytes 262144 | tf_op jit(solution)/shard_map/all_to_all | solution.py:769
  46.6 0.3 shard_map.152
  46.8 10.0 %all_to_all.22.residual = bf16[32,16,128]{2,1,0:T(8,128)(2,1)S(1)} all-to-all(bf16[32,16,128]{2,1,0:T(8,128)(2,1)S(1)} %get-tuple-element.43), channel_id=1, replica_groups=mesh['kv'=16,'tp'=2] {'kv','tp'}, dimensions={0} | all-to-all | bytes 262144 | tf_op jit(solution)/shard_map/all_to_all | solution.py:776
  56.8 1.5 %shard_map.153 = bf16[32,16,128]{2,1,0:T(8,128)(2,1)S(1)} custom-call(bf16[32,16,128]{2,1,0:T(8,128)(2,1)S(1)} %all_to_all.22.residual, bf16[32,128]{1,0:T(8,128)(2,1)S(1)} %bitcast.3, bf16[4096,512]{1,0:T(8,128)(2,1)S(1)} %copy-done, bf16[512,4096]{1,0:T(8,128)(2,1)S(1)} %copy-done.1), custom_call_target="tpu_custom_call" | custom-call | tf_op jit(solution)/shard_map/pallas_call | solution.py:777
  58.3 10.0 %all_to_all.23.pieces = bf16[32,16,128]{2,1,0:T(8,128)(2,1)S(1)} all-to-all(bf16[32,16,128]{2,1,0:T(8,128)(2,1)S(1)} %shard_map.153), channel_id=1, replica_groups=mesh['kv'=16,'tp'=2] {'kv','tp'}, dimensions={0} | all-to-all | bytes 262144 | tf_op jit(solution)/shard_map/all_to_all | solution.py:780
  68.2 0.6 shard_map.154
  (6 shorter events, 0.0 us)
Async XLA Ops:
  0.0 1.6 %collective-permute-start = (bf16[16,128]{1,0:T(8,128)(2,1)}, bf16[16,128]{1,0:T(8,128)(2,1)S(1)}, u32[]{:S(2)}, u32[]{:S(2)}) collective-permute-start(bf16[16,128]{1,0:T(8,128)(2,1)} %tokens.1), channel_id=1, source_target_pairs={{0,1},{1,0},{2,3},{3,2},{4,5},{5,4},{6,7},{7,6},{8,9},{9,8},{10,11... | collective-permute-start | bytes 12296 | tf_op jit(solution)/shard_map/ppermute | solution.py:662
  3.9 17.2 %collective-permute-start.1 = (bf16[2048,128]{1,0:T(8,128)(2,1)S(1)}, bf16[2048,128]{1,0:T(8,128)(2,1)S(1)}, u32[]{:S(2)}, u32[]{:S(2)}) collective-permute-start(bf16[2048,128]{1,0:T(8,128)(2,1)S(1)} %get-tuple-element.31), channel_id=1, source_target_pairs={{0,1},{1,0},{2,3},{3,2},{4,5},{5,4},{6,7},{7,6},{8,9},{9,8},{10,11... | collective-permute-start | bytes 1572872 | tf_op jit(solution)/shard_map/ppermute | solution.py:720
  4.2 5.7 %collective-permute-start.4 = (bf16[16,1280]{1,0:T(8,128)(2,1)S(1)}, bf16[16,1280]{1,0:T(8,128)(2,1)S(1)}, u32[]{:S(2)}, u32[]{:S(2)}) collective-permute-start(bf16[16,1280]{1,0:T(8,128)(2,1)S(1)} %get-tuple-element.28.after), channel_id=1, source_target_pairs={{0,6},{2,4},{4,2},{6,0},{8,14},{10,12},{12,10},{14,8},{16,22},{18,... | collective-permute-start | bytes 122888 | tf_op jit(solution)/shard_map/ppermute | solution.py:690
  7.9 4.0 %collective-permute-start.3 = (bf16[16,1280]{1,0:T(8,128)(2,1)S(1)}, bf16[16,1280]{1,0:T(8,128)(2,1)S(1)}, u32[]{:S(2)}, u32[]{:S(2)}) collective-permute-start(bf16[16,1280]{1,0:T(8,128)(2,1)S(1)} %get-tuple-element.28.after), channel_id=1, source_target_pairs={{0,4},{2,6},{4,0},{6,2},{8,12},{10,14},{12,8},{14,10},{16,20},{18,... | collective-permute-start | bytes 122888 | tf_op jit(solution)/shard_map/ppermute | solution.py:690
  8.4 4.0 %collective-permute-start.2 = (bf16[16,1280]{1,0:T(8,128)(2,1)S(1)}, bf16[16,1280]{1,0:T(8,128)(2,1)S(1)}, u32[]{:S(2)}, u32[]{:S(2)}) collective-permute-start(bf16[16,1280]{1,0:T(8,128)(2,1)S(1)} %get-tuple-element.28.after), channel_id=1, source_target_pairs={{0,2},{2,0},{4,6},{6,4},{8,10},{10,8},{12,14},{14,12},{16,18},{18,... | collective-permute-start | bytes 122888 | tf_op jit(solution)/shard_map/ppermute | solution.py:690
  12.6 8.4 %collective-permute-start.7 = (bf16[16,1280]{1,0:T(8,128)(2,1)S(1)}, bf16[16,1280]{1,0:T(8,128)(2,1)S(1)}, u32[]{:S(2)}, u32[]{:S(2)}) collective-permute-start(bf16[16,1280]{1,0:T(8,128)(2,1)S(1)} %get-tuple-element.34.after), channel_id=1, source_target_pairs={{0,24},{2,26},{4,28},{6,30},{8,16},{10,18},{12,20},{14,22},{16,8},... | collective-permute-start | bytes 122888 | tf_op jit(solution)/shard_map/ppermute | solution.py:690
  16.2 4.9 %collective-permute-start.6 = (bf16[16,1280]{1,0:T(8,128)(2,1)S(1)}, bf16[16,1280]{1,0:T(8,128)(2,1)S(1)}, u32[]{:S(2)}, u32[]{:S(2)}) collective-permute-start(bf16[16,1280]{1,0:T(8,128)(2,1)S(1)} %get-tuple-element.34.after), channel_id=1, source_target_pairs={{0,16},{2,18},{4,20},{6,22},{8,24},{10,26},{12,28},{14,30},{16,0},... | collective-permute-start | bytes 122888 | tf_op jit(solution)/shard_map/ppermute | solution.py:690
  16.2 4.9 %collective-permute-start.5 = (bf16[16,1280]{1,0:T(8,128)(2,1)S(1)}, bf16[16,1280]{1,0:T(8,128)(2,1)S(1)}, u32[]{:S(2)}, u32[]{:S(2)}) collective-permute-start(bf16[16,1280]{1,0:T(8,128)(2,1)S(1)} %get-tuple-element.34.after), channel_id=1, source_target_pairs={{0,8},{2,10},{4,12},{6,14},{8,0},{10,2},{12,4},{14,6},{16,24},{18,... | collective-permute-start | bytes 122888 | tf_op jit(solution)/shard_map/ppermute | solution.py:690
  21.1 14.8 %copy-start.3 = (bf16[2048]{0:T(1024)(128)(2,1)S(1)}, bf16[2048]{0:T(1024)(128)(2,1)}, u32[]{:S(2)}) copy-start(bf16[2048]{0:T(1024)(128)(2,1)} %param.25) | copy-start | bytes 12292
  21.1 35.7 %copy-start = (bf16[4096,512]{1,0:T(8,128)(2,1)S(1)}, bf16[4096,512]{1,0:T(8,128)(2,1)}, u32[]{:S(2)}) copy-start(bf16[4096,512]{1,0:T(8,128)(2,1)} %w_up.1) | copy-start | bytes 12582916
  21.1 35.7 %copy-start.1 = (bf16[512,4096]{1,0:T(8,128)(2,1)S(1)}, bf16[512,4096]{1,0:T(8,128)(2,1)}, u32[]{:S(2)}) copy-start(bf16[512,4096]{1,0:T(8,128)(2,1)} %w_down.1) | copy-start | bytes 12582916
  21.1 35.7 %copy-start.2 = (bf16[4096]{0:T(1024)(128)(2,1)S(1)}, bf16[4096]{0:T(1024)(128)(2,1)}, u32[]{:S(2)}) copy-start(bf16[4096]{0:T(1024)(128)(2,1)} %param.27) | copy-start | bytes 24580

commit v7 on v5

--- a/solution.py
+++ b/solution.py
@@ -301,30 +301,31 @@
     return [values[s, 0] > base for s in range(values.shape[0])]
 
 
+def when_live(flags, copies, act):
+    for flag, copy in zip(flags, copies):
+
+        @pl.when(flag)
+        def _():
+            act(copy)
+
+
+def copies_of(source, target, sems, first, count):
+    return [
+        pltpu.make_async_copy(source.at[s], target.at[s], sems.at[s - first])
+        for s in range(first, first + count)
+    ]
+
+
 def cache_load_kernel(
-    after, lengths, keys, values, keys_out, values_out, key_sems, value_sems
+    after, lengths, keys, values, keys_begun, keys_out, values_out, key_sems, value_sems
 ):
-    live = live_scalars(lengths, lax.axis_index("kv") * keys.shape[1])
-
-    def copies(s):
-        return (
-            pltpu.make_async_copy(keys.at[s], keys_out.at[s], key_sems.at[s]),
-            pltpu.make_async_copy(values.at[s], values_out.at[s], value_sems.at[s]),
-        )
-
-    for s in range(keys.shape[0]):
-
-        @pl.when(live[s])
-        def _():
-            for copy in copies(s):
-                copy.start()
-
-    for s in range(keys.shape[0]):
-
-        @pl.when(live[s])
-        def _():
-            for copy in copies(s):
-                copy.wait()
+    rows, span = keys.shape[:2]
+    live = live_scalars(lengths, lax.axis_index("kv") * span)
+    half = rows // 2
+    copies = copies_of(keys, keys_out, key_sems, half, rows - half)
+    copies += copies_of(values, values_out, value_sems, 0, rows)
+    when_live(live[half:] + live, copies, lambda copy: copy.start())
+    when_live(live[half:] + live, copies, lambda copy: copy.wait())
 
 
 def query_kernel(first, second, gain, w_query, state, message):
@@ -363,28 +364,27 @@
     w_value,
     w_gate,
     w_output,
+    keys,
     k_out,
     v_out,
     g_out,
     turn,
     weights,
     w_keep,
-    w_send,
+    keys_out,
     key_buffer,
     value_buffer,
     gate_buffer,
     sems,
+    cache_sems,
 ):
     own = w_keep.shape[1]
-    t = lax.axis_index("tp")
-    kept = pl.ds(pl.multiple_of(t * own, own), own)
-    sent = pl.ds(pl.multiple_of((1 - t) * own, own), own)
+    kept = pl.ds(pl.multiple_of(lax.axis_index("tp") * own, own), own)
     buffers = (key_buffer, value_buffer, gate_buffer)
     pairs = (
         (w_key, key_buffer),
         (w_value, value_buffer),
         (w_gate, gate_buffer),
-        (w_output.at[:, sent], w_send),
         (w_output.at[:, kept], w_keep),
     )
     copies = [pltpu.make_async_copy(a, b, sems.at[i]) for i, (a, b) in enumerate(pairs)]
@@ -392,6 +392,9 @@
         copy.start()
     lhs, wide = projection_rows(first, second, gain)
     rows = wide.shape[0]
+    live = live_scalars(lengths, lax.axis_index("kv") * keys.shape[1])[: rows // 2]
+    caches = copies_of(keys, keys_out, cache_sems, 0, rows // 2)
+    when_live(live, caches, lambda copy: copy.start())
     half = HEAD_KEY // 2
     entry = (lane_ids(rows) % half).astype(F32)
     inverse = jnp.exp(entry * (-math.log(THETA) / half))
@@ -411,6 +414,7 @@
         out[...] = product[: rows + 8]
     for copy in copies[len(buffers) :]:
         copy.wait()
+    when_live(live, caches, lambda copy: copy.wait())
 
 
 def attend_kernel(
@@ -537,9 +541,11 @@
     heads = gated.shape[0] // 2
     t = lax.axis_index("tp")
     branch = 0.0
-    for group, w in ((t, w_keep), (1 - t, w_got)):
+    width = own.shape[1]
+    columns = pl.ds(pl.multiple_of(t * width, width), width)
+    for group, w in ((t, w_keep[...]), (1 - t, w_got[:, columns])):
         lhs = jnp.concatenate([gated[2 * h + group] for h in range(heads)], 1)
-        part = jnp.dot(lhs, w[...], preferred_element_type=F32)
+        part = jnp.dot(lhs, w, preferred_element_type=F32)
         branch = branch + part.astype(BF).astype(F32)
     residual = (tokens[...].astype(F32) + branch).astype(BF)
     own[...] = residual
@@ -585,13 +591,14 @@
     return [pltpu.with_memory_space_constraint(x, pltpu.HBM) for x in arrays]
 
 
-def call(kernel, outs, in_specs, flops=0, bytes_accessed=0, scratch=(), limit=None):
+def call(kernel, outs, in_specs, flops=0, bytes_accessed=0, scratch=(), limit=None, aliases={}):
     return pl.pallas_call(
         kernel,
         out_shape=outs,
         in_specs=in_specs,
         out_specs=jax.tree.map(lambda _: VMEM, outs),
         scratch_shapes=list(scratch),
+        input_output_aliases=aliases,
         cost_estimate=pl.CostEstimate(
             flops=flops, bytes_accessed=bytes_accessed, transcendentals=0
         ),
@@ -626,6 +633,7 @@
         sds = jax.ShapeDtypeStruct
 
         other = lax.ppermute(tokens, "tp", swap)
+        w_got = lax.ppermute(w_output, "tp", swap)
         gain = attn_gain.reshape(-1, LANES)
         w_query, tokens, gain, length_rows, rates = call(
             first_load_kernel,
@@ -658,7 +666,7 @@
             ]
 
         got = exchange(message, 1)
-        k_part, v_part, g_part, turn, weights, w_keep, w_send = call(
+        k_part, v_part, g_part, turn, weights, w_keep, keys = call(
             other_kernel,
             (
                 sds((S + 8, qc), F32),
@@ -667,12 +675,12 @@
                 sds((2, S, LANES), F32),
                 sds((S, H, LANES), F32),
                 sds((w_output.shape[0], own), BF),
-                sds((w_output.shape[0], own), BF),
+                sds(key_cache.shape, BF),
             ),
-            [ANY] + [VMEM] * 5 + [HBM] * 4,
+            [ANY] + [VMEM] * 5 + [HBM] * 5,
             flops=10**9,
             scratch=[pltpu.VMEM(w.shape, BF) for w in (w_key, w_value, w_gate)]
-            + [pltpu.SemaphoreType.DMA((5,))],
+            + [pltpu.SemaphoreType.DMA((4,)), pltpu.SemaphoreType.DMA((S // 2,))],
             limit=6 * mib,
         )(
             message,
@@ -681,9 +689,8 @@
             tokens,
             other,
             gain,
-            *in_hbm(w_key, w_value, w_gate, w_output),
-        )
-        w_got = lax.ppermute(w_send, "tp", swap)
+            *in_hbm(w_key, w_value, w_gate, w_output, key_cache),
+        )
 
         stride = 4
         while stride < kv:
@@ -695,11 +702,12 @@
         keys, values = call(
             cache_load_kernel,
             (sds(key_cache.shape, BF), sds(value_cache.shape, BF)),
-            [ANY, VMEM] + [HBM] * 2,
+            [ANY, VMEM] + [HBM] * 2 + [VMEM],
             flops=10**9,
             scratch=[pltpu.SemaphoreType.DMA((S,))] * 2,
             limit=2 * mib,
-        )(message, length_rows, *in_hbm(key_cache, value_cache))
+            aliases={4: 0},
+        )(message, length_rows, *in_hbm(key_cache, value_cache), keys)
 
         pieces = call(
             functools.partial(attend_kernel, width),

time: 69.1 us -> 69.9 us (1.012)
  waiting for transfers between devices: 3.95 us -> 4.92 us
    ppermute x1, waiting for transfers between devices: 0.01 us -> 1.36 us  [on_device(): other = lax.ppermute(tokens, 'tp', swap)]
  transfers between devices with their start and end apart: 8 -> 8, of which waited for: 3 -> 3; matrix products, arithmetic and copies ran while one was open for 0% -> 0% of each run, Pallas kernels for 9% -> 12%
where the time goes in v7:
time: 69.9 us; the launch traced here: 69.6 us
  blocking collectives  41.1 us (59%)
  Pallas kernels  14.1 us (20%)
  starting transfers between devices  9.35 us (13%)
  waiting for transfers between devices  4.92 us (7%)
    all_to_all x1, blocking collectives, on_device(): pieces = lax.all_to_all(pieces, 'kv', 0, 0, tiled=True)  10.9 us
    all_to_all x1, blocking collectives, on_device(): gated = lax.all_to_all(gated, ('kv', 'tp'), 0, 0, tiled=True)  10.3 us
    all_to_all x1, blocking collectives, on_device(): spread = lax.all_to_all(spread, ('kv', 'tp'), 0, 0, tiled=True)  9.97 us
    all_to_all x1, blocking collectives, on_device(): down = lax.all_to_all(down, ('kv', 'tp'), 0, 0, tiled=True)  9.97 us
    ppermute x6, starting transfers between devices, exchange(): lax.ppermute(message, 'kv', [(i, i ^ j * stride) for i in range(kv)])  8.84 us
    pallas_call x1, Pallas kernels, on_device(): call(cache_load_kernel, (sds(key_cache.shape, BF), sds(value_cache.shape,...  4.29 us
    ppermute x6, waiting for transfers between devices, exchange(): lax.ppermute(message, 'kv', [(i, i ^ j * stride) for i in range(kv)])  3.55 us
    pallas_call x1, Pallas kernels, on_device(): call(functools.partial(attend_kernel, width), sds((H, 3 * S + S // 2, LAN...  3.04 us
  transfers between devices with their start and end apart: 8, of which 3 were waited for; matrix products, arithmetic and copies ran while one was open for 0% of the time, Pallas kernels for 12%

profile of v7, /device:TPU:0, one launch (start us, length us, event | category | flops | bytes accessed | tf_op | source)
XLA Modules:
  0.0 69.6 jit_solution(11772782000289374001)
XLA Ops:
  0.0 0.5 collective-permute-start
  0.5 0.0 collective-permute-start.1
  0.5 1.1 %shard_map.145 = (bf16[256,1024]{1,0:T(8,128)(2,1)S(1)}, bf16[16,128]{1,0:T(8,128)(2,1)S(1)}, bf16[2,128]{1,0:T(2,128)(2,1)S(1)}, s32[16,128]{1,0:T(8,128)S(1)}, f32[16,128]{1,0:T(8,128)S(1)}) custom-call(bf16[256,1024]{1,0:T(8,128)(2,1)} %w_query.1, bf16[16,128]{1,0:T(8,128)(2,1)} %tokens.1, bf16[2,128]{1,0:T(2,128)(2,1)} %bitcast.5, s32[16]{0:T(128)} %lengths.1, ...), custom_call_target="tpu_custom_call" | custom-call | flops 1000000000 | tf_op jit(solution)/shard_map/pallas_call | solution.py:638
  1.6 1.4 %collective-permute-done.1.second = bf16[16,128]{1,0:T(8,128)(2,1)S(1)} collective-permute-done((bf16[16,128]{1,0:T(8,128)(2,1)}, bf16[16,128]{1,0:T(8,128)(2,1)S(1)}, u32[]{:S(2)}, u32[]{:S(2)}) %collective-permute-start.1) | collective-permute-done | bytes 4128 | tf_op jit(solution)/shard_map/ppermute | solution.py:635
  3.0 0.2 shard_map.146
  3.2 2.9 %collective-permute-start.2 = (bf16[16,1280]{1,0:T(8,128)(2,1)S(1)}, bf16[16,1280]{1,0:T(8,128)(2,1)S(1)}, u32[]{:S(2)}, u32[]{:S(2)}) collective-permute-start(bf16[16,1280]{1,0:T(8,128)(2,1)S(1)} %get-tuple-element.30.after), channel_id=1, source_target_pairs={{0,2},{2,0},{4,6},{6,4},{8,10},{10,8},{12,14},{14,12},{16,18},{18,... | collective-permute-start | bytes 122888 | tf_op jit(solution)/shard_map/ppermute | solution.py:664
  6.1 1.5 %collective-permute-start.3 = (bf16[16,1280]{1,0:T(8,128)(2,1)S(1)}, bf16[16,1280]{1,0:T(8,128)(2,1)S(1)}, u32[]{:S(2)}, u32[]{:S(2)}) collective-permute-start(bf16[16,1280]{1,0:T(8,128)(2,1)S(1)} %get-tuple-element.30.after), channel_id=1, source_target_pairs={{0,4},{2,6},{4,0},{6,2},{8,12},{10,14},{12,8},{14,10},{16,20},{18,... | collective-permute-start | bytes 122888 | tf_op jit(solution)/shard_map/ppermute | solution.py:664
  7.6 0.0 collective-permute-start.4
  7.7 2.6 %shard_map.148 = (f32[24,1024]{1,0:T(8,128)S(1)}, f32[24,2048]{1,0:T(8,128)S(1)}, f32[24,2048]{1,0:T(8,128)S(1)}, f32[2,16,128]{2,1,0:T(8,128)S(1)}, f32[16,16,1...) custom-call(bf16[16,1280]{1,0:T(8,128)(2,1)S(1)} %get-tuple-element.30.after, ...), custom_call_target="tpu_custom_call" | custom-call | flops 1000000000 | tf_op jit(solution)/shard_map/pallas_call | solution.py:669
  10.2 0.0 collective-permute-done.2.m1
  10.2 0.0 collective-permute-done.3.m2
  10.3 2.3 %collective-permute-done.4.m3 = bf16[16,1280]{1,0:T(8,128)(2,1)S(1)} collective-permute-done((bf16[16,1280]{1,0:T(8,128)(2,1)S(1)}, bf16[16,1280]{1,0:T(8,128)(2,1)S(1)}, u32[]{:S(2)}, u32[]{:S(2)}) %collective-permute-start.4) | collective-permute-done | bytes 40992 | tf_op jit(solution)/shard_map/ppermute | solution.py:664
  12.5 0.2 shard_map.147
  12.7 1.6 %collective-permute-start.5 = (bf16[16,1280]{1,0:T(8,128)(2,1)S(1)}, bf16[16,1280]{1,0:T(8,128)(2,1)S(1)}, u32[]{:S(2)}, u32[]{:S(2)}) collective-permute-start(bf16[16,1280]{1,0:T(8,128)(2,1)S(1)} %get-tuple-element.32.after), channel_id=1, source_target_pairs={{0,8},{2,10},{4,12},{6,14},{8,0},{10,2},{12,4},{14,6},{16,24},{18,... | collective-permute-start | bytes 122888 | tf_op jit(solution)/shard_map/ppermute | solution.py:664
  14.3 2.6 %collective-permute-start.6 = (bf16[16,1280]{1,0:T(8,128)(2,1)S(1)}, bf16[16,1280]{1,0:T(8,128)(2,1)S(1)}, u32[]{:S(2)}, u32[]{:S(2)}) collective-permute-start(bf16[16,1280]{1,0:T(8,128)(2,1)S(1)} %get-tuple-element.32.after), channel_id=1, source_target_pairs={{0,16},{2,18},{4,20},{6,22},{8,24},{10,26},{12,28},{14,30},{16,0},... | collective-permute-start | bytes 122888 | tf_op jit(solution)/shard_map/ppermute | solution.py:664
  16.9 0.2 collective-permute-start.7
  17.1 4.3 %shard_map.149 = (bf16[16,128,1024]{2,1,0:T(8,128)(2,1)S(1)}, bf16[16,128,2048]{2,1,0:T(8,128)(2,1)S(1)}) custom-call(bf16[16,1280]{1,0:T(8,128)(2,1)S(1)} %get-tuple-element.32.after, s32[16,128]{1,0:T(8,128)S(1)} %get-tuple-element.25.lengths, bf16[16,128,1024]{2,1,0:T(8,128)(2,1)} %keys.3, ...), custom_call_target="tpu_custom_call", output_to_operand_aliasing={{0}: (4, {})} | custom-call | flops 1000000000 | tf_op jit(solution)/shard_map/pallas_call | solution.py:702
  21.4 0.0 collective-permute-done.5.m1
  21.4 0.0 collective-permute-done.6.m2
  21.4 1.3 %collective-permute-done.7.m3 = bf16[16,1280]{1,0:T(8,128)(2,1)S(1)} collective-permute-done((bf16[16,1280]{1,0:T(8,128)(2,1)S(1)}, bf16[16,1280]{1,0:T(8,128)(2,1)S(1)}, u32[]{:S(2)}, u32[]{:S(2)}) %collective-permute-start.7) | collective-permute-done | bytes 40992 | tf_op jit(solution)/shard_map/ppermute | solution.py:664
  22.7 0.0 collective-permute-done.after.w_got
  22.7 0.0 copy-start.2
  22.7 3.0 %shard_map.150 = bf16[16,56,128]{2,1,0:T(8,128)(2,1)S(1)} custom-call(bf16[2048,256]{1,0:T(8,128)(2,1)S(1)} %collective-permute-done.after.w_got, s32[16,128]{1,0:T(8,128)S(1)} %get-tuple-element.25.lengths, f32[16,1280]{1,0:T(8,128)S(1)} %get-tuple-element.31.old, bf16[16,1280]{1,0:T(8,128)(2,1)S(1)} %collective-permute-done.5.m1, ...), custom_call_target="tpu_custom_call" | custom-call | tf_op jit(solution)/shard_map/pallas_call | solution.py:712
  25.7 10.9 %all_to_all.20.pieces = bf16[16,56,128]{2,1,0:T(8,128)(2,1)S(1)} all-to-all(bf16[16,56,128]{2,1,0:T(8,128)(2,1)S(1)} %shard_map.150), channel_id=1, replica_groups=mesh['kv'=16,'tp'=2] {'kv'}, dimensions={0} | all-to-all | bytes 458752 | tf_op jit(solution)/shard_map/all_to_all | solution.py:724
  36.7 0.4 shard_map.151
  37.1 10.3 %all_to_all.21.gated = bf16[32,16,128]{2,1,0:T(8,128)(2,1)S(1)} all-to-all(bf16[32,16,128]{2,1,0:T(8,128)(2,1)S(1)} %shard_map.151), channel_id=1, replica_groups=mesh['kv'=16,'tp'=2] {'kv','tp'}, dimensions={0} | all-to-all | bytes 262144 | tf_op jit(solution)/shard_map/all_to_all | solution.py:728
  47.3 0.3 shard_map.152
  47.6 10.0 %all_to_all.22.residual = bf16[32,16,128]{2,1,0:T(8,128)(2,1)S(1)} all-to-all(bf16[32,16,128]{2,1,0:T(8,128)(2,1)S(1)} %get-tuple-element.43), channel_id=1, replica_groups=mesh['kv'=16,'tp'=2] {'kv','tp'}, dimensions={0} | all-to-all | bytes 262144 | tf_op jit(solution)/shard_map/all_to_all | solution.py:735
  57.6 0.0 copy-done.1
  57.6 1.5 %shard_map.153 = bf16[32,16,128]{2,1,0:T(8,128)(2,1)S(1)} custom-call(bf16[32,16,128]{2,1,0:T(8,128)(2,1)S(1)} %all_to_all.22.residual, bf16[32,128]{1,0:T(8,128)(2,1)S(1)} %bitcast.3, bf16[4096,512]{1,0:T(8,128)(2,1)S(1)} %copy-done, bf16[512,4096]{1,0:T(8,128)(2,1)S(1)} %copy-done.1), custom_call_target="tpu_custom_call" | custom-call | tf_op jit(solution)/shard_map/pallas_call | solution.py:736
  59.0 10.0 %all_to_all.23.pieces = bf16[32,16,128]{2,1,0:T(8,128)(2,1)S(1)} all-to-all(bf16[32,16,128]{2,1,0:T(8,128)(2,1)S(1)} %shard_map.153), channel_id=1, replica_groups=mesh['kv'=16,'tp'=2] {'kv','tp'}, dimensions={0} | all-to-all | bytes 262144 | tf_op jit(solution)/shard_map/all_to_all | solution.py:739
  69.0 0.6 shard_map.154
  (6 shorter events, 0.0 us)
Async XLA Ops:
  0.0 22.7 %collective-permute-start = (bf16[2048,256]{1,0:T(8,128)(2,1)}, bf16[2048,256]{1,0:T(8,128)(2,1)S(1)}, u32[]{:S(2)}, u32[]{:S(2)}) collective-permute-start(bf16[2048,256]{1,0:T(8,128)(2,1)} %w_output.1), channel_id=1, source_target_pairs={{0,1},{1,0},{2,3},{3,2},{4,5},{5,4},{6,7},{7,6},{8,9},{9,8},{10,11... | collective-permute-start | bytes 3145736 | tf_op jit(solution)/shard_map/ppermute | solution.py:636
  0.5 2.5 %collective-permute-start.1 = (bf16[16,128]{1,0:T(8,128)(2,1)}, bf16[16,128]{1,0:T(8,128)(2,1)S(1)}, u32[]{:S(2)}, u32[]{:S(2)}) collective-permute-start(bf16[16,128]{1,0:T(8,128)(2,1)} %tokens.1), channel_id=1, source_target_pairs={{0,1},{1,0},{2,3},{3,2},{4,5},{5,4},{6,7},{7,6},{8,9},{9,8},{10,11... | collective-permute-start | bytes 12296 | tf_op jit(solution)/shard_map/ppermute | solution.py:635
  3.2 7.0 %collective-permute-start.2 = (bf16[16,1280]{1,0:T(8,128)(2,1)S(1)}, bf16[16,1280]{1,0:T(8,128)(2,1)S(1)}, u32[]{:S(2)}, u32[]{:S(2)}) collective-permute-start(bf16[16,1280]{1,0:T(8,128)(2,1)S(1)} %get-tuple-element.30.after), channel_id=1, source_target_pairs={{0,2},{2,0},{4,6},{6,4},{8,10},{10,8},{12,14},{14,12},{16,18},{18,... | collective-permute-start | bytes 122888 | tf_op jit(solution)/shard_map/ppermute | solution.py:664
  6.1 4.1 %collective-permute-start.3 = (bf16[16,1280]{1,0:T(8,128)(2,1)S(1)}, bf16[16,1280]{1,0:T(8,128)(2,1)S(1)}, u32[]{:S(2)}, u32[]{:S(2)}) collective-permute-start(bf16[16,1280]{1,0:T(8,128)(2,1)S(1)} %get-tuple-element.30.after), channel_id=1, source_target_pairs={{0,4},{2,6},{4,0},{6,2},{8,12},{10,14},{12,8},{14,10},{16,20},{18,... | collective-permute-start | bytes 122888 | tf_op jit(solution)/shard_map/ppermute | solution.py:664
  7.6 4.9 %collective-permute-start.4 = (bf16[16,1280]{1,0:T(8,128)(2,1)S(1)}, bf16[16,1280]{1,0:T(8,128)(2,1)S(1)}, u32[]{:S(2)}, u32[]{:S(2)}) collective-permute-start(bf16[16,1280]{1,0:T(8,128)(2,1)S(1)} %get-tuple-element.30.after), channel_id=1, source_target_pairs={{0,6},{2,4},{4,2},{6,0},{8,14},{10,12},{12,10},{14,8},{16,22},{18,... | collective-permute-start | bytes 122888 | tf_op jit(solution)/shard_map/ppermute | solution.py:664
  12.7 8.7 %collective-permute-start.5 = (bf16[16,1280]{1,0:T(8,128)(2,1)S(1)}, bf16[16,1280]{1,0:T(8,128)(2,1)S(1)}, u32[]{:S(2)}, u32[]{:S(2)}) collective-permute-start(bf16[16,1280]{1,0:T(8,128)(2,1)S(1)} %get-tuple-element.32.after), channel_id=1, source_target_pairs={{0,8},{2,10},{4,12},{6,14},{8,0},{10,2},{12,4},{14,6},{16,24},{18,... | collective-permute-start | bytes 122888 | tf_op jit(solution)/shard_map/ppermute | solution.py:664
  14.3 7.1 %collective-permute-start.6 = (bf16[16,1280]{1,0:T(8,128)(2,1)S(1)}, bf16[16,1280]{1,0:T(8,128)(2,1)S(1)}, u32[]{:S(2)}, u32[]{:S(2)}) collective-permute-start(bf16[16,1280]{1,0:T(8,128)(2,1)S(1)} %get-tuple-element.32.after), channel_id=1, source_target_pairs={{0,16},{2,18},{4,20},{6,22},{8,24},{10,26},{12,28},{14,30},{16,0},... | collective-permute-start | bytes 122888 | tf_op jit(solution)/shard_map/ppermute | solution.py:664
  16.9 5.8 %collective-permute-start.7 = (bf16[16,1280]{1,0:T(8,128)(2,1)S(1)}, bf16[16,1280]{1,0:T(8,128)(2,1)S(1)}, u32[]{:S(2)}, u32[]{:S(2)}) collective-permute-start(bf16[16,1280]{1,0:T(8,128)(2,1)S(1)} %get-tuple-element.32.after), channel_id=1, source_target_pairs={{0,24},{2,26},{4,28},{6,30},{8,16},{10,18},{12,20},{14,22},{16,8},... | collective-permute-start | bytes 122888 | tf_op jit(solution)/shard_map/ppermute | solution.py:664
  22.7 14.0 %copy-start.3 = (bf16[2048]{0:T(1024)(128)(2,1)S(1)}, bf16[2048]{0:T(1024)(128)(2,1)}, u32[]{:S(2)}) copy-start(bf16[2048]{0:T(1024)(128)(2,1)} %param.25) | copy-start | bytes 12292
  22.7 34.9 %copy-start = (bf16[4096,512]{1,0:T(8,128)(2,1)S(1)}, bf16[4096,512]{1,0:T(8,128)(2,1)}, u32[]{:S(2)}) copy-start(bf16[4096,512]{1,0:T(8,128)(2,1)} %w_up.1) | copy-start | bytes 12582916
  22.7 34.9 %copy-start.1 = (bf16[512,4096]{1,0:T(8,128)(2,1)S(1)}, bf16[512,4096]{1,0:T(8,128)(2,1)}, u32[]{:S(2)}) copy-start(bf16[512,4096]{1,0:T(8,128)(2,1)} %w_down.1) | copy-start | bytes 12582916
  22.7 34.9 %copy-start.2 = (bf16[4096]{0:T(1024)(128)(2,1)S(1)}, bf16[4096]{0:T(1024)(128)(2,1)}, u32[]{:S(2)}) copy-start(bf16[4096]{0:T(1024)(128)(2,1)} %param.27) | copy-start | bytes 24580

commit v8 on v7

--- a/solution.py
+++ b/solution.py
@@ -660,10 +660,11 @@
         )(tokens, other, gain, w_query)
 
         def exchange(message, stride):
-            return [
-                lax.ppermute(message, "kv", [(i, i ^ (j * stride)) for i in range(kv)])
-                for j in range(1, 4)
-            ]
+            got = []
+            for j in range(1, 4):
+                pairs = [(i, i ^ (j * stride)) for i in range(kv)]
+                got.append(lax.ppermute(message, "kv", pairs))
+            return got
 
         got = exchange(message, 1)
         k_part, v_part, g_part, turn, weights, w_keep, keys = call(

time: 69.9 us -> 69.9 us (level)
  no operation moved by 1% of the time
where the time goes in v8:
time: 69.9 us; the launch traced here: 69.6 us
  blocking collectives  41.1 us (59%)
  Pallas kernels  14.1 us (20%)
  starting transfers between devices  9.35 us (13%)
  waiting for transfers between devices  4.92 us (7%)
    all_to_all x1, blocking collectives, on_device(): pieces = lax.all_to_all(pieces, 'kv', 0, 0, tiled=True)  10.9 us
    all_to_all x1, blocking collectives, on_device(): gated = lax.all_to_all(gated, ('kv', 'tp'), 0, 0, tiled=True)  10.3 us
    all_to_all x1, blocking collectives, on_device(): spread = lax.all_to_all(spread, ('kv', 'tp'), 0, 0, tiled=True)  9.97 us
    all_to_all x1, blocking collectives, on_device(): down = lax.all_to_all(down, ('kv', 'tp'), 0, 0, tiled=True)  9.97 us
    ppermute x6, starting transfers between devices, exchange(): got.append(lax.ppermute(message, 'kv', pairs))  8.84 us
    pallas_call x1, Pallas kernels, on_device(): call(cache_load_kernel, (sds(key_cache.shape, BF), sds(value_cache.shape,...  4.29 us
    ppermute x6, waiting for transfers between devices, exchange(): got.append(lax.ppermute(message, 'kv', pairs))  3.55 us
    pallas_call x1, Pallas kernels, on_device(): call(functools.partial(attend_kernel, width), sds((H, 3 * S + S // 2, LAN...  3.04 us
  transfers between devices with their start and end apart: 8, of which 3 were waited for; matrix products, arithmetic and copies ran while one was open for 0% of the time, Pallas kernels for 12%

profile of v8, /device:TPU:0, one launch (start us, length us, event | category | flops | bytes accessed | tf_op | source)
XLA Modules:
  0.0 69.6 jit_solution(11772782000289374001)
XLA Ops:
  0.0 0.5 collective-permute-start
  0.5 0.0 collective-permute-start.1
  0.5 1.1 %shard_map.145 = (bf16[256,1024]{1,0:T(8,128)(2,1)S(1)}, bf16[16,128]{1,0:T(8,128)(2,1)S(1)}, bf16[2,128]{1,0:T(2,128)(2,1)S(1)}, s32[16,128]{1,0:T(8,128)S(1)}, f32[16,128]{1,0:T(8,128)S(1)}) custom-call(bf16[256,1024]{1,0:T(8,128)(2,1)} %w_query.1, bf16[16,128]{1,0:T(8,128)(2,1)} %tokens.1, bf16[2,128]{1,0:T(2,128)(2,1)} %bitcast.5, s32[16]{0:T(128)} %lengths.1, ...), custom_call_target="tpu_custom_call" | custom-call | flops 1000000000 | tf_op jit(solution)/shard_map/pallas_call | solution.py:638
  1.6 1.4 %collective-permute-done.1.second = bf16[16,128]{1,0:T(8,128)(2,1)S(1)} collective-permute-done((bf16[16,128]{1,0:T(8,128)(2,1)}, bf16[16,128]{1,0:T(8,128)(2,1)S(1)}, u32[]{:S(2)}, u32[]{:S(2)}) %collective-permute-start.1) | collective-permute-done | bytes 4128 | tf_op jit(solution)/shard_map/ppermute | solution.py:635
  3.0 0.2 shard_map.146
  3.2 2.9 %collective-permute-start.2 = (bf16[16,1280]{1,0:T(8,128)(2,1)S(1)}, bf16[16,1280]{1,0:T(8,128)(2,1)S(1)}, u32[]{:S(2)}, u32[]{:S(2)}) collective-permute-start(bf16[16,1280]{1,0:T(8,128)(2,1)S(1)} %get-tuple-element.30.after), channel_id=1, source_target_pairs={{0,2},{2,0},{4,6},{6,4},{8,10},{10,8},{12,14},{14,12},{16,18},{18,... | collective-permute-start | bytes 122888 | tf_op jit(solution)/shard_map/ppermute | solution.py:666
  6.1 1.5 %collective-permute-start.3 = (bf16[16,1280]{1,0:T(8,128)(2,1)S(1)}, bf16[16,1280]{1,0:T(8,128)(2,1)S(1)}, u32[]{:S(2)}, u32[]{:S(2)}) collective-permute-start(bf16[16,1280]{1,0:T(8,128)(2,1)S(1)} %get-tuple-element.30.after), channel_id=1, source_target_pairs={{0,4},{2,6},{4,0},{6,2},{8,12},{10,14},{12,8},{14,10},{16,20},{18,... | collective-permute-start | bytes 122888 | tf_op jit(solution)/shard_map/ppermute | solution.py:666
  7.6 0.0 collective-permute-start.4
  7.7 2.6 %shard_map.148 = (f32[24,1024]{1,0:T(8,128)S(1)}, f32[24,2048]{1,0:T(8,128)S(1)}, f32[24,2048]{1,0:T(8,128)S(1)}, f32[2,16,128]{2,1,0:T(8,128)S(1)}, f32[16,16,1...) custom-call(bf16[16,1280]{1,0:T(8,128)(2,1)S(1)} %get-tuple-element.30.after, ...), custom_call_target="tpu_custom_call" | custom-call | flops 1000000000 | tf_op jit(solution)/shard_map/pallas_call | solution.py:670
  10.2 0.0 collective-permute-done.2.m1
  10.2 0.0 collective-permute-done.3.m2
  10.3 2.3 %collective-permute-done.4.m3 = bf16[16,1280]{1,0:T(8,128)(2,1)S(1)} collective-permute-done((bf16[16,1280]{1,0:T(8,128)(2,1)S(1)}, bf16[16,1280]{1,0:T(8,128)(2,1)S(1)}, u32[]{:S(2)}, u32[]{:S(2)}) %collective-permute-start.4) | collective-permute-done | bytes 40992 | tf_op jit(solution)/shard_map/ppermute | solution.py:666
  12.5 0.2 shard_map.147
  12.7 1.6 %collective-permute-start.5 = (bf16[16,1280]{1,0:T(8,128)(2,1)S(1)}, bf16[16,1280]{1,0:T(8,128)(2,1)S(1)}, u32[]{:S(2)}, u32[]{:S(2)}) collective-permute-start(bf16[16,1280]{1,0:T(8,128)(2,1)S(1)} %get-tuple-element.32.after), channel_id=1, source_target_pairs={{0,8},{2,10},{4,12},{6,14},{8,0},{10,2},{12,4},{14,6},{16,24},{18,... | collective-permute-start | bytes 122888 | tf_op jit(solution)/shard_map/ppermute | solution.py:666
  14.3 2.6 %collective-permute-start.6 = (bf16[16,1280]{1,0:T(8,128)(2,1)S(1)}, bf16[16,1280]{1,0:T(8,128)(2,1)S(1)}, u32[]{:S(2)}, u32[]{:S(2)}) collective-permute-start(bf16[16,1280]{1,0:T(8,128)(2,1)S(1)} %get-tuple-element.32.after), channel_id=1, source_target_pairs={{0,16},{2,18},{4,20},{6,22},{8,24},{10,26},{12,28},{14,30},{16,0},... | collective-permute-start | bytes 122888 | tf_op jit(solution)/shard_map/ppermute | solution.py:666
  16.9 0.2 collective-permute-start.7
  17.1 4.3 %shard_map.149 = (bf16[16,128,1024]{2,1,0:T(8,128)(2,1)S(1)}, bf16[16,128,2048]{2,1,0:T(8,128)(2,1)S(1)}) custom-call(bf16[16,1280]{1,0:T(8,128)(2,1)S(1)} %get-tuple-element.32.after, s32[16,128]{1,0:T(8,128)S(1)} %get-tuple-element.25.lengths, bf16[16,128,1024]{2,1,0:T(8,128)(2,1)} %keys.3, ...), custom_call_target="tpu_custom_call", output_to_operand_aliasing={{0}: (4, {})} | custom-call | flops 1000000000 | tf_op jit(solution)/shard_map/pallas_call | solution.py:703
  21.4 0.0 collective-permute-done.5.m1
  21.4 0.0 collective-permute-done.6.m2
  21.4 1.3 %collective-permute-done.7.m3 = bf16[16,1280]{1,0:T(8,128)(2,1)S(1)} collective-permute-done((bf16[16,1280]{1,0:T(8,128)(2,1)S(1)}, bf16[16,1280]{1,0:T(8,128)(2,1)S(1)}, u32[]{:S(2)}, u32[]{:S(2)}) %collective-permute-start.7) | collective-permute-done | bytes 40992 | tf_op jit(solution)/shard_map/ppermute | solution.py:666
  22.7 0.0 collective-permute-done.after.w_got
  22.7 0.0 copy-start.2
  22.7 3.0 %shard_map.150 = bf16[16,56,128]{2,1,0:T(8,128)(2,1)S(1)} custom-call(bf16[2048,256]{1,0:T(8,128)(2,1)S(1)} %collective-permute-done.after.w_got, s32[16,128]{1,0:T(8,128)S(1)} %get-tuple-element.25.lengths, f32[16,1280]{1,0:T(8,128)S(1)} %get-tuple-element.31.old, bf16[16,1280]{1,0:T(8,128)(2,1)S(1)} %collective-permute-done.5.m1, ...), custom_call_target="tpu_custom_call" | custom-call | tf_op jit(solution)/shard_map/pallas_call | solution.py:713
  25.7 10.9 %all_to_all.20.pieces = bf16[16,56,128]{2,1,0:T(8,128)(2,1)S(1)} all-to-all(bf16[16,56,128]{2,1,0:T(8,128)(2,1)S(1)} %shard_map.150), channel_id=1, replica_groups=mesh['kv'=16,'tp'=2] {'kv'}, dimensions={0} | all-to-all | bytes 458752 | tf_op jit(solution)/shard_map/all_to_all | solution.py:725
  36.7 0.4 shard_map.151
  37.1 10.3 %all_to_all.21.gated = bf16[32,16,128]{2,1,0:T(8,128)(2,1)S(1)} all-to-all(bf16[32,16,128]{2,1,0:T(8,128)(2,1)S(1)} %shard_map.151), channel_id=1, replica_groups=mesh['kv'=16,'tp'=2] {'kv','tp'}, dimensions={0} | all-to-all | bytes 262144 | tf_op jit(solution)/shard_map/all_to_all | solution.py:729
  47.3 0.3 shard_map.152
  47.6 10.0 %all_to_all.22.residual = bf16[32,16,128]{2,1,0:T(8,128)(2,1)S(1)} all-to-all(bf16[32,16,128]{2,1,0:T(8,128)(2,1)S(1)} %get-tuple-element.43), channel_id=1, replica_groups=mesh['kv'=16,'tp'=2] {'kv','tp'}, dimensions={0} | all-to-all | bytes 262144 | tf_op jit(solution)/shard_map/all_to_all | solution.py:736
  57.6 0.0 copy-done.1
  57.6 1.5 %shard_map.153 = bf16[32,16,128]{2,1,0:T(8,128)(2,1)S(1)} custom-call(bf16[32,16,128]{2,1,0:T(8,128)(2,1)S(1)} %all_to_all.22.residual, bf16[32,128]{1,0:T(8,128)(2,1)S(1)} %bitcast.3, bf16[4096,512]{1,0:T(8,128)(2,1)S(1)} %copy-done, bf16[512,4096]{1,0:T(8,128)(2,1)S(1)} %copy-done.1), custom_call_target="tpu_custom_call" | custom-call | tf_op jit(solution)/shard_map/pallas_call | solution.py:737
  59.0 10.0 %all_to_all.23.pieces = bf16[32,16,128]{2,1,0:T(8,128)(2,1)S(1)} all-to-all(bf16[32,16,128]{2,1,0:T(8,128)(2,1)S(1)} %shard_map.153), channel_id=1, replica_groups=mesh['kv'=16,'tp'=2] {'kv','tp'}, dimensions={0} | all-to-all | bytes 262144 | tf_op jit(solution)/shard_map/all_to_all | solution.py:740
  69.0 0.6 shard_map.154
  (6 shorter events, 0.0 us)
Async XLA Ops:
  0.0 22.7 %collective-permute-start = (bf16[2048,256]{1,0:T(8,128)(2,1)}, bf16[2048,256]{1,0:T(8,128)(2,1)S(1)}, u32[]{:S(2)}, u32[]{:S(2)}) collective-permute-start(bf16[2048,256]{1,0:T(8,128)(2,1)} %w_output.1), channel_id=1, source_target_pairs={{0,1},{1,0},{2,3},{3,2},{4,5},{5,4},{6,7},{7,6},{8,9},{9,8},{10,11... | collective-permute-start | bytes 3145736 | tf_op jit(solution)/shard_map/ppermute | solution.py:636
  0.5 2.5 %collective-permute-start.1 = (bf16[16,128]{1,0:T(8,128)(2,1)}, bf16[16,128]{1,0:T(8,128)(2,1)S(1)}, u32[]{:S(2)}, u32[]{:S(2)}) collective-permute-start(bf16[16,128]{1,0:T(8,128)(2,1)} %tokens.1), channel_id=1, source_target_pairs={{0,1},{1,0},{2,3},{3,2},{4,5},{5,4},{6,7},{7,6},{8,9},{9,8},{10,11... | collective-permute-start | bytes 12296 | tf_op jit(solution)/shard_map/ppermute | solution.py:635
  3.2 7.0 %collective-permute-start.2 = (bf16[16,1280]{1,0:T(8,128)(2,1)S(1)}, bf16[16,1280]{1,0:T(8,128)(2,1)S(1)}, u32[]{:S(2)}, u32[]{:S(2)}) collective-permute-start(bf16[16,1280]{1,0:T(8,128)(2,1)S(1)} %get-tuple-element.30.after), channel_id=1, source_target_pairs={{0,2},{2,0},{4,6},{6,4},{8,10},{10,8},{12,14},{14,12},{16,18},{18,... | collective-permute-start | bytes 122888 | tf_op jit(solution)/shard_map/ppermute | solution.py:666
  6.1 4.1 %collective-permute-start.3 = (bf16[16,1280]{1,0:T(8,128)(2,1)S(1)}, bf16[16,1280]{1,0:T(8,128)(2,1)S(1)}, u32[]{:S(2)}, u32[]{:S(2)}) collective-permute-start(bf16[16,1280]{1,0:T(8,128)(2,1)S(1)} %get-tuple-element.30.after), channel_id=1, source_target_pairs={{0,4},{2,6},{4,0},{6,2},{8,12},{10,14},{12,8},{14,10},{16,20},{18,... | collective-permute-start | bytes 122888 | tf_op jit(solution)/shard_map/ppermute | solution.py:666
  7.6 4.9 %collective-permute-start.4 = (bf16[16,1280]{1,0:T(8,128)(2,1)S(1)}, bf16[16,1280]{1,0:T(8,128)(2,1)S(1)}, u32[]{:S(2)}, u32[]{:S(2)}) collective-permute-start(bf16[16,1280]{1,0:T(8,128)(2,1)S(1)} %get-tuple-element.30.after), channel_id=1, source_target_pairs={{0,6},{2,4},{4,2},{6,0},{8,14},{10,12},{12,10},{14,8},{16,22},{18,... | collective-permute-start | bytes 122888 | tf_op jit(solution)/shard_map/ppermute | solution.py:666
  12.7 8.7 %collective-permute-start.5 = (bf16[16,1280]{1,0:T(8,128)(2,1)S(1)}, bf16[16,1280]{1,0:T(8,128)(2,1)S(1)}, u32[]{:S(2)}, u32[]{:S(2)}) collective-permute-start(bf16[16,1280]{1,0:T(8,128)(2,1)S(1)} %get-tuple-element.32.after), channel_id=1, source_target_pairs={{0,8},{2,10},{4,12},{6,14},{8,0},{10,2},{12,4},{14,6},{16,24},{18,... | collective-permute-start | bytes 122888 | tf_op jit(solution)/shard_map/ppermute | solution.py:666
  14.3 7.1 %collective-permute-start.6 = (bf16[16,1280]{1,0:T(8,128)(2,1)S(1)}, bf16[16,1280]{1,0:T(8,128)(2,1)S(1)}, u32[]{:S(2)}, u32[]{:S(2)}) collective-permute-start(bf16[16,1280]{1,0:T(8,128)(2,1)S(1)} %get-tuple-element.32.after), channel_id=1, source_target_pairs={{0,16},{2,18},{4,20},{6,22},{8,24},{10,26},{12,28},{14,30},{16,0},... | collective-permute-start | bytes 122888 | tf_op jit(solution)/shard_map/ppermute | solution.py:666
  16.9 5.8 %collective-permute-start.7 = (bf16[16,1280]{1,0:T(8,128)(2,1)S(1)}, bf16[16,1280]{1,0:T(8,128)(2,1)S(1)}, u32[]{:S(2)}, u32[]{:S(2)}) collective-permute-start(bf16[16,1280]{1,0:T(8,128)(2,1)S(1)} %get-tuple-element.32.after), channel_id=1, source_target_pairs={{0,24},{2,26},{4,28},{6,30},{8,16},{10,18},{12,20},{14,22},{16,8},... | collective-permute-start | bytes 122888 | tf_op jit(solution)/shard_map/ppermute | solution.py:666
  22.7 14.0 %copy-start.3 = (bf16[2048]{0:T(1024)(128)(2,1)S(1)}, bf16[2048]{0:T(1024)(128)(2,1)}, u32[]{:S(2)}) copy-start(bf16[2048]{0:T(1024)(128)(2,1)} %param.25) | copy-start | bytes 12292
  22.7 34.9 %copy-start = (bf16[4096,512]{1,0:T(8,128)(2,1)S(1)}, bf16[4096,512]{1,0:T(8,128)(2,1)}, u32[]{:S(2)}) copy-start(bf16[4096,512]{1,0:T(8,128)(2,1)} %w_up.1) | copy-start | bytes 12582916
  22.7 34.9 %copy-start.1 = (bf16[512,4096]{1,0:T(8,128)(2,1)S(1)}, bf16[512,4096]{1,0:T(8,128)(2,1)}, u32[]{:S(2)}) copy-start(bf16[512,4096]{1,0:T(8,128)(2,1)} %w_down.1) | copy-start | bytes 12582916
  22.7 34.9 %copy-start.2 = (bf16[4096]{0:T(1024)(128)(2,1)S(1)}, bf16[4096]{0:T(1024)(128)(2,1)}, u32[]{:S(2)}) copy-start(bf16[4096]{0:T(1024)(128)(2,1)} %param.27) | copy-start | bytes 24580

commit v9 on v8

--- a/solution.py
+++ b/solution.py
@@ -434,6 +434,7 @@
     values,
     out,
     query_rows,
+    plain_rows,
     cached,
     order,
 ):
@@ -455,11 +456,17 @@
             -pltpu.roll(plain, LANES - HEAD_KEY // 2, 1),
             pltpu.roll(plain, HEAD_KEY // 2, 1),
         )
-        turned = plain * cosine + partner * sine
-        query_rows[:, cut] = turned.astype(BF).astype(F32)
-        part = inverse * (k_part[:rows, cut] - average * k_part[rows : rows + 1, cut])
-        both = plain * part * HEAD_KEY ** (-0.5)
+        plain_rows[:, cut] = plain
+        query_rows[:, cut] = (plain * cosine + partner * sine).astype(BF).astype(F32)
+
+    def normed(part, cut):
+        return inverse * (part[:rows, cut] - average * part[rows : rows + 1, cut])
+
+    def side(i):
+        cut = slice(i * LANES, (i + 1) * LANES)
+        both = plain_rows[:, cut] * normed(k_part, cut) * HEAD_KEY ** (-0.5)
         for j in range(2):
+            h = 2 * i + j
             picked = jnp.where(low_head == (j == 0), both, 0.0)
             score = jnp.sum(picked, 1, keepdims=True)
             high = score.astype(BF).astype(F32)
@@ -469,12 +476,10 @@
                 jnp.where(in_first[:top], high[:top], low[:top]),
                 jnp.where(in_first[:top], high[top:], low[top:]),
             )
-            out[2 * i + j, 3 * rows :, :] = folded.astype(BF)
-    for h in range(heads):
-        cut = slice(h * LANES, (h + 1) * LANES)
-        for place, part in ((1, v_part), (2, g_part)):
-            normed = inverse * (part[:rows, cut] - average * part[rows : rows + 1, cut])
-            out[h, place * rows : (place + 1) * rows, :] = normed.astype(BF)
+            out[h, 3 * rows :, :] = folded.astype(BF)
+            cut = slice(h * LANES, (h + 1) * LANES)
+            for place, part in ((1, v_part), (2, g_part)):
+                out[h, place * rows : (place + 1) * rows, :] = normed(part, cut).astype(BF)
 
     head_of_key = lax.broadcasted_iota(jnp.int32, (heads, key_columns), 1) // HEAD_KEY
     own_key = head_of_key == row_ids(heads, key_columns)
@@ -500,18 +505,24 @@
         kept = jnp.logical_and(own_value, is_live)
         cached[row, :] = jnp.sum(jnp.where(kept, product, 0.0), 0, keepdims=True)
 
-    steps = [n for n in (4, 8) if n < rows] + [rows]
-    for least, most in zip([-1] + steps[:-1], steps):
+    quarter = rows // 4
+    pairs = heads // 2
+    for most in range(quarter, rows + 1, quarter):
+        least = most - quarter if most > quarter else -1
 
         @pl.when(jnp.logical_and(count > least, count <= most))
         def _():
-            if most == rows:
-                for s in range(rows):
-                    one(s, live[s])
-            else:
+            if most < rows:
                 cached[...] = jnp.zeros_like(cached)
-                for i in range(most):
+            done = 0
+            for i in range(most):
+                if most == rows:
+                    one(i, live[i])
+                else:
                     one(order[jnp.minimum(i, jnp.maximum(count - 1, 0))], count > 0)
+                while done * most < (i + 1) * pairs:
+                    side(done)
+                    done += 1
 
     for h in range(heads):
         out[h, :rows, :] = cached[:, h * LANES : (h + 1) * LANES].astype(BF)
@@ -716,6 +727,7 @@
             [ANY] + [VMEM] * 12,
             scratch=[
                 pltpu.VMEM((S, qc), F32),
+                pltpu.VMEM((S, qc), F32),
                 pltpu.VMEM((S, vc), F32),
                 pltpu.SMEM((S,), jnp.int32),
             ],

time: 69.9 us -> 69.8 us (level)
  no operation moved by 1% of the time
where the time goes in v9:
time: 69.8 us; the launch traced here: 69.6 us
  blocking collectives  41.1 us (59%)
  Pallas kernels  14 us (20%)
  starting transfers between devices  9.35 us (13%)
  waiting for transfers between devices  4.92 us (7%)
    all_to_all x1, blocking collectives, on_device(): pieces = lax.all_to_all(pieces, 'kv', 0, 0, tiled=True)  10.9 us
    all_to_all x1, blocking collectives, on_device(): gated = lax.all_to_all(gated, ('kv', 'tp'), 0, 0, tiled=True)  10.3 us
    all_to_all x1, blocking collectives, on_device(): spread = lax.all_to_all(spread, ('kv', 'tp'), 0, 0, tiled=True)  9.97 us
    all_to_all x1, blocking collectives, on_device(): down = lax.all_to_all(down, ('kv', 'tp'), 0, 0, tiled=True)  9.97 us
    ppermute x6, starting transfers between devices, exchange(): got.append(lax.ppermute(message, 'kv', pairs))  8.84 us
    pallas_call x1, Pallas kernels, on_device(): call(cache_load_kernel, (sds(key_cache.shape, BF), sds(value_cache.shape,...  4.29 us
    ppermute x6, waiting for transfers between devices, exchange(): got.append(lax.ppermute(message, 'kv', pairs))  3.55 us
    pallas_call x1, Pallas kernels, on_device(): call(functools.partial(attend_kernel, width), sds((H, 3 * S + S // 2, LAN...  2.95 us
  transfers between devices with their start and end apart: 8, of which 3 were waited for; matrix products, arithmetic and copies ran while one was open for 0% of the time, Pallas kernels for 12%

profile of v9, /device:TPU:0, one launch (start us, length us, event | category | flops | bytes accessed | tf_op | source)
XLA Modules:
  0.0 69.6 jit_solution(5183480742796992043)
XLA Ops:
  0.0 0.5 collective-permute-start
  0.5 0.0 collective-permute-start.1
  0.5 1.1 %shard_map.145 = (bf16[256,1024]{1,0:T(8,128)(2,1)S(1)}, bf16[16,128]{1,0:T(8,128)(2,1)S(1)}, bf16[2,128]{1,0:T(2,128)(2,1)S(1)}, s32[16,128]{1,0:T(8,128)S(1)}, f32[16,128]{1,0:T(8,128)S(1)}) custom-call(bf16[256,1024]{1,0:T(8,128)(2,1)} %w_query.1, bf16[16,128]{1,0:T(8,128)(2,1)} %tokens.1, bf16[2,128]{1,0:T(2,128)(2,1)} %bitcast.5, s32[16]{0:T(128)} %lengths.1, ...), custom_call_target="tpu_custom_call" | custom-call | flops 1000000000 | tf_op jit(solution)/shard_map/pallas_call | solution.py:649
  1.6 1.4 %collective-permute-done.1.second = bf16[16,128]{1,0:T(8,128)(2,1)S(1)} collective-permute-done((bf16[16,128]{1,0:T(8,128)(2,1)}, bf16[16,128]{1,0:T(8,128)(2,1)S(1)}, u32[]{:S(2)}, u32[]{:S(2)}) %collective-permute-start.1) | collective-permute-done | bytes 4128 | tf_op jit(solution)/shard_map/ppermute | solution.py:646
  3.0 0.2 shard_map.146
  3.2 2.9 %collective-permute-start.2 = (bf16[16,1280]{1,0:T(8,128)(2,1)S(1)}, bf16[16,1280]{1,0:T(8,128)(2,1)S(1)}, u32[]{:S(2)}, u32[]{:S(2)}) collective-permute-start(bf16[16,1280]{1,0:T(8,128)(2,1)S(1)} %get-tuple-element.30.after), channel_id=1, source_target_pairs={{0,2},{2,0},{4,6},{6,4},{8,10},{10,8},{12,14},{14,12},{16,18},{18,... | collective-permute-start | bytes 122888 | tf_op jit(solution)/shard_map/ppermute | solution.py:677
  6.1 1.5 %collective-permute-start.3 = (bf16[16,1280]{1,0:T(8,128)(2,1)S(1)}, bf16[16,1280]{1,0:T(8,128)(2,1)S(1)}, u32[]{:S(2)}, u32[]{:S(2)}) collective-permute-start(bf16[16,1280]{1,0:T(8,128)(2,1)S(1)} %get-tuple-element.30.after), channel_id=1, source_target_pairs={{0,4},{2,6},{4,0},{6,2},{8,12},{10,14},{12,8},{14,10},{16,20},{18,... | collective-permute-start | bytes 122888 | tf_op jit(solution)/shard_map/ppermute | solution.py:677
  7.6 0.0 collective-permute-start.4
  7.7 2.6 %shard_map.148 = (f32[24,1024]{1,0:T(8,128)S(1)}, f32[24,2048]{1,0:T(8,128)S(1)}, f32[24,2048]{1,0:T(8,128)S(1)}, f32[2,16,128]{2,1,0:T(8,128)S(1)}, f32[16,16,1...) custom-call(bf16[16,1280]{1,0:T(8,128)(2,1)S(1)} %get-tuple-element.30.after, ...), custom_call_target="tpu_custom_call" | custom-call | flops 1000000000 | tf_op jit(solution)/shard_map/pallas_call | solution.py:681
  10.2 0.0 collective-permute-done.2.m1
  10.2 0.0 collective-permute-done.3.m2
  10.3 2.3 %collective-permute-done.4.m3 = bf16[16,1280]{1,0:T(8,128)(2,1)S(1)} collective-permute-done((bf16[16,1280]{1,0:T(8,128)(2,1)S(1)}, bf16[16,1280]{1,0:T(8,128)(2,1)S(1)}, u32[]{:S(2)}, u32[]{:S(2)}) %collective-permute-start.4) | collective-permute-done | bytes 40992 | tf_op jit(solution)/shard_map/ppermute | solution.py:677
  12.5 0.2 shard_map.147
  12.7 1.6 %collective-permute-start.5 = (bf16[16,1280]{1,0:T(8,128)(2,1)S(1)}, bf16[16,1280]{1,0:T(8,128)(2,1)S(1)}, u32[]{:S(2)}, u32[]{:S(2)}) collective-permute-start(bf16[16,1280]{1,0:T(8,128)(2,1)S(1)} %get-tuple-element.32.after), channel_id=1, source_target_pairs={{0,8},{2,10},{4,12},{6,14},{8,0},{10,2},{12,4},{14,6},{16,24},{18,... | collective-permute-start | bytes 122888 | tf_op jit(solution)/shard_map/ppermute | solution.py:677
  14.3 2.6 %collective-permute-start.6 = (bf16[16,1280]{1,0:T(8,128)(2,1)S(1)}, bf16[16,1280]{1,0:T(8,128)(2,1)S(1)}, u32[]{:S(2)}, u32[]{:S(2)}) collective-permute-start(bf16[16,1280]{1,0:T(8,128)(2,1)S(1)} %get-tuple-element.32.after), channel_id=1, source_target_pairs={{0,16},{2,18},{4,20},{6,22},{8,24},{10,26},{12,28},{14,30},{16,0},... | collective-permute-start | bytes 122888 | tf_op jit(solution)/shard_map/ppermute | solution.py:677
  16.9 0.2 collective-permute-start.7
  17.1 4.3 %shard_map.149 = (bf16[16,128,1024]{2,1,0:T(8,128)(2,1)S(1)}, bf16[16,128,2048]{2,1,0:T(8,128)(2,1)S(1)}) custom-call(bf16[16,1280]{1,0:T(8,128)(2,1)S(1)} %get-tuple-element.32.after, s32[16,128]{1,0:T(8,128)S(1)} %get-tuple-element.25.lengths, bf16[16,128,1024]{2,1,0:T(8,128)(2,1)} %keys.3, ...), custom_call_target="tpu_custom_call", output_to_operand_aliasing={{0}: (4, {})} | custom-call | flops 1000000000 | tf_op jit(solution)/shard_map/pallas_call | solution.py:714
  21.4 0.0 collective-permute-done.5.m1
  21.4 0.0 collective-permute-done.6.m2
  21.4 1.3 %collective-permute-done.7.m3 = bf16[16,1280]{1,0:T(8,128)(2,1)S(1)} collective-permute-done((bf16[16,1280]{1,0:T(8,128)(2,1)S(1)}, bf16[16,1280]{1,0:T(8,128)(2,1)S(1)}, u32[]{:S(2)}, u32[]{:S(2)}) %collective-permute-start.7) | collective-permute-done | bytes 40992 | tf_op jit(solution)/shard_map/ppermute | solution.py:677
  22.7 0.0 collective-permute-done.after.w_got
  22.7 0.0 copy-start.2
  22.7 3.0 %shard_map.150 = bf16[16,56,128]{2,1,0:T(8,128)(2,1)S(1)} custom-call(bf16[2048,256]{1,0:T(8,128)(2,1)S(1)} %collective-permute-done.after.w_got, s32[16,128]{1,0:T(8,128)S(1)} %get-tuple-element.25.lengths, f32[16,1280]{1,0:T(8,128)S(1)} %get-tuple-element.31.old, bf16[16,1280]{1,0:T(8,128)(2,1)S(1)} %collective-permute-done.5.m1, ...), custom_call_target="tpu_custom_call" | custom-call | tf_op jit(solution)/shard_map/pallas_call | solution.py:724
  25.7 10.9 %all_to_all.20.pieces = bf16[16,56,128]{2,1,0:T(8,128)(2,1)S(1)} all-to-all(bf16[16,56,128]{2,1,0:T(8,128)(2,1)S(1)} %shard_map.150), channel_id=1, replica_groups=mesh['kv'=16,'tp'=2] {'kv'}, dimensions={0} | all-to-all | bytes 458752 | tf_op jit(solution)/shard_map/all_to_all | solution.py:737
  36.6 0.4 shard_map.151
  37.0 10.3 %all_to_all.21.gated = bf16[32,16,128]{2,1,0:T(8,128)(2,1)S(1)} all-to-all(bf16[32,16,128]{2,1,0:T(8,128)(2,1)S(1)} %shard_map.151), channel_id=1, replica_groups=mesh['kv'=16,'tp'=2] {'kv','tp'}, dimensions={0} | all-to-all | bytes 262144 | tf_op jit(solution)/shard_map/all_to_all | solution.py:741
  47.3 0.3 shard_map.152
  47.5 10.0 %all_to_all.22.residual = bf16[32,16,128]{2,1,0:T(8,128)(2,1)S(1)} all-to-all(bf16[32,16,128]{2,1,0:T(8,128)(2,1)S(1)} %get-tuple-element.43), channel_id=1, replica_groups=mesh['kv'=16,'tp'=2] {'kv','tp'}, dimensions={0} | all-to-all | bytes 262144 | tf_op jit(solution)/shard_map/all_to_all | solution.py:748
  57.5 0.0 copy-done
  57.5 1.5 %shard_map.153 = bf16[32,16,128]{2,1,0:T(8,128)(2,1)S(1)} custom-call(bf16[32,16,128]{2,1,0:T(8,128)(2,1)S(1)} %all_to_all.22.residual, bf16[32,128]{1,0:T(8,128)(2,1)S(1)} %bitcast.3, bf16[4096,512]{1,0:T(8,128)(2,1)S(1)} %copy-done, bf16[512,4096]{1,0:T(8,128)(2,1)S(1)} %copy-done.1), custom_call_target="tpu_custom_call" | custom-call | tf_op jit(solution)/shard_map/pallas_call | solution.py:749
  59.0 10.0 %all_to_all.23.pieces = bf16[32,16,128]{2,1,0:T(8,128)(2,1)S(1)} all-to-all(bf16[32,16,128]{2,1,0:T(8,128)(2,1)S(1)} %shard_map.153), channel_id=1, replica_groups=mesh['kv'=16,'tp'=2] {'kv','tp'}, dimensions={0} | all-to-all | bytes 262144 | tf_op jit(solution)/shard_map/all_to_all | solution.py:752
  68.9 0.6 shard_map.154
  (6 shorter events, 0.0 us)
Async XLA Ops:
  0.0 22.7 %collective-permute-start = (bf16[2048,256]{1,0:T(8,128)(2,1)}, bf16[2048,256]{1,0:T(8,128)(2,1)S(1)}, u32[]{:S(2)}, u32[]{:S(2)}) collective-permute-start(bf16[2048,256]{1,0:T(8,128)(2,1)} %w_output.1), channel_id=1, source_target_pairs={{0,1},{1,0},{2,3},{3,2},{4,5},{5,4},{6,7},{7,6},{8,9},{9,8},{10,11... | collective-permute-start | bytes 3145736 | tf_op jit(solution)/shard_map/ppermute | solution.py:647
  0.5 2.5 %collective-permute-start.1 = (bf16[16,128]{1,0:T(8,128)(2,1)}, bf16[16,128]{1,0:T(8,128)(2,1)S(1)}, u32[]{:S(2)}, u32[]{:S(2)}) collective-permute-start(bf16[16,128]{1,0:T(8,128)(2,1)} %tokens.1), channel_id=1, source_target_pairs={{0,1},{1,0},{2,3},{3,2},{4,5},{5,4},{6,7},{7,6},{8,9},{9,8},{10,11... | collective-permute-start | bytes 12296 | tf_op jit(solution)/shard_map/ppermute | solution.py:646
  3.2 7.0 %collective-permute-start.2 = (bf16[16,1280]{1,0:T(8,128)(2,1)S(1)}, bf16[16,1280]{1,0:T(8,128)(2,1)S(1)}, u32[]{:S(2)}, u32[]{:S(2)}) collective-permute-start(bf16[16,1280]{1,0:T(8,128)(2,1)S(1)} %get-tuple-element.30.after), channel_id=1, source_target_pairs={{0,2},{2,0},{4,6},{6,4},{8,10},{10,8},{12,14},{14,12},{16,18},{18,... | collective-permute-start | bytes 122888 | tf_op jit(solution)/shard_map/ppermute | solution.py:677
  6.1 4.1 %collective-permute-start.3 = (bf16[16,1280]{1,0:T(8,128)(2,1)S(1)}, bf16[16,1280]{1,0:T(8,128)(2,1)S(1)}, u32[]{:S(2)}, u32[]{:S(2)}) collective-permute-start(bf16[16,1280]{1,0:T(8,128)(2,1)S(1)} %get-tuple-element.30.after), channel_id=1, source_target_pairs={{0,4},{2,6},{4,0},{6,2},{8,12},{10,14},{12,8},{14,10},{16,20},{18,... | collective-permute-start | bytes 122888 | tf_op jit(solution)/shard_map/ppermute | solution.py:677
  7.6 4.9 %collective-permute-start.4 = (bf16[16,1280]{1,0:T(8,128)(2,1)S(1)}, bf16[16,1280]{1,0:T(8,128)(2,1)S(1)}, u32[]{:S(2)}, u32[]{:S(2)}) collective-permute-start(bf16[16,1280]{1,0:T(8,128)(2,1)S(1)} %get-tuple-element.30.after), channel_id=1, source_target_pairs={{0,6},{2,4},{4,2},{6,0},{8,14},{10,12},{12,10},{14,8},{16,22},{18,... | collective-permute-start | bytes 122888 | tf_op jit(solution)/shard_map/ppermute | solution.py:677
  12.7 8.7 %collective-permute-start.5 = (bf16[16,1280]{1,0:T(8,128)(2,1)S(1)}, bf16[16,1280]{1,0:T(8,128)(2,1)S(1)}, u32[]{:S(2)}, u32[]{:S(2)}) collective-permute-start(bf16[16,1280]{1,0:T(8,128)(2,1)S(1)} %get-tuple-element.32.after), channel_id=1, source_target_pairs={{0,8},{2,10},{4,12},{6,14},{8,0},{10,2},{12,4},{14,6},{16,24},{18,... | collective-permute-start | bytes 122888 | tf_op jit(solution)/shard_map/ppermute | solution.py:677
  14.3 7.1 %collective-permute-start.6 = (bf16[16,1280]{1,0:T(8,128)(2,1)S(1)}, bf16[16,1280]{1,0:T(8,128)(2,1)S(1)}, u32[]{:S(2)}, u32[]{:S(2)}) collective-permute-start(bf16[16,1280]{1,0:T(8,128)(2,1)S(1)} %get-tuple-element.32.after), channel_id=1, source_target_pairs={{0,16},{2,18},{4,20},{6,22},{8,24},{10,26},{12,28},{14,30},{16,0},... | collective-permute-start | bytes 122888 | tf_op jit(solution)/shard_map/ppermute | solution.py:677
  16.9 5.8 %collective-permute-start.7 = (bf16[16,1280]{1,0:T(8,128)(2,1)S(1)}, bf16[16,1280]{1,0:T(8,128)(2,1)S(1)}, u32[]{:S(2)}, u32[]{:S(2)}) collective-permute-start(bf16[16,1280]{1,0:T(8,128)(2,1)S(1)} %get-tuple-element.32.after), channel_id=1, source_target_pairs={{0,24},{2,26},{4,28},{6,30},{8,16},{10,18},{12,20},{14,22},{16,8},... | collective-permute-start | bytes 122888 | tf_op jit(solution)/shard_map/ppermute | solution.py:677
  22.7 13.9 %copy-start.3 = (bf16[2048]{0:T(1024)(128)(2,1)S(1)}, bf16[2048]{0:T(1024)(128)(2,1)}, u32[]{:S(2)}) copy-start(bf16[2048]{0:T(1024)(128)(2,1)} %param.25) | copy-start | bytes 12292
  22.7 34.8 %copy-start = (bf16[4096,512]{1,0:T(8,128)(2,1)S(1)}, bf16[4096,512]{1,0:T(8,128)(2,1)}, u32[]{:S(2)}) copy-start(bf16[4096,512]{1,0:T(8,128)(2,1)} %w_up.1) | copy-start | bytes 12582916
  22.7 34.8 %copy-start.1 = (bf16[512,4096]{1,0:T(8,128)(2,1)S(1)}, bf16[512,4096]{1,0:T(8,128)(2,1)}, u32[]{:S(2)}) copy-start(bf16[512,4096]{1,0:T(8,128)(2,1)} %w_down.1) | copy-start | bytes 12582916
  22.7 34.8 %copy-start.2 = (bf16[4096]{0:T(1024)(128)(2,1)S(1)}, bf16[4096]{0:T(1024)(128)(2,1)}, u32[]{:S(2)}) copy-start(bf16[4096]{0:T(1024)(128)(2,1)} %param.27) | copy-start | bytes 24580

commit v10 on v9

--- a/solution.py
+++ b/solution.py
@@ -321,7 +321,7 @@
 ):
     rows, span = keys.shape[:2]
     live = live_scalars(lengths, lax.axis_index("kv") * span)
-    half = rows // 2
+    half = rows * 3 // 4
     copies = copies_of(keys, keys_out, key_sems, half, rows - half)
     copies += copies_of(values, values_out, value_sems, 0, rows)
     when_live(live[half:] + live, copies, lambda copy: copy.start())
@@ -392,8 +392,8 @@
         copy.start()
     lhs, wide = projection_rows(first, second, gain)
     rows = wide.shape[0]
-    live = live_scalars(lengths, lax.axis_index("kv") * keys.shape[1])[: rows // 2]
-    caches = copies_of(keys, keys_out, cache_sems, 0, rows // 2)
+    live = live_scalars(lengths, lax.axis_index("kv") * keys.shape[1])[: rows * 3 // 4]
+    caches = copies_of(keys, keys_out, cache_sems, 0, rows * 3 // 4)
     when_live(live, caches, lambda copy: copy.start())
     half = HEAD_KEY // 2
     entry = (lane_ids(rows) % half).astype(F32)
@@ -692,7 +692,7 @@
             [ANY] + [VMEM] * 5 + [HBM] * 5,
             flops=10**9,
             scratch=[pltpu.VMEM(w.shape, BF) for w in (w_key, w_value, w_gate)]
-            + [pltpu.SemaphoreType.DMA((4,)), pltpu.SemaphoreType.DMA((S // 2,))],
+            + [pltpu.SemaphoreType.DMA((4,)), pltpu.SemaphoreType.DMA((S,))],
             limit=6 * mib,
         )(
             message,

time: 69.8 us -> 69.8 us (level)
  no operation moved by 1% of the time
where the time goes in v10:
time: 69.8 us; the launch traced here: 69.6 us
  blocking collectives  41.1 us (59%)
  Pallas kernels  14.1 us (20%)
  starting transfers between devices  9.35 us (13%)
  waiting for transfers between devices  4.83 us (7%)
    all_to_all x1, blocking collectives, on_device(): pieces = lax.all_to_all(pieces, 'kv', 0, 0, tiled=True)  10.9 us
    all_to_all x1, blocking collectives, on_device(): gated = lax.all_to_all(gated, ('kv', 'tp'), 0, 0, tiled=True)  10.3 us
    all_to_all x1, blocking collectives, on_device(): spread = lax.all_to_all(spread, ('kv', 'tp'), 0, 0, tiled=True)  9.97 us
    all_to_all x1, blocking collectives, on_device(): down = lax.all_to_all(down, ('kv', 'tp'), 0, 0, tiled=True)  9.97 us
    ppermute x6, starting transfers between devices, exchange(): got.append(lax.ppermute(message, 'kv', pairs))  8.84 us
    pallas_call x1, Pallas kernels, on_device(): call(cache_load_kernel, (sds(key_cache.shape, BF), sds(value_cache.shape,...  3.99 us
    ppermute x6, waiting for transfers between devices, exchange(): got.append(lax.ppermute(message, 'kv', pairs))  3.47 us
    pallas_call x1, Pallas kernels, on_device(): call(functools.partial(attend_kernel, width), sds((H, 3 * S + S // 2, LAN...  2.95 us
  transfers between devices with their start and end apart: 8, of which 3 were waited for; matrix products, arithmetic and copies ran while one was open for 0% of the time, Pallas kernels for 12%

profile of v10, /device:TPU:0, one launch (start us, length us, event | category | flops | bytes accessed | tf_op | source)
XLA Modules:
  0.0 69.6 jit_solution(12142148213987761912)
XLA Ops:
  0.0 0.5 collective-permute-start
  0.5 0.0 collective-permute-start.1
  0.5 1.1 %shard_map.145 = (bf16[256,1024]{1,0:T(8,128)(2,1)S(1)}, bf16[16,128]{1,0:T(8,128)(2,1)S(1)}, bf16[2,128]{1,0:T(2,128)(2,1)S(1)}, s32[16,128]{1,0:T(8,128)S(1)}, f32[16,128]{1,0:T(8,128)S(1)}) custom-call(bf16[256,1024]{1,0:T(8,128)(2,1)} %w_query.1, bf16[16,128]{1,0:T(8,128)(2,1)} %tokens.1, bf16[2,128]{1,0:T(2,128)(2,1)} %bitcast.5, s32[16]{0:T(128)} %lengths.1, ...), custom_call_target="tpu_custom_call" | custom-call | flops 1000000000 | tf_op jit(solution)/shard_map/pallas_call | solution.py:649
  1.6 1.4 %collective-permute-done.1.second = bf16[16,128]{1,0:T(8,128)(2,1)S(1)} collective-permute-done((bf16[16,128]{1,0:T(8,128)(2,1)}, bf16[16,128]{1,0:T(8,128)(2,1)S(1)}, u32[]{:S(2)}, u32[]{:S(2)}) %collective-permute-start.1) | collective-permute-done | bytes 4128 | tf_op jit(solution)/shard_map/ppermute | solution.py:646
  3.0 0.2 shard_map.146
  3.2 2.9 %collective-permute-start.2 = (bf16[16,1280]{1,0:T(8,128)(2,1)S(1)}, bf16[16,1280]{1,0:T(8,128)(2,1)S(1)}, u32[]{:S(2)}, u32[]{:S(2)}) collective-permute-start(bf16[16,1280]{1,0:T(8,128)(2,1)S(1)} %get-tuple-element.30.after), channel_id=1, source_target_pairs={{0,2},{2,0},{4,6},{6,4},{8,10},{10,8},{12,14},{14,12},{16,18},{18,... | collective-permute-start | bytes 122888 | tf_op jit(solution)/shard_map/ppermute | solution.py:677
  6.1 1.5 %collective-permute-start.3 = (bf16[16,1280]{1,0:T(8,128)(2,1)S(1)}, bf16[16,1280]{1,0:T(8,128)(2,1)S(1)}, u32[]{:S(2)}, u32[]{:S(2)}) collective-permute-start(bf16[16,1280]{1,0:T(8,128)(2,1)S(1)} %get-tuple-element.30.after), channel_id=1, source_target_pairs={{0,4},{2,6},{4,0},{6,2},{8,12},{10,14},{12,8},{14,10},{16,20},{18,... | collective-permute-start | bytes 122888 | tf_op jit(solution)/shard_map/ppermute | solution.py:677
  7.6 0.0 collective-permute-start.4
  7.7 2.9 %shard_map.148 = (f32[24,1024]{1,0:T(8,128)S(1)}, f32[24,2048]{1,0:T(8,128)S(1)}, f32[24,2048]{1,0:T(8,128)S(1)}, f32[2,16,128]{2,1,0:T(8,128)S(1)}, f32[16,16,1...) custom-call(bf16[16,1280]{1,0:T(8,128)(2,1)S(1)} %get-tuple-element.30.after, ...), custom_call_target="tpu_custom_call" | custom-call | flops 1000000000 | tf_op jit(solution)/shard_map/pallas_call | solution.py:681
  10.6 0.0 collective-permute-done.2.m1
  10.6 0.0 collective-permute-done.3.m2
  10.6 1.9 %collective-permute-done.4.m3 = bf16[16,1280]{1,0:T(8,128)(2,1)S(1)} collective-permute-done((bf16[16,1280]{1,0:T(8,128)(2,1)S(1)}, bf16[16,1280]{1,0:T(8,128)(2,1)S(1)}, u32[]{:S(2)}, u32[]{:S(2)}) %collective-permute-start.4) | collective-permute-done | bytes 40992 | tf_op jit(solution)/shard_map/ppermute | solution.py:677
  12.5 0.2 shard_map.147
  12.7 1.6 %collective-permute-start.5 = (bf16[16,1280]{1,0:T(8,128)(2,1)S(1)}, bf16[16,1280]{1,0:T(8,128)(2,1)S(1)}, u32[]{:S(2)}, u32[]{:S(2)}) collective-permute-start(bf16[16,1280]{1,0:T(8,128)(2,1)S(1)} %get-tuple-element.32.after), channel_id=1, source_target_pairs={{0,8},{2,10},{4,12},{6,14},{8,0},{10,2},{12,4},{14,6},{16,24},{18,... | collective-permute-start | bytes 122888 | tf_op jit(solution)/shard_map/ppermute | solution.py:677
  14.3 2.6 %collective-permute-start.6 = (bf16[16,1280]{1,0:T(8,128)(2,1)S(1)}, bf16[16,1280]{1,0:T(8,128)(2,1)S(1)}, u32[]{:S(2)}, u32[]{:S(2)}) collective-permute-start(bf16[16,1280]{1,0:T(8,128)(2,1)S(1)} %get-tuple-element.32.after), channel_id=1, source_target_pairs={{0,16},{2,18},{4,20},{6,22},{8,24},{10,26},{12,28},{14,30},{16,0},... | collective-permute-start | bytes 122888 | tf_op jit(solution)/shard_map/ppermute | solution.py:677
  16.9 0.2 collective-permute-start.7
  17.1 4.0 %shard_map.149 = (bf16[16,128,1024]{2,1,0:T(8,128)(2,1)S(1)}, bf16[16,128,2048]{2,1,0:T(8,128)(2,1)S(1)}) custom-call(bf16[16,1280]{1,0:T(8,128)(2,1)S(1)} %get-tuple-element.32.after, s32[16,128]{1,0:T(8,128)S(1)} %get-tuple-element.25.lengths, bf16[16,128,1024]{2,1,0:T(8,128)(2,1)} %keys.3, ...), custom_call_target="tpu_custom_call", output_to_operand_aliasing={{0}: (4, {})} | custom-call | flops 1000000000 | tf_op jit(solution)/shard_map/pallas_call | solution.py:714
  21.1 0.0 collective-permute-done.5.m1
  21.1 0.0 collective-permute-done.6.m2
  21.1 1.6 %collective-permute-done.7.m3 = bf16[16,1280]{1,0:T(8,128)(2,1)S(1)} collective-permute-done((bf16[16,1280]{1,0:T(8,128)(2,1)S(1)}, bf16[16,1280]{1,0:T(8,128)(2,1)S(1)}, u32[]{:S(2)}, u32[]{:S(2)}) %collective-permute-start.7) | collective-permute-done | bytes 40992 | tf_op jit(solution)/shard_map/ppermute | solution.py:677
  22.7 0.0 collective-permute-done.after.w_got
  22.7 0.0 copy-start.2
  22.7 3.0 %shard_map.150 = bf16[16,56,128]{2,1,0:T(8,128)(2,1)S(1)} custom-call(bf16[2048,256]{1,0:T(8,128)(2,1)S(1)} %collective-permute-done.after.w_got, s32[16,128]{1,0:T(8,128)S(1)} %get-tuple-element.25.lengths, f32[16,1280]{1,0:T(8,128)S(1)} %get-tuple-element.31.old, bf16[16,1280]{1,0:T(8,128)(2,1)S(1)} %collective-permute-done.5.m1, ...), custom_call_target="tpu_custom_call" | custom-call | tf_op jit(solution)/shard_map/pallas_call | solution.py:724
  25.7 10.9 %all_to_all.20.pieces = bf16[16,56,128]{2,1,0:T(8,128)(2,1)S(1)} all-to-all(bf16[16,56,128]{2,1,0:T(8,128)(2,1)S(1)} %shard_map.150), channel_id=1, replica_groups=mesh['kv'=16,'tp'=2] {'kv'}, dimensions={0} | all-to-all | bytes 458752 | tf_op jit(solution)/shard_map/all_to_all | solution.py:737
  36.6 0.4 shard_map.151
  37.0 10.3 %all_to_all.21.gated = bf16[32,16,128]{2,1,0:T(8,128)(2,1)S(1)} all-to-all(bf16[32,16,128]{2,1,0:T(8,128)(2,1)S(1)} %shard_map.151), channel_id=1, replica_groups=mesh['kv'=16,'tp'=2] {'kv','tp'}, dimensions={0} | all-to-all | bytes 262144 | tf_op jit(solution)/shard_map/all_to_all | solution.py:741
  47.3 0.3 shard_map.152
  47.5 10.0 %all_to_all.22.residual = bf16[32,16,128]{2,1,0:T(8,128)(2,1)S(1)} all-to-all(bf16[32,16,128]{2,1,0:T(8,128)(2,1)S(1)} %get-tuple-element.43), channel_id=1, replica_groups=mesh['kv'=16,'tp'=2] {'kv','tp'}, dimensions={0} | all-to-all | bytes 262144 | tf_op jit(solution)/shard_map/all_to_all | solution.py:748
  57.5 0.0 copy-done
  57.5 1.5 %shard_map.153 = bf16[32,16,128]{2,1,0:T(8,128)(2,1)S(1)} custom-call(bf16[32,16,128]{2,1,0:T(8,128)(2,1)S(1)} %all_to_all.22.residual, bf16[32,128]{1,0:T(8,128)(2,1)S(1)} %bitcast.3, bf16[4096,512]{1,0:T(8,128)(2,1)S(1)} %copy-done, bf16[512,4096]{1,0:T(8,128)(2,1)S(1)} %copy-done.1), custom_call_target="tpu_custom_call" | custom-call | tf_op jit(solution)/shard_map/pallas_call | solution.py:749
  59.0 10.0 %all_to_all.23.pieces = bf16[32,16,128]{2,1,0:T(8,128)(2,1)S(1)} all-to-all(bf16[32,16,128]{2,1,0:T(8,128)(2,1)S(1)} %shard_map.153), channel_id=1, replica_groups=mesh['kv'=16,'tp'=2] {'kv','tp'}, dimensions={0} | all-to-all | bytes 262144 | tf_op jit(solution)/shard_map/all_to_all | solution.py:752
  68.9 0.6 shard_map.154
  (6 shorter events, 0.0 us)
Async XLA Ops:
  0.0 22.7 %collective-permute-start = (bf16[2048,256]{1,0:T(8,128)(2,1)}, bf16[2048,256]{1,0:T(8,128)(2,1)S(1)}, u32[]{:S(2)}, u32[]{:S(2)}) collective-permute-start(bf16[2048,256]{1,0:T(8,128)(2,1)} %w_output.1), channel_id=1, source_target_pairs={{0,1},{1,0},{2,3},{3,2},{4,5},{5,4},{6,7},{7,6},{8,9},{9,8},{10,11... | collective-permute-start | bytes 3145736 | tf_op jit(solution)/shard_map/ppermute | solution.py:647
  0.5 2.5 %collective-permute-start.1 = (bf16[16,128]{1,0:T(8,128)(2,1)}, bf16[16,128]{1,0:T(8,128)(2,1)S(1)}, u32[]{:S(2)}, u32[]{:S(2)}) collective-permute-start(bf16[16,128]{1,0:T(8,128)(2,1)} %tokens.1), channel_id=1, source_target_pairs={{0,1},{1,0},{2,3},{3,2},{4,5},{5,4},{6,7},{7,6},{8,9},{9,8},{10,11... | collective-permute-start | bytes 12296 | tf_op jit(solution)/shard_map/ppermute | solution.py:646
  3.2 7.4 %collective-permute-start.2 = (bf16[16,1280]{1,0:T(8,128)(2,1)S(1)}, bf16[16,1280]{1,0:T(8,128)(2,1)S(1)}, u32[]{:S(2)}, u32[]{:S(2)}) collective-permute-start(bf16[16,1280]{1,0:T(8,128)(2,1)S(1)} %get-tuple-element.30.after), channel_id=1, source_target_pairs={{0,2},{2,0},{4,6},{6,4},{8,10},{10,8},{12,14},{14,12},{16,18},{18,... | collective-permute-start | bytes 122888 | tf_op jit(solution)/shard_map/ppermute | solution.py:677
  6.1 4.5 %collective-permute-start.3 = (bf16[16,1280]{1,0:T(8,128)(2,1)S(1)}, bf16[16,1280]{1,0:T(8,128)(2,1)S(1)}, u32[]{:S(2)}, u32[]{:S(2)}) collective-permute-start(bf16[16,1280]{1,0:T(8,128)(2,1)S(1)} %get-tuple-element.30.after), channel_id=1, source_target_pairs={{0,4},{2,6},{4,0},{6,2},{8,12},{10,14},{12,8},{14,10},{16,20},{18,... | collective-permute-start | bytes 122888 | tf_op jit(solution)/shard_map/ppermute | solution.py:677
  7.6 4.9 %collective-permute-start.4 = (bf16[16,1280]{1,0:T(8,128)(2,1)S(1)}, bf16[16,1280]{1,0:T(8,128)(2,1)S(1)}, u32[]{:S(2)}, u32[]{:S(2)}) collective-permute-start(bf16[16,1280]{1,0:T(8,128)(2,1)S(1)} %get-tuple-element.30.after), channel_id=1, source_target_pairs={{0,6},{2,4},{4,2},{6,0},{8,14},{10,12},{12,10},{14,8},{16,22},{18,... | collective-permute-start | bytes 122888 | tf_op jit(solution)/shard_map/ppermute | solution.py:677
  12.7 8.4 %collective-permute-start.5 = (bf16[16,1280]{1,0:T(8,128)(2,1)S(1)}, bf16[16,1280]{1,0:T(8,128)(2,1)S(1)}, u32[]{:S(2)}, u32[]{:S(2)}) collective-permute-start(bf16[16,1280]{1,0:T(8,128)(2,1)S(1)} %get-tuple-element.32.after), channel_id=1, source_target_pairs={{0,8},{2,10},{4,12},{6,14},{8,0},{10,2},{12,4},{14,6},{16,24},{18,... | collective-permute-start | bytes 122888 | tf_op jit(solution)/shard_map/ppermute | solution.py:677
  14.3 6.8 %collective-permute-start.6 = (bf16[16,1280]{1,0:T(8,128)(2,1)S(1)}, bf16[16,1280]{1,0:T(8,128)(2,1)S(1)}, u32[]{:S(2)}, u32[]{:S(2)}) collective-permute-start(bf16[16,1280]{1,0:T(8,128)(2,1)S(1)} %get-tuple-element.32.after), channel_id=1, source_target_pairs={{0,16},{2,18},{4,20},{6,22},{8,24},{10,26},{12,28},{14,30},{16,0},... | collective-permute-start | bytes 122888 | tf_op jit(solution)/shard_map/ppermute | solution.py:677
  16.9 5.8 %collective-permute-start.7 = (bf16[16,1280]{1,0:T(8,128)(2,1)S(1)}, bf16[16,1280]{1,0:T(8,128)(2,1)S(1)}, u32[]{:S(2)}, u32[]{:S(2)}) collective-permute-start(bf16[16,1280]{1,0:T(8,128)(2,1)S(1)} %get-tuple-element.32.after), channel_id=1, source_target_pairs={{0,24},{2,26},{4,28},{6,30},{8,16},{10,18},{12,20},{14,22},{16,8},... | collective-permute-start | bytes 122888 | tf_op jit(solution)/shard_map/ppermute | solution.py:677
  22.7 13.9 %copy-start.3 = (bf16[2048]{0:T(1024)(128)(2,1)S(1)}, bf16[2048]{0:T(1024)(128)(2,1)}, u32[]{:S(2)}) copy-start(bf16[2048]{0:T(1024)(128)(2,1)} %param.25) | copy-start | bytes 12292
  22.7 34.8 %copy-start = (bf16[4096,512]{1,0:T(8,128)(2,1)S(1)}, bf16[4096,512]{1,0:T(8,128)(2,1)}, u32[]{:S(2)}) copy-start(bf16[4096,512]{1,0:T(8,128)(2,1)} %w_up.1) | copy-start | bytes 12582916
  22.7 34.8 %copy-start.1 = (bf16[512,4096]{1,0:T(8,128)(2,1)S(1)}, bf16[512,4096]{1,0:T(8,128)(2,1)}, u32[]{:S(2)}) copy-start(bf16[512,4096]{1,0:T(8,128)(2,1)} %w_down.1) | copy-start | bytes 12582916
  22.7 34.8 %copy-start.2 = (bf16[4096]{0:T(1024)(128)(2,1)S(1)}, bf16[4096]{0:T(1024)(128)(2,1)}, u32[]{:S(2)}) copy-start(bf16[4096]{0:T(1024)(128)(2,1)} %param.27) | copy-start | bytes 24580
